TPU v7x, 512 devices: a whole 4x8x8 slice. The times are simulated.
512 devices in a mesh: fs: 128 (over z, y, core), tp: 4 (over x).
Axes of the slice: x: 4, y: 8, z: 8, core: 2. Of those that a mesh axis runs over, the one named last changes fastest.
Arguments:
- tokens: bfloat16 [16384, 2048], P('fs', 'tp'), may hold values from -6 to 6
- routes: int32 [16384, 2], P('fs'), may hold values from 0 to 127, all different within a row; in each aligned block of 128 rows (0 to 127, 128 to 255, ...) at most 3 rows name the same one
- route_weight: float32 [16384, 2], P('fs'), may hold values from 0.05 to 1
- gain: float32 [2048], P('fs'), may hold values from 0.1 to 1.9
- gate_weight: float32 [128, 2048, 512], P(None, 'fs', 'tp'), may hold values from -0.125 to 0.125
- up_weight: float32 [128, 2048, 512], P(None, 'fs', 'tp'), may hold values from -0.125 to 0.125
- down_weight: float32 [128, 512, 2048], P(None, 'tp', 'fs'), may hold values from -0.25 to 0.25
Outputs:
- gate_out: bfloat16 [128, 2048, 512], P('fs', None, 'tp')
- up_out: bfloat16 [128, 2048, 512], P('fs', None, 'tp')
- down_out: bfloat16 [128, 512, 2048], P('fs', 'tp')
- mixed: bfloat16 [16384, 2048], P('fs', 'tp')
Inputs may be any that keep to these rules, and one draw needn't show every extreme that they name: `routes`: each row names 2 different experts. Among the rows of one index of fs (aligned blocks of 128 rows) no expert is named more than 3 times, a bound that some block reaches.
All inputs are finite; a program needn't handle non-finite values.
Results may differ from a plain program's by a relative error of at most 0.0095.
Values may be sent and summed in bfloat16 or wider, within the bound.
No kernel may reach another device: no remote copies, remote signals or barrier semaphores. Data moves between devices by JAX's collectives and lax.ppermute only.
A program may use at most 64 MiB of HBM per device.

v0:
```python
import jax
import jax.numpy as jnp
from jax import lax
from jax.sharding import PartitionSpec as P


def side_by_side(arrays, axis, split_dim, concat_dim, along):
    widths = [a.shape[along] for a in arrays]
    both = jnp.concatenate(arrays, axis=along)
    out = lax.all_to_all(both, axis, split_axis=split_dim, concat_axis=concat_dim, tiled=True)
    return tuple(jnp.split(out, [sum(widths[:k]) for k in range(1, len(widths))], axis=along))


def in_order(tiles, dim):
    tiles = jnp.moveaxis(tiles, 0, dim)
    dims = tiles.shape
    return tiles.reshape(*dims[:dim], dims[dim] * dims[dim + 1], *dims[dim + 2 :])


def sent_to_all(value, axis):
    size = lax.axis_size(axis)
    return lax.all_to_all(
        jnp.broadcast_to(value[None], (size, *value.shape)), axis, 0, 0, tiled=True
    )


def gather_directly(value, axis, dim):
    return in_order(sent_to_all(value, axis), dim)


def normalize(rows):
    values = rows.astype(jnp.float32)
    return (values * lax.rsqrt(jnp.mean(values * values, axis=-1, keepdims=True) + 1e-06)).astype(
        jnp.bfloat16
    )


def local(tokens, routes, route_weight, gain, gate_weight, up_weight, down_weight):
    fs_count = lax.axis_size("fs")
    tp_count = lax.axis_size("tp")
    gain_rows = gain[None, :, None]
    gate_new = (gain_rows * gate_weight).astype(jnp.bfloat16)
    up_new = (gain_rows * up_weight).astype(jnp.bfloat16)
    gate_out, up_out = side_by_side((gate_new, up_new), "fs", 0, 1, 2)
    down_out = lax.all_to_all(
        down_weight.astype(jnp.bfloat16), "fs", split_axis=0, concat_axis=2, tiled=True
    )
    tok_rows, top = routes.shape
    capacity = min(tok_rows, max(2, 3 * tok_rows * top // (2 * fs_count)))
    flat = routes.reshape(-1)
    count = flat.shape[0]
    hits = (flat[:, None] == jnp.arange(fs_count, dtype=jnp.int32)[None, :]).astype(jnp.int32)
    ranks = jnp.sum((jnp.cumsum(hits, axis=0) - 1) * hits, axis=1)
    slots = flat * capacity + ranks
    source = jnp.full((fs_count * capacity,), count, jnp.int32)
    source = source.at[slots].set(jnp.arange(count, dtype=jnp.int32))
    filled = (source < count)[:, None]
    row_of = jnp.minimum(source // top, tok_rows - 1)
    packed = jnp.where(filled, tokens[row_of], jnp.zeros((), jnp.bfloat16))
    arrived = lax.all_to_all(
        packed.reshape(fs_count, capacity, -1), "fs", split_axis=0, concat_axis=0, tiled=True
    )
    arrived = lax.all_gather(arrived.reshape(fs_count * capacity, -1), "tp", axis=1, tiled=True)
    arrived = normalize(arrived)
    gate_act = jnp.dot(arrived, gate_out[0], preferred_element_type=jnp.float32)
    up_act = jnp.dot(arrived, up_out[0], preferred_element_type=jnp.float32)
    hidden = (jax.nn.silu(gate_act) * up_act).astype(jnp.bfloat16)
    slot_rows = hidden.shape[0]
    unit_rows = down_out.shape[1]
    hidden_all = gather_directly(hidden, "tp", 1)
    column_block = lax.all_to_all(
        down_out[0].reshape(unit_rows, tp_count, -1), "tp", split_axis=1, concat_axis=0, tiled=True
    )
    column_block = column_block.reshape(tp_count, unit_rows, -1)
    hidden_blocks = hidden_all.reshape(slot_rows, tp_count, unit_rows)
    partial_value = jnp.einsum(
        "sju,jud->sjd", hidden_blocks, column_block, preferred_element_type=jnp.float32
    ).astype(jnp.bfloat16)
    expert_out = jnp.sum(partial_value, axis=1, dtype=jnp.float32).astype(jnp.bfloat16)
    returned = lax.all_to_all(
        expert_out.reshape(fs_count, capacity, -1), "fs", split_axis=0, concat_axis=0, tiled=True
    )
    returned = returned.reshape(fs_count * capacity, -1)
    picked = returned[slots].reshape(tok_rows, top, -1)
    share = route_weight / jnp.sum(route_weight, axis=1, keepdims=True)
    mixed = jnp.sum(share[:, :, None] * picked.astype(jnp.float32), axis=1).astype(jnp.bfloat16)
    return (gate_out, up_out, down_out, mixed)


def solution(mesh):
    in_specs = (
        P("fs", "tp"),
        P("fs", None),
        P("fs", None),
        P("fs"),
        P(None, "fs", "tp"),
        P(None, "fs", "tp"),
        P(None, "tp", "fs"),
    )
    out_specs = (P("fs", None, "tp"), P("fs", None, "tp"), P("fs", "tp", None), P("fs", "tp"))
    return jax.shard_map(local, mesh=mesh, in_specs=in_specs, out_specs=out_specs, check_vma=False)
```

profile of v0, /device:TPU:1, one launch (start us, length us, event | category | flops | bytes accessed | tf_op | source)
XLA Modules:
  0.0 185.3 jit_solution(10691966583907754370)
XLA Ops:
  7.2 0.0 copy-start
  7.2 0.8 copy.15
  8.0 0.1 eq.29
  8.1 0.1 eq.25
  8.3 0.7 broadcast_multiply_fusion
  9.0 0.1 copy.17
  9.1 0.2 fusion.11
  9.3 0.1 add_add_fusion
  9.4 0.1 copy.14
  9.5 0.1 mul.65
  9.7 0.2 fusion.12
  9.9 1.4 scatter_custom_fusion
  11.3 0.0 copy-done
  11.3 2.1 %gather_fusion = bf16[384,512]{1,0:T(8,128)(2,1)S(1)} fusion(bf16[128,512]{1,0:T(8,128)(2,1)S(1)} %copy-done, s32[1024]{0:T(1024)S(1)} %pad_clamp_fusion.1), kind=kCustom, calls=%fused_computation | custom fusion | bytes 787968 | tf_op jit(solution)/shard_map/gather | solution.py:59
  13.4 0.0 copy-start.2
  13.4 0.2 gather.9
  13.6 0.2 broadcast_in_dim.18
  13.9 1.1 broadcast_select_fusion
  15.0 18.4 %all-to-all-start.2 = ((bf16[128,3,512]{2,1,0:T(4,128)(2,1)}), bf16[128,3,512]{2,1,0:T(4,128)(2,1)S(1)}, u32[]{:S(2)}, u32[]{:S(2)}) async-start(bf16[128,3,512]{2,1,0:T(4,128)(2,1)} %broadcast_select_fusion), calls=%async_computation.2 | async-start | bytes 1048576 | tf_op jit(solution)/shard_map/all_to_all | solution.py:60
  33.4 0.0 copy-done.2
  33.5 0.0 copy-start.3
  33.5 0.0 copy-start.8
  33.5 0.9 convert_element_type.40
  34.3 0.0 copy-start.4
  34.3 19.7 %all-to-all-done.2 = bf16[128,3,512]{2,1,0:T(4,128)(2,1)S(1)} async-done(((bf16[128,3,512]{2,1,0:T(4,128)(2,1)}), bf16[128,3,512]{2,1,0:T(4,128)(2,1)S(1)}, u32[]{:S(2)}, u32[]{:S(2)}) %all-to-all-start.2) | async-done | bytes 393248 | tf_op jit(solution)/shard_map/all_to_all | solution.py:60
  54.0 5.4 %all-to-all-start.1 = ((bf16[128,128,16]{1,2,0:T(8,128)(2,1)}), bf16[128,128,16]{1,2,0:T(8,128)(2,1)S(1)}, u32[]{:S(2)}, u32[]{:S(2)}) async-start(bf16[128,128,16]{1,2,0:T(8,128)(2,1)} %convert_element_type.40), calls=%async_computation.1 | async-start | bytes 1048576 | tf_op jit(solution)/shard_map/all_to_all | solution.py:45
  59.4 0.0 copy-done.3
  59.4 0.0 copy-done.8
  59.4 0.0 copy-done.4
  59.4 0.2 multiply_convert_fusion.1
  59.7 1.1 pad_maximum_fusion
  60.8 19.2 %all-to-all-done.1 = bf16[128,128,16]{1,2,0:T(8,128)(2,1)S(1)} async-done(((bf16[128,128,16]{1,2,0:T(8,128)(2,1)}), bf16[128,128,16]{1,2,0:T(8,128)(2,1)S(1)}, u32[]{:S(2)}, u32[]{:S(2)}) %all-to-all-start.1) | async-done | bytes 524320 | tf_op jit(solution)/shard_map/all_to_all | solution.py:45
  80.0 5.4 %all-to-all-start = ((bf16[128,16,256]{2,1,0:T(8,128)(2,1)}), bf16[128,16,256]{2,1,0:T(8,128)(2,1)S(1)}, u32[]{:S(2)}, u32[]{:S(2)}) async-start(bf16[128,16,256]{2,1,0:T(8,128)(2,1)} %pad_maximum_fusion), calls=%async_computation | async-start | bytes 2097152 | tf_op jit(solution)/shard_map/all_to_all | solution.py:10
  85.4 0.0 all-gather.2.cloned.1.call-start
  85.4 1.1 reshape.97
  86.5 0.0 all-gather.2.cloned.1.call-update
  86.5 1.0 copy.19
  87.5 28.8 %all-to-all-done = bf16[128,16,256]{2,1,0:T(8,128)(2,1)S(1)} async-done(((bf16[128,16,256]{2,1,0:T(8,128)(2,1)}), bf16[128,16,256]{2,1,0:T(8,128)(2,1)S(1)}, u32[]{:S(2)}, u32[]{:S(2)}) %all-to-all-start) | async-done | bytes 1048608 | tf_op jit(solution)/shard_map/all_to_all | solution.py:10
  116.3 4.0 %all-to-all-start.4 = ((bf16[128,4,512]{2,0,1:T(8,128)(2,1)}), bf16[128,4,512]{2,0,1:T(8,128)(2,1)S(1)}, u32[]{:S(2)}, u32[]{:S(2)}) async-start(bf16[128,4,512]{2,0,1:T(8,128)(2,1)} %copy.19), calls=%async_computation.4 | async-start | bytes 1048576 | tf_op jit(solution)/shard_map/all_to_all | solution.py:71
  120.4 0.1 fusion.20
  120.4 0.0 copy-start.6
  120.4 0.0 copy-start.5
  120.4 0.3 all-gather.2.cloned.1.call-done
  120.7 0.0 copy-start.1
  120.7 1.9 %fusion = f32[384]{0:T(512)S(1)} fusion(bf16[384,2048]{1,0:T(8,128)(2,1)} %all-gather.2.cloned.1.call-done), kind=kLoop, calls=%fused_computation.5 | loop fusion | flops 2358912 | bytes 1574400 | tf_op jit(solution)/shard_map/reduce_sum | solution.py:33
  122.6 0.0 copy-done.1
  122.7 0.6 fusion.5
  123.3 0.0 copy-done.6
  123.3 0.0 copy-done.5
  123.3 0.6 fusion.3
  124.0 5.5 %all-to-all-done.4 = bf16[128,4,512]{2,0,1:T(8,128)(2,1)S(1)} async-done(((bf16[128,4,512]{2,0,1:T(8,128)(2,1)}), bf16[128,4,512]{2,0,1:T(8,128)(2,1)S(1)}, u32[]{:S(2)}, u32[]{:S(2)}) %all-to-all-start.4) | async-done | bytes 524320 | tf_op jit(solution)/shard_map/all_to_all | solution.py:71
  129.5 0.1 broadcast_in_dim.35
  129.6 9.5 %all_to_all.60 = bf16[4,384,128]{2,1,0:T(8,128)(2,1)S(1)} all-to-all(bf16[4,384,128]{2,1,0:T(8,128)(2,1)S(1)} %broadcast_in_dim.35), channel_id=1, replica_groups=mesh['fs'=128,'tp'=4] {'tp'}, dimensions={0} | all-to-all | bytes 786432 | tf_op jit(solution)/shard_map/all_to_all | solution.py:22
  139.0 0.5 fusion.2
  139.6 1.0 reshape.99
  140.6 14.1 %all-to-all-start.5 = ((bf16[128,3,512]{2,1,0:T(4,128)(2,1)}), bf16[128,3,512]{2,1,0:T(4,128)(2,1)S(1)}, u32[]{:S(2)}, u32[]{:S(2)}) async-start(bf16[128,3,512]{2,1,0:T(4,128)(2,1)} %reshape.99), calls=%async_computation.5 | async-start | bytes 1048576 | tf_op jit(solution)/shard_map/all_to_all | solution.py:80
  154.7 0.0 copy-done.7
  154.8 0.1 copy.13
  154.9 1.0 copy.20
  155.9 19.4 %all-to-all-done.5 = bf16[128,3,512]{2,1,0:T(4,128)(2,1)S(1)} async-done(((bf16[128,3,512]{2,1,0:T(4,128)(2,1)}), bf16[128,3,512]{2,1,0:T(4,128)(2,1)S(1)}, u32[]{:S(2)}, u32[]{:S(2)}) %all-to-all-start.5) | async-done | bytes 393248 | tf_op jit(solution)/shard_map/all_to_all | solution.py:80
  175.3 0.3 reshape.100
  175.6 1.2 gather_fusion.1
  176.8 0.3 reshape.101
  177.1 1.4 multiply_reduce_fusion
  (14 shorter events, 0.1 us)
Async XLA Ops:
  7.2 4.2 %copy-start = (bf16[128,512]{1,0:T(8,128)(2,1)S(1)}, bf16[128,512]{1,0:T(8,128)(2,1)}, u32[]{:S(2)}) copy-start(bf16[128,512]{1,0:T(8,128)(2,1)} %param.7) | copy-start | bytes 393220
  13.4 20.0 %copy-start.2 = (f32[128,128,16]{1,2,0:T(8,128)S(1)}, f32[128,128,16]{1,2,0:T(8,128)}, u32[]{:S(2)}) copy-start(f32[128,128,16]{1,2,0:T(8,128)} %param.13) | copy-start | bytes 3145732
  15.0 39.0 %all-to-all-start.2 = ((bf16[128,3,512]{2,1,0:T(4,128)(2,1)}), bf16[128,3,512]{2,1,0:T(4,128)(2,1)S(1)}, u32[]{:S(2)}, u32[]{:S(2)}) async-start(bf16[128,3,512]{2,1,0:T(4,128)(2,1)} %broadcast_select_fusion), calls=%async_computation.2 | async-start | bytes 1048576 | tf_op jit(solution)/shard_map/all_to_all | solution.py:60
  33.5 26.0 %copy-start.3 = (f32[128,16,128]{2,1,0:T(8,128)S(1)}, f32[128,16,128]{2,1,0:T(8,128)}, u32[]{:S(2)}) copy-start(f32[128,16,128]{2,1,0:T(8,128)} %param.11) | copy-start | bytes 3145732
  33.5 26.0 %copy-start.8 = (f32[16]{0:T(128)S(1)}, f32[16]{0:T(128)}, u32[]{:S(2)}) copy-start(f32[16]{0:T(128)} %param.10) | copy-start | bytes 196
  34.3 25.1 %copy-start.4 = (f32[128,16,128]{2,1,0:T(8,128)S(1)}, f32[128,16,128]{2,1,0:T(8,128)}, u32[]{:S(2)}) copy-start(f32[128,16,128]{2,1,0:T(8,128)} %param.12) | copy-start | bytes 3145732
  54.0 26.0 %all-to-all-start.1 = ((bf16[128,128,16]{1,2,0:T(8,128)(2,1)}), bf16[128,128,16]{1,2,0:T(8,128)(2,1)S(1)}, u32[]{:S(2)}, u32[]{:S(2)}) async-start(bf16[128,128,16]{1,2,0:T(8,128)(2,1)} %convert_element_type.40), calls=%async_computation.1 | async-start | bytes 1048576 | tf_op jit(solution)/shard_map/all_to_all | solution.py:45
  80.0 36.4 %all-to-all-start = ((bf16[128,16,256]{2,1,0:T(8,128)(2,1)}), bf16[128,16,256]{2,1,0:T(8,128)(2,1)S(1)}, u32[]{:S(2)}, u32[]{:S(2)}) async-start(bf16[128,16,256]{2,1,0:T(8,128)(2,1)} %pad_maximum_fusion), calls=%async_computation | async-start | bytes 2097152 | tf_op jit(solution)/shard_map/all_to_all | solution.py:10
  85.4 35.4 %all-gather.2.cloned.1.call-start = ((), (), s32[]{:S(2)}) async-start(), calls=%async_computation.6 | async-start | bytes 1966080 | tf_op jit(solution)/shard_map/all_gather | solution.py:63
  116.3 13.2 %all-to-all-start.4 = ((bf16[128,4,512]{2,0,1:T(8,128)(2,1)}), bf16[128,4,512]{2,0,1:T(8,128)(2,1)S(1)}, u32[]{:S(2)}, u32[]{:S(2)}) async-start(bf16[128,4,512]{2,0,1:T(8,128)(2,1)} %copy.19), calls=%async_computation.4 | async-start | bytes 1048576 | tf_op jit(solution)/shard_map/all_to_all | solution.py:71
  120.4 2.9 %copy-start.6 = (bf16[1,2048,128]{2,1,0:T(8,128)(2,1)}, bf16[1,2048,128]{2,1,0:T(8,128)(2,1)S(1)}, u32[]{:S(2)}) copy-start(bf16[1,2048,128]{2,1,0:T(8,128)(2,1)S(1)} %get-tuple-element.9) | copy-start | bytes 1572868
  120.4 2.9 %copy-start.5 = (bf16[1,2048,128]{2,1,0:T(8,128)(2,1)}, bf16[1,2048,128]{2,1,0:T(8,128)(2,1)S(1)}, u32[]{:S(2)}) copy-start(bf16[1,2048,128]{2,1,0:T(8,128)(2,1)S(1)} %get-tuple-element.8) | copy-start | bytes 1572868
  120.7 2.0 %copy-start.1 = (bf16[384,2048]{1,0:T(8,128)(2,1)S(1)}, bf16[384,2048]{1,0:T(8,128)(2,1)}, u32[]{:S(2)}) copy-start(bf16[384,2048]{1,0:T(8,128)(2,1)} %all-gather.2.cloned.1.call-done) | copy-start | bytes 4718596
  139.0 15.7 %copy-start.7 = (f32[128,2]{0,1:T(2,128)S(1)}, f32[128,2]{0,1:T(2,128)}, u32[]{:S(2)}) copy-start(f32[128,2]{0,1:T(2,128)} %param.9) | copy-start | bytes 3076
  140.6 34.7 %all-to-all-start.5 = ((bf16[128,3,512]{2,1,0:T(4,128)(2,1)}), bf16[128,3,512]{2,1,0:T(4,128)(2,1)S(1)}, u32[]{:S(2)}, u32[]{:S(2)}) async-start(bf16[128,3,512]{2,1,0:T(4,128)(2,1)} %reshape.99), calls=%async_computation.5 | async-start | bytes 1048576 | tf_op jit(solution)/shard_map/all_to_all | solution.py:80
Sparse Core Ops, SparseCore 0:
  88.3 32.3 all-gather.1
where the time goes:
time: 186 us; the launch traced here: 185 us
  waiting for transfers between devices  92.9 us (50%)
  starting transfers between devices  47.4 us (25%)
  between operations  14.3 us (8%)
  local copies, waits for them, and re-layouts  11.6 us (6%)
  blocking collectives  9.47 us (5%)
  other arithmetic  7.85 us (4%)
    all_to_all x1, waiting for transfers between devices, side_by_side(): lax.all_to_all(both, axis, split_axis=split_dim, concat_axis=concat_dim,...  28.8 us
    all_to_all x1, waiting for transfers between devices, local(): lax.all_to_all(packed.reshape(fs_count, capacity, -1), 'fs', split_axis=0...  19.7 us
    all_to_all x1, waiting for transfers between devices, local(): lax.all_to_all(expert_out.reshape(fs_count, capacity, -1), 'fs', split_ax...  19.4 us
    all_to_all x1, waiting for transfers between devices, local(): lax.all_to_all(down_weight.astype(jnp.bfloat16), 'fs', split_axis=0, conc...  19.2 us
    all_to_all x1, starting transfers between devices, local(): lax.all_to_all(packed.reshape(fs_count, capacity, -1), 'fs', split_axis=0...  18.4 us
    all_to_all x1, starting transfers between devices, local(): lax.all_to_all(expert_out.reshape(fs_count, capacity, -1), 'fs', split_ax...  14.1 us
    all_to_all x1, blocking collectives, sent_to_all(): lax.all_to_all(jnp.broadcast_to(value[None], (size, *value.shape)), axis,...  9.47 us
    all_to_all x1, waiting for transfers between devices, local(): lax.all_to_all(down_out[0].reshape(unit_rows, tp_count, -1), 'tp', split_...  5.55 us
  transfers between devices with their start and end apart: 6, of which 6 were waited for; matrix products, arithmetic and copies ran while one was open for 5% of the time, Pallas kernels for 0%

commit v1 on v0

v1 whole, which is shorter than its diff:
```python
import jax
import jax.numpy as jnp
from jax import lax
from jax.experimental import pallas as pl
from jax.experimental.pallas import tpu as pltpu
from jax.sharding import PartitionSpec as P

SLOTS = 3
BF = jnp.bfloat16
F32 = jnp.float32


def vmem(count):
    return [pl.BlockSpec(memory_space=pltpu.VMEM)] * count


def slot_hits(routes):
    experts = lax.axis_size("fs")
    count = routes.shape[1]
    expert = lax.broadcasted_iota(jnp.int32, (experts, count), 0)
    first = routes[0:1, :] == expert
    second = routes[1:2, :] == expert
    hit = jnp.where(first | second, 1.0, 0.0)
    before = lax.broadcasted_iota(jnp.int32, (count, count), 0) < lax.broadcasted_iota(
        jnp.int32, (count, count), 1
    )
    order = jnp.dot(hit.astype(BF), jnp.where(before, 1.0, 0.0).astype(BF), preferred_element_type=F32)
    return first, hit, order


def pack_kernel(routes_ref, tokens_ref, down_ref, out_ref):
    _, hit, order = slot_hits(routes_ref[...])
    tokens = tokens_ref[...]
    experts = out_ref.shape[0]
    for s in range(SLOTS):
        chosen = jnp.where((hit > 0.0) & (order == float(s)), 1.0, 0.0).astype(BF)
        rows = jnp.dot(chosen, tokens, preferred_element_type=F32)
        out_ref[:, :, s * 128 : (s + 1) * 128] = rows.reshape(experts, 4, 128).astype(BF)
    base = SLOTS * 128
    for k in range(4):
        out_ref[:, :, base + k * 128 : base + (k + 1) * 128] = down_ref[:, 4 * k : 4 * k + 4, :].astype(BF)


def unpack_kernel(place_ref, got_ref, rows_ref, *down_refs):
    sources = got_ref.shape[0]
    for s in range(SLOTS):
        block = got_ref[:, :, s * 128 : (s + 1) * 128].astype(F32)
        rows_ref[s * sources : (s + 1) * sources, :] = block.reshape(sources, 512).astype(BF)
    base = SLOTS * 128
    part = sources // 4
    for shift, ref in enumerate(down_refs):
        start = ((place_ref[0] + shift) % 4) * part
        for k in range(4):
            ref[:, 4 * k : 4 * k + 4, :] = got_ref[
                pl.ds(start, part), :, base + k * 128 : base + (k + 1) * 128
            ]


def down_kernel(got_ref, out_ref):
    sources = got_ref.shape[0]
    base = SLOTS * 128
    parts = [got_ref[:, :, base + k * 128 : base + (k + 1) * 128] for k in range(4)]
    block = jnp.concatenate([p.astype(F32) for p in parts], axis=1)
    out_ref[...] = block.reshape(sources * 16, 128).T.astype(BF)


def norm_kernel(*refs):
    ins, outs = refs[:4], refs[4]
    values = [r[...].astype(F32) for r in ins]
    total = sum(jnp.sum(v * v, axis=1, keepdims=True) for v in values)
    scale = lax.rsqrt(total / 2048.0 + 1e-06)
    for k in range(4):
        outs[k] = (values[k] * scale).astype(BF)


def hidden_kernel(place_ref, rows_ref, weight_ref, out_ref):
    acc = None
    for k in range(4):
        block = (place_ref[0] + 4 - k) % 4
        part = jnp.dot(rows_ref[k], weight_ref[block], preferred_element_type=F32)
        acc = part if acc is None else acc + part
    gate = acc[:, :128]
    up = acc[:, 128:]
    out_ref[...] = (gate / (1.0 + jnp.exp(-gate)) * up).astype(BF)


def expert_kernel(place_ref, hidden_ref, d0, d1, d2, d3, out_ref):
    acc = None
    for k, ref in enumerate((d0, d1, d2, d3)):
        block = (place_ref[0] + 4 - k) % 4
        part = lax.dot_general(
            hidden_ref[block], ref[...], (((1,), (1,)), ((), ())), preferred_element_type=F32
        )
        acc = part if acc is None else acc + part
    sources = out_ref.shape[0]
    for s in range(SLOTS):
        rows = acc[s * sources : (s + 1) * sources, :].astype(BF).astype(F32)
        out_ref[:, :, s * 128 : (s + 1) * 128] = rows.reshape(sources, 4, 128).astype(BF)


def share_kernel(routes_ref, weight_ref, high_ref, low_ref):
    first, hit, order = slot_hits(routes_ref[...])
    weight = weight_ref[...]
    share = weight / jnp.sum(weight, axis=0, keepdims=True)
    mine = jnp.where(first, share[0:1, :], share[1:2, :])
    for s in range(SLOTS):
        part = jnp.where((hit > 0.0) & (order == float(s)), mine, 0.0).T
        high = part.astype(BF)
        high_ref[s] = high
        low_ref[s] = (part - high.astype(F32)).astype(BF)


def mix_kernel(high_ref, low_ref, back_ref, out_ref):
    experts = back_ref.shape[0]
    acc = None
    for s in range(SLOTS):
        rows = back_ref[:, :, s * 128 : (s + 1) * 128].astype(F32).reshape(experts, 512).astype(BF)
        part = jnp.dot(high_ref[s], rows, preferred_element_type=F32)
        part = part + jnp.dot(low_ref[s], rows, preferred_element_type=F32)
        acc = part if acc is None else acc + part
    out_ref[...] = acc.astype(BF)


def local(tokens, routes, route_weight, gain, gate_weight, up_weight, down_weight):
    place = lax.axis_index("tp").astype(jnp.int32).reshape(1)
    fs = lax.axis_size("fs")
    count = tokens.shape[0]
    wide = SLOTS * 128 + 512
    scalar = pl.BlockSpec(memory_space=pltpu.SMEM)
    routes = routes.T
    route_weight = route_weight.T

    packed = pl.pallas_call(
        pack_kernel, out_shape=jax.ShapeDtypeStruct((fs, 4, wide), BF), name="pack"
    )(routes, tokens, jnp.transpose(down_weight, (0, 2, 1)))
    got = lax.all_to_all(packed, "fs", 0, 0, tiled=True)

    gain_rows = gain[None, :, None]
    gate_new = (gain_rows * gate_weight).astype(BF)
    up_new = (gain_rows * up_weight).astype(BF)
    both = lax.all_to_all(jnp.concatenate((gate_new, up_new), axis=2), "fs", 0, 0, tiled=True)

    part = jax.ShapeDtypeStruct((fs // 4, 16, 128), BF)
    rows, *downs = pl.pallas_call(
        unpack_kernel,
        out_shape=(jax.ShapeDtypeStruct((SLOTS * fs, 512), BF), part, part, part, part),
        in_specs=[scalar] + vmem(1),
        name="unpack",
    )(place, got)

    def shifted(value, k):
        return lax.ppermute(value, "tp", [(i, (i + k) % 4) for i in range(4)])

    row_parts = [rows, None, None, None]
    down_parts = [downs[0], None, None, None]
    for k in (1, 3, 2):
        row_parts[k] = shifted(rows, k)
    for k in (1, 3, 2):
        down_parts[k] = shifted(downs[k], k)
    normed = pl.pallas_call(
        norm_kernel, out_shape=jax.ShapeDtypeStruct((4, SLOTS * fs, 512), BF), name="norm"
    )(*row_parts)

    hidden = pl.pallas_call(
        hidden_kernel,
        out_shape=jax.ShapeDtypeStruct((SLOTS * fs, 128), BF),
        in_specs=[scalar] + vmem(2),
        name="hidden",
    )(place, normed, both.reshape(4, 512, 256))
    hidden = lax.all_gather(hidden, "tp", axis=0, tiled=False)
    result = pl.pallas_call(
        expert_kernel,
        out_shape=jax.ShapeDtypeStruct((fs, 4, SLOTS * 128), BF),
        in_specs=[scalar] + vmem(5),
        name="expert",
    )(place, hidden, *[d.reshape(512, 128) for d in down_parts])
    back = lax.all_to_all(result, "fs", 0, 0, tiled=True)

    pair = jax.ShapeDtypeStruct((SLOTS, count, fs), BF)
    high, low = pl.pallas_call(share_kernel, out_shape=(pair, pair), name="share")(routes, route_weight)
    mixed = pl.pallas_call(
        mix_kernel, out_shape=jax.ShapeDtypeStruct((count, 512), BF), name="mix"
    )(high, low, back)
    down_out = pl.pallas_call(
        down_kernel, out_shape=jax.ShapeDtypeStruct((128, fs * 16), BF), name="down"
    )(got)
    both = both.reshape(1, fs * 16, 256)
    return (both[:, :, :128], both[:, :, 128:], down_out[None], mixed)


def solution(mesh):
    in_specs = (
        P("fs", "tp"),
        P("fs", None),
        P("fs", None),
        P("fs"),
        P(None, "fs", "tp"),
        P(None, "fs", "tp"),
        P(None, "tp", "fs"),
    )
    out_specs = (P("fs", None, "tp"), P("fs", None, "tp"), P("fs", "tp", None), P("fs", "tp"))
    return jax.shard_map(local, mesh=mesh, in_specs=in_specs, out_specs=out_specs, check_vma=False)
```

time: 186 us -> 150 us (0.81)
  waiting for transfers between devices: 92.9 us -> 48.6 us
  Pallas kernels: 0 us -> 20.2 us
  starting transfers between devices: 47.4 us -> 63.3 us
  between operations: 14.3 us -> 0.84 us
  local copies, waits for them, and re-layouts: 11.6 us -> 4.26 us
  other arithmetic: 7.85 us -> 1.34 us
    all_to_all x5 -> x3, waiting for transfers between devices: 92.6 us -> 40.2 us  [the longest x1 27.2 us: local(): got = lax.all_to_all(packed, 'fs', 0, 0, tiled=True)]
    pallas_call x0 -> x8, Pallas kernels: none -> 20.2 us  [the longest x1 3.06 us: local(): pl.pallas_call(pack_kernel, out_shape=jax.ShapeDtypeStruct((fs, 4, wide),...]
    ppermute x0 -> x6, starting transfers between devices: none -> 19 us  [shifted(): return lax.ppermute(value, 'tp', [(i, (i + k) % 4) for i in range(4)])]
    all_gather x0 -> x1, blocking collectives: none -> 11.2 us  [local(): hidden = lax.all_gather(hidden, 'tp', axis=0, tiled=False)]
    all_to_all x1 -> x0, blocking collectives: 9.47 us -> none  [sent_to_all(): lax.all_to_all(jnp.broadcast_to(value[None], (size, *value.shape)), axis,...]
    ppermute x0 -> x6, waiting for transfers between devices: none -> 8.41 us  [shifted(): return lax.ppermute(value, 'tp', [(i, (i + k) % 4) for i in range(4)])]
    reduce_sum x4 -> x0, other arithmetic: 3.48 us -> none  [the longest x1 1.91 us: normalize(): jnp.mean(values * values, axis=-1, keepdims=True) + 1e-06]
    gather x3 -> x0, local copies, waits for them, and re-layouts: 3.43 us -> none  [the longest x2 2.28 us: local(): packed = jnp.where(filled, tokens[row_of], jnp.zeros((), jnp.bfloat16))]
  transfers between devices with their start and end apart: 6 -> 9, of which waited for: 6 -> 3; matrix products, arithmetic and copies ran while one was open for 5% -> 2% of each run, Pallas kernels for 0% -> 8%
where the time goes in v1:
time: 150 us
  starting transfers between devices  63.3 us (42%)
  waiting for transfers between devices  48.6 us (32%)
  Pallas kernels  20.2 us (13%)
  blocking collectives  11.2 us (7%)
  local copies, waits for them, and re-layouts  4.26 us (3%)
    all_to_all x1, waiting for transfers between devices, local(): got = lax.all_to_all(packed, 'fs', 0, 0, tiled=True)  27.2 us
    all_to_all x1, starting transfers between devices, local(): back = lax.all_to_all(result, 'fs', 0, 0, tiled=True)  20 us
    ppermute x6, starting transfers between devices, shifted(): return lax.ppermute(value, 'tp', [(i, (i + k) % 4) for i in range(4)])  19 us
    all_to_all x1, starting transfers between devices, local(): got = lax.all_to_all(packed, 'fs', 0, 0, tiled=True)  18.4 us
    all_to_all x1, waiting for transfers between devices, local(): back = lax.all_to_all(result, 'fs', 0, 0, tiled=True)  12.9 us
    all_gather x1, blocking collectives, local(): hidden = lax.all_gather(hidden, 'tp', axis=0, tiled=False)  11.2 us
    ppermute x6, waiting for transfers between devices, shifted(): return lax.ppermute(value, 'tp', [(i, (i + k) % 4) for i in range(4)])  8.41 us
    all_to_all x1, starting transfers between devices, local(): lax.all_to_all(jnp.concatenate((gate_new, up_new), axis=2), 'fs', 0, 0, t...  5.9 us
  transfers between devices with their start and end apart: 9, of which 3 were waited for; matrix products, arithmetic and copies ran while one was open for 2% of the time, Pallas kernels for 8%

profile of v1, /device:TPU:1, one launch (start us, length us, event | category | flops | bytes accessed | tf_op | source)
XLA Modules:
  0.0 149.7 jit_solution(7680683489678124459)
XLA Ops:
  0.6 0.0 copy-start.4
  0.6 0.0 copy-start.5
  0.7 0.0 copy-start.12
  0.7 3.1 %pack.1 = bf16[128,4,896]{2,1,0:T(4,128)(2,1)} custom-call(s32[2,128]{1,0:T(2,128)} %bitcast.21, bf16[128,512]{1,0:T(8,128)(2,1)} %tokens_ref.1, f32[128,16,128]{2,1,0:T(8,128)} %bitcast.15), custom_call_target="tpu_custom_call" | custom-call | tf_op jit(solution)/shard_map/pack/pallas_call | solution.py:133
  3.7 18.4 %all-to-all-start.1 = ((bf16[128,4,896]{2,1,0:T(4,128)(2,1)}), bf16[128,4,896]{2,1,0:T(4,128)(2,1)S(1)}, u32[]{:S(2)}, u32[]{:S(2)}) async-start(bf16[128,4,896]{2,1,0:T(4,128)(2,1)} %pack.1), calls=%async_computation.1 | async-start | bytes 1835008 | tf_op jit(solution)/shard_map/all_to_all | solution.py:136
  22.1 0.0 copy-done.4
  22.1 0.0 copy-done.5
  22.2 0.0 copy-done.12
  22.2 0.2 multiply_convert_fusion.1
  22.4 1.1 pad_maximum_fusion
  23.5 27.2 %all-to-all-done.1.got_ref = bf16[128,4,896]{2,1,0:T(4,128)(2,1)S(1)} async-done(((bf16[128,4,896]{2,1,0:T(4,128)(2,1)}), bf16[128,4,896]{2,1,0:T(4,128)(2,1)S(1)}, u32[]{:S(2)}, u32[]{:S(2)}) %all-to-all-start.1) | async-done | bytes 917536 | tf_op jit(solution)/shard_map/all_to_all | solution.py:136
  50.7 0.0 copy-start.2
  50.7 5.9 %all-to-all-start = ((bf16[128,16,256]{2,1,0:T(8,128)(2,1)}), bf16[128,16,256]{2,1,0:T(8,128)(2,1)S(1)}, u32[]{:S(2)}, u32[]{:S(2)}) async-start(bf16[128,16,256]{2,1,0:T(8,128)(2,1)} %pad_maximum_fusion), calls=%async_computation | async-start | bytes 2097152 | tf_op jit(solution)/shard_map/all_to_all | solution.py:141
  56.6 0.0 copy-done.2
  56.7 2.4 %unpack.1 = (bf16[384,512]{1,0:T(8,128)(2,1)}, bf16[32,16,128]{2,1,0:T(8,128)(2,1)}, bf16[32,16,128]{2,1,0:T(8,128)(2,1)}, bf16[32,16,128]{2,1,0:T(8,128)(2,1)}, bf16[32,16,128]{2,1,0:T(8,128)(2,1)}) custom-call(s32[1]{0:T(128)} %bitcast.5.place_ref, bf16[128,4,896]{2,1,0:T(4,128)(2,1)} %copy-done.2), custom_call_target="tpu_custom_call" | custom-call | tf_op jit(solution)/shard_map/unpack/pallas_call | solution.py:144
  59.0 4.4 %collective-permute-start.2 = (bf16[384,512]{1,0:T(8,128)(2,1)}, bf16[384,512]{1,0:T(8,128)(2,1)S(1)}, u32[]{:S(2)}, u32[]{:S(2)}) collective-permute-start(bf16[384,512]{1,0:T(8,128)(2,1)} %get-tuple-element.13.refs_0_), channel_id=1, source_target_pairs={{0,3},{1,0},{2,1},{3,2},{4,7},{5,4},{6,5},{7,6},{8,11},{9,8},{10,9... | collective-permute-start | bytes 1179656 | tf_op jit(solution)/shard_map/ppermute | solution.py:152
  63.4 2.4 %collective-permute-start.1 = (bf16[384,512]{1,0:T(8,128)(2,1)}, bf16[384,512]{1,0:T(8,128)(2,1)S(1)}, u32[]{:S(2)}, u32[]{:S(2)}) collective-permute-start(bf16[384,512]{1,0:T(8,128)(2,1)} %get-tuple-element.13.refs_0_), channel_id=1, source_target_pairs={{0,2},{1,3},{2,0},{3,1},{4,6},{5,7},{6,4},{7,5},{8,10},{9,11},{10,... | collective-permute-start | bytes 1179656 | tf_op jit(solution)/shard_map/ppermute | solution.py:152
  65.9 2.5 %collective-permute-start = (bf16[384,512]{1,0:T(8,128)(2,1)}, bf16[384,512]{1,0:T(8,128)(2,1)S(1)}, u32[]{:S(2)}, u32[]{:S(2)}) collective-permute-start(bf16[384,512]{1,0:T(8,128)(2,1)} %get-tuple-element.13.refs_0_), channel_id=1, source_target_pairs={{0,1},{1,2},{2,3},{3,0},{4,5},{5,6},{6,7},{7,4},{8,9},{9,10},{10,1... | collective-permute-start | bytes 1179656 | tf_op jit(solution)/shard_map/ppermute | solution.py:152
  68.4 3.4 %collective-permute-start.3 = (bf16[32,16,128]{2,1,0:T(8,128)(2,1)}, bf16[32,16,128]{2,1,0:T(8,128)(2,1)S(1)}, u32[]{:S(2)}, u32[]{:S(2)}) collective-permute-start(bf16[32,16,128]{2,1,0:T(8,128)(2,1)} %get-tuple-element.15), channel_id=1, source_target_pairs={{0,1},{1,2},{2,3},{3,0},{4,5},{5,6},{6,7},{7,4},{8,9},{9,10},{10,1... | collective-permute-start | bytes 393224 | tf_op jit(solution)/shard_map/ppermute | solution.py:152
  71.8 3.6 %collective-permute-start.4 = (bf16[32,16,128]{2,1,0:T(8,128)(2,1)}, bf16[32,16,128]{2,1,0:T(8,128)(2,1)S(1)}, u32[]{:S(2)}, u32[]{:S(2)}) collective-permute-start(bf16[32,16,128]{2,1,0:T(8,128)(2,1)} %get-tuple-element.16), channel_id=1, source_target_pairs={{0,2},{1,3},{2,0},{3,1},{4,6},{5,7},{6,4},{7,5},{8,10},{9,11},{10,... | collective-permute-start | bytes 393224 | tf_op jit(solution)/shard_map/ppermute | solution.py:152
  75.5 0.0 collective-permute-done.2.refs_3_
  75.5 0.0 copy-start.6
  75.5 2.6 %collective-permute-start.5 = (bf16[32,16,128]{2,1,0:T(8,128)(2,1)}, bf16[32,16,128]{2,1,0:T(8,128)(2,1)S(1)}, u32[]{:S(2)}, u32[]{:S(2)}) collective-permute-start(bf16[32,16,128]{2,1,0:T(8,128)(2,1)} %get-tuple-element.17), channel_id=1, source_target_pairs={{0,3},{1,0},{2,1},{3,2},{4,7},{5,4},{6,5},{7,6},{8,11},{9,8},{10,9... | collective-permute-start | bytes 393224 | tf_op jit(solution)/shard_map/ppermute | solution.py:152
  78.1 0.0 collective-permute-done.1.refs_2_
  78.1 0.0 copy-start.7
  78.1 8.4 %collective-permute-done.refs_1_ = bf16[384,512]{1,0:T(8,128)(2,1)S(1)} collective-permute-done((bf16[384,512]{1,0:T(8,128)(2,1)}, bf16[384,512]{1,0:T(8,128)(2,1)S(1)}, u32[]{:S(2)}, u32[]{:S(2)}) %collective-permute-start) | collective-permute-done | bytes 393248 | tf_op jit(solution)/shard_map/ppermute | solution.py:152
  86.5 0.0 copy-done.6
  86.5 0.0 copy-done.7
  86.5 0.0 copy-start.8
  86.5 0.7 copy-done.8
  87.2 3.0 %norm.1.rows_ref = bf16[4,384,512]{2,1,0:T(8,128)(2,1)} custom-call(bf16[384,512]{1,0:T(8,128)(2,1)} %get-tuple-element.13.refs_0_, bf16[384,512]{1,0:T(8,128)(2,1)} %copy-done.8, bf16[384,512]{1,0:T(8,128)(2,1)} %copy-done.7, bf16[384,512]{1,0:T(8,128)(2,1)} %copy-done.6), custom_call_target="tpu_custom_call" | custom-call | tf_op jit(solution)/shard_map/norm/pallas_call | solution.py:160
  90.3 0.0 all-to-all-done
  90.3 0.0 copy-start
  90.3 1.0 copy-done
  91.2 2.9 %hidden.1 = bf16[384,128]{1,0:T(8,128)(2,1)} custom-call(s32[1]{0:T(128)} %bitcast.5.place_ref, bf16[4,384,512]{2,1,0:T(8,128)(2,1)} %norm.1.rows_ref, bf16[4,512,256]{2,1,0:T(8,128)(2,1)} %bitcast.12), custom_call_target="tpu_custom_call" | custom-call | tf_op jit(solution)/shard_map/hidden/pallas_call | solution.py:164
  94.2 11.2 %all-gather = bf16[1536,128]{1,0:T(8,128)(2,1)} all-gather(bf16[384,128]{1,0:T(8,128)(2,1)} %hidden.1), channel_id=2, replica_groups=mesh['fs'=128,'tp'=4] {'tp'}, dimensions={0}, use_global_device_ids=true | all-gather | bytes 491520 | tf_op jit(solution)/shard_map/all_gather | solution.py:170
  105.3 0.0 collective-permute-done.3
  105.3 0.0 copy-start.9
  105.3 0.0 collective-permute-done.4
  105.4 0.0 copy-start.10
  105.4 0.0 collective-permute-done.5
  105.4 0.0 copy-start.11
  105.4 0.6 copy-done.9
  106.0 0.0 copy-done.10
  106.0 0.0 copy-done.11
  106.1 0.0 copy-start.1
  106.1 2.7 %expert.1 = bf16[128,4,384]{2,1,0:T(4,128)(2,1)} custom-call(s32[1]{0:T(128)} %bitcast.5.place_ref, bf16[4,384,128]{2,1,0:T(8,128)(2,1)} %bitcast.14, bf16[512,128]{1,0:T(8,128)(2,1)} %bitcast.17, bf16[512,128]{1,0:T(8,128)(2,1)} %bitcast.18, bf16[512,128]{1,0:T(8,128)(2,1)} %bitcast.19, bf16[512,128]{1,0:T(8,128)(2,1)} %bitcast.20), custom_call_target="tpu_custom_call" | custom-call | tf_op jit(solution)/shard_map/expert/pallas_call | solution.py:171
  108.8 20.0 %all-to-all-start.2 = ((bf16[128,4,384]{2,1,0:T(4,128)(2,1)}), bf16[128,4,384]{2,1,0:T(4,128)(2,1)S(1)}, u32[]{:S(2)}, u32[]{:S(2)}) async-start(bf16[128,4,384]{2,1,0:T(4,128)(2,1)} %expert.1), calls=%async_computation.2 | async-start | bytes 786432 | tf_op jit(solution)/shard_map/all_to_all | solution.py:177
  128.9 1.6 %share.1 = (bf16[3,128,128]{2,1,0:T(8,128)(2,1)}, bf16[3,128,128]{2,1,0:T(8,128)(2,1)}) custom-call(s32[2,128]{1,0:T(2,128)} %bitcast.22, f32[2,128]{1,0:T(2,128)} %bitcast.23), custom_call_target="tpu_custom_call" | custom-call | tf_op jit(solution)/shard_map/share/pallas_call | solution.py:180
  130.5 2.2 %down.1 = bf16[128,2048]{1,0:T(8,128)(2,1)} custom-call(bf16[128,4,896]{2,1,0:T(4,128)(2,1)} %copy-done.2), custom_call_target="tpu_custom_call" | custom-call | tf_op jit(solution)/shard_map/down/pallas_call | solution.py:184
  132.7 0.0 copy-done.1
  132.7 1.0 fusion
  133.8 12.9 %all-to-all-done.2.back_ref = bf16[128,4,384]{2,1,0:T(4,128)(2,1)S(1)} async-done(((bf16[128,4,384]{2,1,0:T(4,128)(2,1)}), bf16[128,4,384]{2,1,0:T(4,128)(2,1)S(1)}, u32[]{:S(2)}, u32[]{:S(2)}) %all-to-all-start.2) | async-done | bytes 393248 | tf_op jit(solution)/shard_map/all_to_all | solution.py:177
  146.7 0.0 copy-start.3
  146.7 0.8 copy-done.3
  147.5 2.2 %mix.1 = bf16[128,512]{1,0:T(8,128)(2,1)} custom-call(bf16[3,128,128]{2,1,0:T(8,128)(2,1)} %get-tuple-element.11.high_ref, bf16[3,128,128]{2,1,0:T(8,128)(2,1)} %get-tuple-element.12.low_ref, bf16[128,4,384]{2,1,0:T(4,128)(2,1)} %copy-done.3), custom_call_target="tpu_custom_call" | custom-call | tf_op jit(solution)/shard_map/mix/pallas_call | solution.py:181
Async XLA Ops:
  0.6 21.5 %copy-start.4 = (f32[128,16,128]{2,1,0:T(8,128)S(1)}, f32[128,16,128]{2,1,0:T(8,128)}, u32[]{:S(2)}) copy-start(f32[128,16,128]{2,1,0:T(8,128)} %param.11) | copy-start | bytes 3145732
  0.6 21.5 %copy-start.5 = (f32[128,16,128]{2,1,0:T(8,128)S(1)}, f32[128,16,128]{2,1,0:T(8,128)}, u32[]{:S(2)}) copy-start(f32[128,16,128]{2,1,0:T(8,128)} %param.12) | copy-start | bytes 3145732
  0.7 21.5 %copy-start.12 = (f32[16]{0:T(128)S(1)}, f32[16]{0:T(128)}, u32[]{:S(2)}) copy-start(f32[16]{0:T(128)} %param.10) | copy-start | bytes 196
  3.7 47.0 %all-to-all-start.1 = ((bf16[128,4,896]{2,1,0:T(4,128)(2,1)}), bf16[128,4,896]{2,1,0:T(4,128)(2,1)S(1)}, u32[]{:S(2)}, u32[]{:S(2)}) async-start(bf16[128,4,896]{2,1,0:T(4,128)(2,1)} %pack.1), calls=%async_computation.1 | async-start | bytes 1835008 | tf_op jit(solution)/shard_map/all_to_all | solution.py:136
  50.7 5.9 %copy-start.2 = (bf16[128,4,896]{2,1,0:T(4,128)(2,1)}, bf16[128,4,896]{2,1,0:T(4,128)(2,1)S(1)}, u32[]{:S(2)}) copy-start(bf16[128,4,896]{2,1,0:T(4,128)(2,1)S(1)} %all-to-all-done.1.got_ref) | copy-start | bytes 2752516
  50.7 39.5 %all-to-all-start = ((bf16[128,16,256]{2,1,0:T(8,128)(2,1)}), bf16[128,16,256]{2,1,0:T(8,128)(2,1)S(1)}, u32[]{:S(2)}, u32[]{:S(2)}) async-start(bf16[128,16,256]{2,1,0:T(8,128)(2,1)} %pad_maximum_fusion), calls=%async_computation | async-start | bytes 2097152 | tf_op jit(solution)/shard_map/all_to_all | solution.py:141
  59.0 16.4 %collective-permute-start.2 = (bf16[384,512]{1,0:T(8,128)(2,1)}, bf16[384,512]{1,0:T(8,128)(2,1)S(1)}, u32[]{:S(2)}, u32[]{:S(2)}) collective-permute-start(bf16[384,512]{1,0:T(8,128)(2,1)} %get-tuple-element.13.refs_0_), channel_id=1, source_target_pairs={{0,3},{1,0},{2,1},{3,2},{4,7},{5,4},{6,5},{7,6},{8,11},{9,8},{10,9... | collective-permute-start | bytes 1179656 | tf_op jit(solution)/shard_map/ppermute | solution.py:152
  63.4 14.7 %collective-permute-start.1 = (bf16[384,512]{1,0:T(8,128)(2,1)}, bf16[384,512]{1,0:T(8,128)(2,1)S(1)}, u32[]{:S(2)}, u32[]{:S(2)}) collective-permute-start(bf16[384,512]{1,0:T(8,128)(2,1)} %get-tuple-element.13.refs_0_), channel_id=1, source_target_pairs={{0,2},{1,3},{2,0},{3,1},{4,6},{5,7},{6,4},{7,5},{8,10},{9,11},{10,... | collective-permute-start | bytes 1179656 | tf_op jit(solution)/shard_map/ppermute | solution.py:152
  65.9 20.6 %collective-permute-start = (bf16[384,512]{1,0:T(8,128)(2,1)}, bf16[384,512]{1,0:T(8,128)(2,1)S(1)}, u32[]{:S(2)}, u32[]{:S(2)}) collective-permute-start(bf16[384,512]{1,0:T(8,128)(2,1)} %get-tuple-element.13.refs_0_), channel_id=1, source_target_pairs={{0,1},{1,2},{2,3},{3,0},{4,5},{5,6},{6,7},{7,4},{8,9},{9,10},{10,1... | collective-permute-start | bytes 1179656 | tf_op jit(solution)/shard_map/ppermute | solution.py:152
  68.4 37.0 %collective-permute-start.3 = (bf16[32,16,128]{2,1,0:T(8,128)(2,1)}, bf16[32,16,128]{2,1,0:T(8,128)(2,1)S(1)}, u32[]{:S(2)}, u32[]{:S(2)}) collective-permute-start(bf16[32,16,128]{2,1,0:T(8,128)(2,1)} %get-tuple-element.15), channel_id=1, source_target_pairs={{0,1},{1,2},{2,3},{3,0},{4,5},{5,6},{6,7},{7,4},{8,9},{9,10},{10,1... | collective-permute-start | bytes 393224 | tf_op jit(solution)/shard_map/ppermute | solution.py:152
  71.8 33.5 %collective-permute-start.4 = (bf16[32,16,128]{2,1,0:T(8,128)(2,1)}, bf16[32,16,128]{2,1,0:T(8,128)(2,1)S(1)}, u32[]{:S(2)}, u32[]{:S(2)}) collective-permute-start(bf16[32,16,128]{2,1,0:T(8,128)(2,1)} %get-tuple-element.16), channel_id=1, source_target_pairs={{0,2},{1,3},{2,0},{3,1},{4,6},{5,7},{6,4},{7,5},{8,10},{9,11},{10,... | collective-permute-start | bytes 393224 | tf_op jit(solution)/shard_map/ppermute | solution.py:152
  75.5 11.0 %copy-start.6 = (bf16[384,512]{1,0:T(8,128)(2,1)}, bf16[384,512]{1,0:T(8,128)(2,1)S(1)}, u32[]{:S(2)}) copy-start(bf16[384,512]{1,0:T(8,128)(2,1)S(1)} %collective-permute-done.2.refs_3_) | copy-start | bytes 1179652
  75.5 29.9 %collective-permute-start.5 = (bf16[32,16,128]{2,1,0:T(8,128)(2,1)}, bf16[32,16,128]{2,1,0:T(8,128)(2,1)S(1)}, u32[]{:S(2)}, u32[]{:S(2)}) collective-permute-start(bf16[32,16,128]{2,1,0:T(8,128)(2,1)} %get-tuple-element.17), channel_id=1, source_target_pairs={{0,3},{1,0},{2,1},{3,2},{4,7},{5,4},{6,5},{7,6},{8,11},{9,8},{10,9... | collective-permute-start | bytes 393224 | tf_op jit(solution)/shard_map/ppermute | solution.py:152
  78.1 8.4 %copy-start.7 = (bf16[384,512]{1,0:T(8,128)(2,1)}, bf16[384,512]{1,0:T(8,128)(2,1)S(1)}, u32[]{:S(2)}) copy-start(bf16[384,512]{1,0:T(8,128)(2,1)S(1)} %collective-permute-done.1.refs_2_) | copy-start | bytes 1179652
  86.5 0.7 copy-start.8
  90.3 1.0 copy-start
  105.3 0.7 copy-start.9
  105.4 0.7 copy-start.10
  105.4 0.7 copy-start.11
  106.1 26.7 %copy-start.1 = (bf16[128,16,256]{2,1,0:T(8,128)(2,1)S(1)}, bf16[128,16,256]{2,1,0:T(8,128)(2,1)}, u32[]{:S(2)}) copy-start(bf16[128,16,256]{2,1,0:T(8,128)(2,1)} %copy-done) | copy-start | bytes 3145732
  108.8 37.9 %all-to-all-start.2 = ((bf16[128,4,384]{2,1,0:T(4,128)(2,1)}), bf16[128,4,384]{2,1,0:T(4,128)(2,1)S(1)}, u32[]{:S(2)}, u32[]{:S(2)}) async-start(bf16[128,4,384]{2,1,0:T(4,128)(2,1)} %expert.1), calls=%async_computation.2 | async-start | bytes 786432 | tf_op jit(solution)/shard_map/all_to_all | solution.py:177
  146.7 0.8 copy-start.3

commit v2 on v1

--- a/solution.py
+++ b/solution.py
@@ -10,8 +10,15 @@
 F32 = jnp.float32
 
 
+LIMIT = pltpu.CompilerParams(vmem_limit_bytes=12 * 2**20)
+
+
 def vmem(count):
     return [pl.BlockSpec(memory_space=pltpu.VMEM)] * count
+
+
+def near(value):
+    return pltpu.with_memory_space_constraint(value, pltpu.VMEM)
 
 
 def slot_hits(routes):
@@ -64,24 +71,31 @@
     out_ref[...] = block.reshape(sources * 16, 128).T.astype(BF)
 
 
-def norm_kernel(*refs):
-    ins, outs = refs[:4], refs[4]
-    values = [r[...].astype(F32) for r in ins]
-    total = sum(jnp.sum(v * v, axis=1, keepdims=True) for v in values)
-    scale = lax.rsqrt(total / 2048.0 + 1e-06)
-    for k in range(4):
-        outs[k] = (values[k] * scale).astype(BF)
-
-
-def hidden_kernel(place_ref, rows_ref, weight_ref, out_ref):
-    acc = None
-    for k in range(4):
-        block = (place_ref[0] + 4 - k) % 4
-        part = jnp.dot(rows_ref[k], weight_ref[block], preferred_element_type=F32)
-        acc = part if acc is None else acc + part
-    gate = acc[:, :128]
-    up = acc[:, 128:]
-    out_ref[...] = (gate / (1.0 + jnp.exp(-gate)) * up).astype(BF)
+def scale_kernel(own, left, right, far_low, far_high, out_ref):
+    def squares(ref):
+        value = ref[...].astype(F32)
+        return jnp.sum(value * value, axis=1, keepdims=True)
+
+    far = jnp.concatenate((squares(far_low), squares(far_high)), axis=0)
+    total = squares(own) + squares(left) + squares(right) + far
+    out_ref[...] = jnp.broadcast_to(lax.rsqrt(total / 2048.0 + 1e-06), out_ref.shape)
+
+
+def hidden_kernel(place_ref, own, left, right, far_low, far_high, scale_ref, weight_ref, out_ref):
+    place = place_ref[0]
+    half = far_low.shape[0]
+
+    def product(value, shift):
+        return jnp.dot(value, weight_ref[(place + shift) % 4], preferred_element_type=F32)
+
+    for start, far in ((0, far_low), (half, far_high)):
+        rows = pl.ds(start, half)
+        acc = product(own[rows, :], 0) + product(left[rows, :], 3)
+        acc = acc + product(right[rows, :], 1) + product(far[...], 2)
+        scale = scale_ref[rows, :]
+        gate = acc[:, :128] * scale
+        up = acc[:, 128:] * scale
+        out_ref[rows, :] = (gate / (1.0 + jnp.exp(-gate)) * up).astype(BF)
 
 
 def expert_kernel(place_ref, hidden_ref, d0, d1, d2, d3, out_ref):
@@ -131,7 +145,7 @@
     route_weight = route_weight.T
 
     packed = pl.pallas_call(
-        pack_kernel, out_shape=jax.ShapeDtypeStruct((fs, 4, wide), BF), name="pack"
+        pack_kernel, out_shape=jax.ShapeDtypeStruct((fs, 4, wide), BF), name="pack", compiler_params=LIMIT
     )(routes, tokens, jnp.transpose(down_weight, (0, 2, 1)))
     got = lax.all_to_all(packed, "fs", 0, 0, tiled=True)
 
@@ -140,49 +154,68 @@
     up_new = (gain_rows * up_weight).astype(BF)
     both = lax.all_to_all(jnp.concatenate((gate_new, up_new), axis=2), "fs", 0, 0, tiled=True)
 
-    part = jax.ShapeDtypeStruct((fs // 4, 16, 128), BF)
+    got = near(got)
+    part = pltpu.VMEM((fs // 4, 16, 128), BF)
     rows, *downs = pl.pallas_call(
         unpack_kernel,
-        out_shape=(jax.ShapeDtypeStruct((SLOTS * fs, 512), BF), part, part, part, part),
+        out_shape=(pltpu.VMEM((SLOTS * fs, 512), BF), part, part, part, part),
         in_specs=[scalar] + vmem(1),
-        name="unpack",
+        out_specs=tuple(vmem(5)),
+        name="unpack", compiler_params=LIMIT,
     )(place, got)
 
     def shifted(value, k):
         return lax.ppermute(value, "tp", [(i, (i + k) % 4) for i in range(4)])
 
-    row_parts = [rows, None, None, None]
-    down_parts = [downs[0], None, None, None]
-    for k in (1, 3, 2):
-        row_parts[k] = shifted(rows, k)
-    for k in (1, 3, 2):
-        down_parts[k] = shifted(downs[k], k)
-    normed = pl.pallas_call(
-        norm_kernel, out_shape=jax.ShapeDtypeStruct((4, SLOTS * fs, 512), BF), name="norm"
-    )(*row_parts)
+    half = SLOTS * fs // 2
+    left = shifted(rows, 1)
+    right = shifted(rows, 3)
+    far_high = shifted(left[half:], 1)
+    far_low = shifted(right[:half], 3)
+    left, right, far_low, far_high, downs = lax.optimization_barrier(
+        (left, right, far_low, far_high, downs)
+    )
+    features = [near(v) for v in (rows, left, right, far_low, far_high)]
+    down_parts = [downs[0]] + [shifted(downs[k], k) for k in (1, 2, 3)]
+    scale = pl.pallas_call(
+        scale_kernel,
+        out_shape=pltpu.VMEM((SLOTS * fs, 128), F32),
+        in_specs=vmem(5),
+        out_specs=vmem(1)[0],
+        name="scale", compiler_params=LIMIT,
+    )(*features)
 
     hidden = pl.pallas_call(
         hidden_kernel,
-        out_shape=jax.ShapeDtypeStruct((SLOTS * fs, 128), BF),
-        in_specs=[scalar] + vmem(2),
-        name="hidden",
-    )(place, normed, both.reshape(4, 512, 256))
+        out_shape=pltpu.VMEM((SLOTS * fs, 128), BF),
+        in_specs=[scalar] + vmem(7),
+        out_specs=vmem(1)[0],
+        name="hidden", compiler_params=LIMIT,
+    )(place, *features, scale, near(both.reshape(4, 512, 256)))
     hidden = lax.all_gather(hidden, "tp", axis=0, tiled=False)
     result = pl.pallas_call(
         expert_kernel,
         out_shape=jax.ShapeDtypeStruct((fs, 4, SLOTS * 128), BF),
         in_specs=[scalar] + vmem(5),
-        name="expert",
-    )(place, hidden, *[d.reshape(512, 128) for d in down_parts])
+        name="expert", compiler_params=LIMIT,
+    )(place, near(hidden), *[near(d.reshape(512, 128)) for d in down_parts])
     back = lax.all_to_all(result, "fs", 0, 0, tiled=True)
 
-    pair = jax.ShapeDtypeStruct((SLOTS, count, fs), BF)
-    high, low = pl.pallas_call(share_kernel, out_shape=(pair, pair), name="share")(routes, route_weight)
+    pair = pltpu.VMEM((SLOTS, count, fs), BF)
+    high, low = pl.pallas_call(
+        share_kernel, out_shape=(pair, pair), out_specs=tuple(vmem(2)), name="share", compiler_params=LIMIT
+    )(routes, route_weight)
     mixed = pl.pallas_call(
-        mix_kernel, out_shape=jax.ShapeDtypeStruct((count, 512), BF), name="mix"
-    )(high, low, back)
+        mix_kernel,
+        out_shape=jax.ShapeDtypeStruct((count, 512), BF),
+        in_specs=vmem(3),
+        name="mix", compiler_params=LIMIT,
+    )(near(high), near(low), near(back))
     down_out = pl.pallas_call(
-        down_kernel, out_shape=jax.ShapeDtypeStruct((128, fs * 16), BF), name="down"
+        down_kernel,
+        out_shape=jax.ShapeDtypeStruct((128, fs * 16), BF),
+        in_specs=vmem(1),
+        name="down", compiler_params=LIMIT,
     )(got)
     both = both.reshape(1, fs * 16, 256)
     return (both[:, :, :128], both[:, :, 128:], down_out[None], mixed)

time: 150 us -> 147 us (0.980)
  Pallas kernels: 20.2 us -> 8.48 us
  waiting for transfers between devices: 48.6 us -> 54.3 us
  starting transfers between devices: 63.3 us -> 66.3 us
    pallas_call x4, Pallas kernels: 9.96 us -> 2.26 us  [the longest x1 0.92 us: local(): pl.pallas_call(unpack_kernel, out_shape=(pltpu.VMEM((SLOTS * fs, 512), BF...]
    ppermute x6 -> x7, waiting for transfers between devices: 8.41 us -> 11.6 us  [shifted(): return lax.ppermute(value, 'tp', [(i, (i + k) % 4) for i in range(4)])]
    ppermute x6 -> x7, starting transfers between devices: 19 us -> 21.9 us  [shifted(): return lax.ppermute(value, 'tp', [(i, (i + k) % 4) for i in range(4)])]
    all_to_all x1, waiting for transfers between devices: 12.9 us -> 15.5 us  [local(): back = lax.all_to_all(result, 'fs', 0, 0, tiled=True)]
    unnamed x26 -> x24, local copies, waits for them, and re-layouts: 3.22 us -> 4.43 us
  transfers between devices with their start and end apart: 9 -> 10, of which waited for: 3 -> 5; matrix products, arithmetic and copies ran while one was open for 2% -> 2% of each run, Pallas kernels for 8% -> 2%
where the time goes in v2:
time: 147 us
  starting transfers between devices  66.3 us (45%)
  waiting for transfers between devices  54.3 us (37%)
  blocking collectives  9.78 us (7%)
  Pallas kernels  8.48 us (6%)
  local copies, waits for them, and re-layouts  5.49 us (4%)
    all_to_all x1, waiting for transfers between devices, local(): got = lax.all_to_all(packed, 'fs', 0, 0, tiled=True)  27.2 us
    ppermute x7, starting transfers between devices, shifted(): return lax.ppermute(value, 'tp', [(i, (i + k) % 4) for i in range(4)])  21.9 us
    all_to_all x1, starting transfers between devices, local(): back = lax.all_to_all(result, 'fs', 0, 0, tiled=True)  19.9 us
    all_to_all x1, starting transfers between devices, local(): got = lax.all_to_all(packed, 'fs', 0, 0, tiled=True)  18.5 us
    all_to_all x1, waiting for transfers between devices, local(): back = lax.all_to_all(result, 'fs', 0, 0, tiled=True)  15.5 us
    ppermute x7, waiting for transfers between devices, shifted(): return lax.ppermute(value, 'tp', [(i, (i + k) % 4) for i in range(4)])  11.6 us
    all_gather x1, blocking collectives, local(): hidden = lax.all_gather(hidden, 'tp', axis=0, tiled=False)  9.78 us
    all_to_all x1, starting transfers between devices, local(): lax.all_to_all(jnp.concatenate((gate_new, up_new), axis=2), 'fs', 0, 0, t...  5.91 us
  transfers between devices with their start and end apart: 10, of which 5 were waited for; matrix products, arithmetic and copies ran while one was open for 2% of the time, Pallas kernels for 2%

profile of v2, /device:TPU:1, one launch (start us, length us, event | category | flops | bytes accessed | tf_op | source)
XLA Modules:
  0.0 146.6 jit_solution(2261661168789185278)
XLA Ops:
  0.6 0.0 copy-start
  0.6 1.2 copy-done
  1.9 0.0 copy-start.5
  1.9 0.9 copy-done.5
  2.8 0.0 copy-start.6
  2.8 0.7 copy-done.6
  3.4 0.0 copy-start.10
  3.4 1.6 %pack.1 = bf16[128,4,896]{2,1,0:T(4,128)(2,1)} custom-call(s32[2,128]{1,0:T(2,128)S(1)} %bitcast.17, bf16[128,512]{1,0:T(8,128)(2,1)S(1)} %copy-done.5, f32[128,16,128]{2,1,0:T(8,128)S(1)} %bitcast.15), custom_call_target="tpu_custom_call" | custom-call | tf_op jit(solution)/shard_map/pack/pallas_call | solution.py:147
  5.0 0.0 copy-start.9
  5.0 0.0 copy-start.11
  5.0 18.5 %all-to-all-start.1 = ((bf16[128,4,896]{2,1,0:T(4,128)(2,1)}), bf16[128,4,896]{2,1,0:T(4,128)(2,1)S(1)}, u32[]{:S(2)}, u32[]{:S(2)}) async-start(bf16[128,4,896]{2,1,0:T(4,128)(2,1)} %pack.1), calls=%async_computation.1 | async-start | bytes 1835008 | tf_op jit(solution)/shard_map/all_to_all | solution.py:150
  23.6 0.0 copy-done.10
  23.6 0.0 copy-done.9
  23.6 0.0 copy-done.11
  23.6 0.2 multiply_convert_fusion.1
  23.9 1.1 pad_maximum_fusion
  25.0 27.2 %all-to-all-done.1.got_ref = bf16[128,4,896]{2,1,0:T(4,128)(2,1)S(1)} async-done(((bf16[128,4,896]{2,1,0:T(4,128)(2,1)}), bf16[128,4,896]{2,1,0:T(4,128)(2,1)S(1)}, u32[]{:S(2)}, u32[]{:S(2)}) %all-to-all-start.1) | async-done | bytes 917536 | tf_op jit(solution)/shard_map/all_to_all | solution.py:150
  52.2 5.9 %all-to-all-start = ((bf16[128,16,256]{2,1,0:T(8,128)(2,1)}), bf16[128,16,256]{2,1,0:T(8,128)(2,1)S(1)}, u32[]{:S(2)}, u32[]{:S(2)}) async-start(bf16[128,16,256]{2,1,0:T(8,128)(2,1)} %pad_maximum_fusion), calls=%async_computation | async-start | bytes 2097152 | tf_op jit(solution)/shard_map/all_to_all | solution.py:155
  58.1 0.9 unpack.1
  59.0 0.0 copy-start.3
  59.0 4.4 %collective-permute-start.1 = (bf16[384,512]{1,0:T(8,128)(2,1)S(1)}, bf16[384,512]{1,0:T(8,128)(2,1)S(1)}, u32[]{:S(2)}, u32[]{:S(2)}) collective-permute-start(bf16[384,512]{1,0:T(8,128)(2,1)S(1)} %get-tuple-element.21.own), channel_id=1, source_target_pairs={{0,3},{1,0},{2,1},{3,2},{4,7},{5,4},{6,5},{7,6},{8,11},{9,8},{10,9... | collective-permute-start | bytes 1179656 | tf_op jit(solution)/shard_map/ppermute | solution.py:168
  63.4 1.9 %collective-permute-start = (bf16[384,512]{1,0:T(8,128)(2,1)S(1)}, bf16[384,512]{1,0:T(8,128)(2,1)S(1)}, u32[]{:S(2)}, u32[]{:S(2)}) collective-permute-start(bf16[384,512]{1,0:T(8,128)(2,1)S(1)} %get-tuple-element.21.own), channel_id=1, source_target_pairs={{0,1},{1,2},{2,3},{3,0},{4,5},{5,6},{6,7},{7,4},{8,9},{9,10},{10,1... | collective-permute-start | bytes 1179656 | tf_op jit(solution)/shard_map/ppermute | solution.py:168
  65.3 5.6 %collective-permute-done.1.right = bf16[384,512]{1,0:T(8,128)(2,1)S(1)} collective-permute-done((bf16[384,512]{1,0:T(8,128)(2,1)S(1)}, bf16[384,512]{1,0:T(8,128)(2,1)S(1)}, u32[]{:S(2)}, u32[]{:S(2)}) %collective-permute-start.1) | collective-permute-done | bytes 393248 | tf_op jit(solution)/shard_map/ppermute | solution.py:168
  71.0 5.3 %collective-permute-start.2 = (bf16[192,512]{1,0:T(8,128)(2,1)S(1)}, bf16[192,512]{1,0:T(8,128)(2,1)S(1)}, u32[]{:S(2)}, u32[]{:S(2)}) collective-permute-start(bf16[192,512]{1,0:T(8,128)(2,1)S(1)} %slice.18), channel_id=1, source_target_pairs={{0,3},{1,0},{2,1},{3,2},{4,7},{5,4},{6,5},{7,6},{8,11},{9,8},{10,9... | collective-permute-start | bytes 589832 | tf_op jit(solution)/shard_map/ppermute | solution.py:168
  76.3 0.0 collective-permute-done.left
  76.3 1.9 %collective-permute-start.3 = (bf16[192,512]{1,0:T(8,128)(2,1)S(1)}, bf16[192,512]{1,0:T(8,128)(2,1)S(1)}, u32[]{:S(2)}, u32[]{:S(2)}) collective-permute-start(bf16[192,512]{1,0:T(8,128)(2,1)S(1)} %slice.19), channel_id=1, source_target_pairs={{0,1},{1,2},{2,3},{3,0},{4,5},{5,6},{6,7},{7,4},{8,9},{9,10},{10,1... | collective-permute-start | bytes 589832 | tf_op jit(solution)/shard_map/ppermute | solution.py:168
  78.3 0.6 collective-permute-done.2.far_low
  78.9 5.4 %collective-permute-done.3.far_high = bf16[192,512]{1,0:T(8,128)(2,1)S(1)} collective-permute-done((bf16[192,512]{1,0:T(8,128)(2,1)S(1)}, bf16[192,512]{1,0:T(8,128)(2,1)S(1)}, u32[]{:S(2)}, u32[]{:S(2)}) %collective-permute-start.3) | collective-permute-done | bytes 196640 | tf_op jit(solution)/shard_map/ppermute | solution.py:168
  84.3 1.9 %collective-permute-start.4 = (bf16[32,16,128]{2,1,0:T(8,128)(2,1)}, bf16[32,16,128]{2,1,0:T(8,128)(2,1)}, u32[]{:S(2)}, u32[]{:S(2)}) collective-permute-start(bf16[32,16,128]{2,1,0:T(8,128)(2,1)} %get-tuple-element.31), channel_id=1, source_target_pairs={{0,1},{1,2},{2,3},{3,0},{4,5},{5,6},{6,7},{7,4},{8,9},{9,10},{10,1... | collective-permute-start | bytes 393224 | tf_op jit(solution)/shard_map/ppermute | solution.py:168
  86.2 2.3 %collective-permute-start.5 = (bf16[32,16,128]{2,1,0:T(8,128)(2,1)}, bf16[32,16,128]{2,1,0:T(8,128)(2,1)}, u32[]{:S(2)}, u32[]{:S(2)}) collective-permute-start(bf16[32,16,128]{2,1,0:T(8,128)(2,1)} %get-tuple-element.32), channel_id=1, source_target_pairs={{0,2},{1,3},{2,0},{3,1},{4,6},{5,7},{6,4},{7,5},{8,10},{9,11},{10,... | collective-permute-start | bytes 393224 | tf_op jit(solution)/shard_map/ppermute | solution.py:168
  88.5 4.2 %collective-permute-start.6 = (bf16[32,16,128]{2,1,0:T(8,128)(2,1)}, bf16[32,16,128]{2,1,0:T(8,128)(2,1)}, u32[]{:S(2)}, u32[]{:S(2)}) collective-permute-start(bf16[32,16,128]{2,1,0:T(8,128)(2,1)} %get-tuple-element.33), channel_id=1, source_target_pairs={{0,3},{1,0},{2,1},{3,2},{4,7},{5,4},{6,5},{7,6},{8,11},{9,8},{10,9... | collective-permute-start | bytes 393224 | tf_op jit(solution)/shard_map/ppermute | solution.py:168
  92.7 0.0 copy-done.3
  92.7 0.5 scale.1.scale_ref
  93.2 0.0 copy-start.1
  93.2 0.7 copy-done.1
  93.8 0.0 all-to-all-done
  93.8 0.0 copy-start.2
  93.8 0.9 copy-done.2
  94.8 0.0 copy-start.4
  94.8 0.6 hidden.1
  95.4 9.8 %all-gather = bf16[1536,128]{1,0:T(8,128)(2,1)S(1)} all-gather(bf16[384,128]{1,0:T(8,128)(2,1)S(1)} %hidden.1), channel_id=2, replica_groups=mesh['fs'=128,'tp'=4] {'tp'}, dimensions={0}, use_global_device_ids=true | all-gather | bytes 491520 | tf_op jit(solution)/shard_map/all_gather | solution.py:195
  105.2 0.0 collective-permute-done.4
  105.2 0.0 collective-permute-done.5
  105.2 0.0 collective-permute-done.6
  105.2 0.0 copy-done.4
  105.2 0.0 copy-start.7
  105.2 0.0 copy-start.8
  105.2 2.5 %expert.1 = bf16[128,4,384]{2,1,0:T(4,128)(2,1)} custom-call(s32[1]{0:T(128)} %bitcast.5.place_ref, bf16[4,384,128]{2,1,0:T(8,128)(2,1)S(1)} %bitcast.14, bf16[512,128]{1,0:T(8,128)(2,1)S(1)} %bitcast.16, bf16[512,128]{1,0:T(8,128)(2,1)} %bitcast.9.d1, bf16[512,128]{1,0:T(8,128)(2,1)} %bitcast.10.d2, bf16[512,128]{1,0:T(8,128)(2,1)} %bitcast.11.d3), custom_call_target="tpu_custom_call" | custom-call | tf_op jit(solution)/shard_map/expert/pallas_call | solution.py:196
  107.7 19.9 %all-to-all-start.2 = ((bf16[128,4,384]{2,1,0:T(4,128)(2,1)}), bf16[128,4,384]{2,1,0:T(4,128)(2,1)S(1)}, u32[]{:S(2)}, u32[]{:S(2)}) async-start(bf16[128,4,384]{2,1,0:T(4,128)(2,1)} %expert.1), calls=%async_computation.2 | async-start | bytes 786432 | tf_op jit(solution)/shard_map/all_to_all | solution.py:202
  127.6 0.0 copy-done.7
  127.6 0.0 copy-done.8
  127.6 0.3 share.1
  127.9 1.0 down.1
  129.0 1.0 fusion
  130.0 15.5 %all-to-all-done.2.back_ref = bf16[128,4,384]{2,1,0:T(4,128)(2,1)S(1)} async-done(((bf16[128,4,384]{2,1,0:T(4,128)(2,1)}), bf16[128,4,384]{2,1,0:T(4,128)(2,1)S(1)}, u32[]{:S(2)}, u32[]{:S(2)}) %all-to-all-start.2) | async-done | bytes 393248 | tf_op jit(solution)/shard_map/all_to_all | solution.py:202
  145.5 1.1 mix.1
  (2 shorter events, 0.0 us)
Async XLA Ops:
  0.6 1.2 copy-start
  1.9 0.9 copy-start.5
  2.8 0.7 copy-start.6
  3.4 20.1 %copy-start.10 = (f32[128,16,128]{2,1,0:T(8,128)S(1)}, f32[128,16,128]{2,1,0:T(8,128)}, u32[]{:S(2)}) copy-start(f32[128,16,128]{2,1,0:T(8,128)} %param.12) | copy-start | bytes 3145732
  5.0 18.6 %copy-start.9 = (f32[128,16,128]{2,1,0:T(8,128)S(1)}, f32[128,16,128]{2,1,0:T(8,128)}, u32[]{:S(2)}) copy-start(f32[128,16,128]{2,1,0:T(8,128)} %param.11) | copy-start | bytes 3145732
  5.0 18.6 %copy-start.11 = (f32[16]{0:T(128)S(1)}, f32[16]{0:T(128)}, u32[]{:S(2)}) copy-start(f32[16]{0:T(128)} %param.10) | copy-start | bytes 196
  5.0 47.1 %all-to-all-start.1 = ((bf16[128,4,896]{2,1,0:T(4,128)(2,1)}), bf16[128,4,896]{2,1,0:T(4,128)(2,1)S(1)}, u32[]{:S(2)}, u32[]{:S(2)}) async-start(bf16[128,4,896]{2,1,0:T(4,128)(2,1)} %pack.1), calls=%async_computation.1 | async-start | bytes 1835008 | tf_op jit(solution)/shard_map/all_to_all | solution.py:150
  52.2 41.7 %all-to-all-start = ((bf16[128,16,256]{2,1,0:T(8,128)(2,1)}), bf16[128,16,256]{2,1,0:T(8,128)(2,1)S(1)}, u32[]{:S(2)}, u32[]{:S(2)}) async-start(bf16[128,16,256]{2,1,0:T(8,128)(2,1)} %pad_maximum_fusion), calls=%async_computation | async-start | bytes 2097152 | tf_op jit(solution)/shard_map/all_to_all | solution.py:155
  59.0 33.7 %copy-start.3 = (bf16[32,16,128]{2,1,0:T(8,128)(2,1)}, bf16[32,16,128]{2,1,0:T(8,128)(2,1)S(1)}, u32[]{:S(2)}) copy-start(bf16[32,16,128]{2,1,0:T(8,128)(2,1)S(1)} %get-tuple-element.30) | copy-start | bytes 393220
  59.0 11.9 %collective-permute-start.1 = (bf16[384,512]{1,0:T(8,128)(2,1)S(1)}, bf16[384,512]{1,0:T(8,128)(2,1)S(1)}, u32[]{:S(2)}, u32[]{:S(2)}) collective-permute-start(bf16[384,512]{1,0:T(8,128)(2,1)S(1)} %get-tuple-element.21.own), channel_id=1, source_target_pairs={{0,3},{1,0},{2,1},{3,2},{4,7},{5,4},{6,5},{7,6},{8,11},{9,8},{10,9... | collective-permute-start | bytes 1179656 | tf_op jit(solution)/shard_map/ppermute | solution.py:168
  63.4 12.9 %collective-permute-start = (bf16[384,512]{1,0:T(8,128)(2,1)S(1)}, bf16[384,512]{1,0:T(8,128)(2,1)S(1)}, u32[]{:S(2)}, u32[]{:S(2)}) collective-permute-start(bf16[384,512]{1,0:T(8,128)(2,1)S(1)} %get-tuple-element.21.own), channel_id=1, source_target_pairs={{0,1},{1,2},{2,3},{3,0},{4,5},{5,6},{6,7},{7,4},{8,9},{9,10},{10,1... | collective-permute-start | bytes 1179656 | tf_op jit(solution)/shard_map/ppermute | solution.py:168
  71.0 7.9 %collective-permute-start.2 = (bf16[192,512]{1,0:T(8,128)(2,1)S(1)}, bf16[192,512]{1,0:T(8,128)(2,1)S(1)}, u32[]{:S(2)}, u32[]{:S(2)}) collective-permute-start(bf16[192,512]{1,0:T(8,128)(2,1)S(1)} %slice.18), channel_id=1, source_target_pairs={{0,3},{1,0},{2,1},{3,2},{4,7},{5,4},{6,5},{7,6},{8,11},{9,8},{10,9... | collective-permute-start | bytes 589832 | tf_op jit(solution)/shard_map/ppermute | solution.py:168
  76.3 7.9 %collective-permute-start.3 = (bf16[192,512]{1,0:T(8,128)(2,1)S(1)}, bf16[192,512]{1,0:T(8,128)(2,1)S(1)}, u32[]{:S(2)}, u32[]{:S(2)}) collective-permute-start(bf16[192,512]{1,0:T(8,128)(2,1)S(1)} %slice.19), channel_id=1, source_target_pairs={{0,1},{1,2},{2,3},{3,0},{4,5},{5,6},{6,7},{7,4},{8,9},{9,10},{10,1... | collective-permute-start | bytes 589832 | tf_op jit(solution)/shard_map/ppermute | solution.py:168
  84.3 20.9 %collective-permute-start.4 = (bf16[32,16,128]{2,1,0:T(8,128)(2,1)}, bf16[32,16,128]{2,1,0:T(8,128)(2,1)}, u32[]{:S(2)}, u32[]{:S(2)}) collective-permute-start(bf16[32,16,128]{2,1,0:T(8,128)(2,1)} %get-tuple-element.31), channel_id=1, source_target_pairs={{0,1},{1,2},{2,3},{3,0},{4,5},{5,6},{6,7},{7,4},{8,9},{9,10},{10,1... | collective-permute-start | bytes 393224 | tf_op jit(solution)/shard_map/ppermute | solution.py:168
  86.2 19.0 %collective-permute-start.5 = (bf16[32,16,128]{2,1,0:T(8,128)(2,1)}, bf16[32,16,128]{2,1,0:T(8,128)(2,1)}, u32[]{:S(2)}, u32[]{:S(2)}) collective-permute-start(bf16[32,16,128]{2,1,0:T(8,128)(2,1)} %get-tuple-element.32), channel_id=1, source_target_pairs={{0,2},{1,3},{2,0},{3,1},{4,6},{5,7},{6,4},{7,5},{8,10},{9,11},{10,... | collective-permute-start | bytes 393224 | tf_op jit(solution)/shard_map/ppermute | solution.py:168
  88.5 16.7 %collective-permute-start.6 = (bf16[32,16,128]{2,1,0:T(8,128)(2,1)}, bf16[32,16,128]{2,1,0:T(8,128)(2,1)}, u32[]{:S(2)}, u32[]{:S(2)}) collective-permute-start(bf16[32,16,128]{2,1,0:T(8,128)(2,1)} %get-tuple-element.33), channel_id=1, source_target_pairs={{0,3},{1,0},{2,1},{3,2},{4,7},{5,4},{6,5},{7,6},{8,11},{9,8},{10,9... | collective-permute-start | bytes 393224 | tf_op jit(solution)/shard_map/ppermute | solution.py:168
  93.2 0.7 copy-start.1
  93.8 0.9 copy-start.2
  94.8 10.4 %copy-start.4 = (bf16[32,16,128]{2,1,0:T(8,128)(2,1)S(1)}, bf16[32,16,128]{2,1,0:T(8,128)(2,1)}, u32[]{:S(2)}) copy-start(bf16[32,16,128]{2,1,0:T(8,128)(2,1)} %copy-done.3) | copy-start | bytes 393220
  105.2 22.4 %copy-start.7 = (s32[128,2]{0,1:T(2,128)S(1)}, s32[128,2]{0,1:T(2,128)}, u32[]{:S(2)}) copy-start(s32[128,2]{0,1:T(2,128)} %param.8) | copy-start | bytes 3076
  105.2 22.4 %copy-start.8 = (f32[128,2]{0,1:T(2,128)S(1)}, f32[128,2]{0,1:T(2,128)}, u32[]{:S(2)}) copy-start(f32[128,2]{0,1:T(2,128)} %param.9) | copy-start | bytes 3076
  107.7 37.7 %all-to-all-start.2 = ((bf16[128,4,384]{2,1,0:T(4,128)(2,1)}), bf16[128,4,384]{2,1,0:T(4,128)(2,1)S(1)}, u32[]{:S(2)}, u32[]{:S(2)}) async-start(bf16[128,4,384]{2,1,0:T(4,128)(2,1)} %expert.1), calls=%async_computation.2 | async-start | bytes 786432 | tf_op jit(solution)/shard_map/all_to_all | solution.py:202

commit v3 on v1

v3 whole, which is shorter than its diff:
```python
import jax
import jax.numpy as jnp
from jax import lax
from jax.experimental import pallas as pl
from jax.experimental.pallas import tpu as pltpu
from jax.sharding import PartitionSpec as P

SLOTS = 3
BF = jnp.bfloat16
F32 = jnp.float32


LIMIT = pltpu.CompilerParams(vmem_limit_bytes=12 * 2**20)


def vmem(count):
    return [pl.BlockSpec(memory_space=pltpu.VMEM)] * count


def near(value):
    return pltpu.with_memory_space_constraint(value, pltpu.VMEM)


def far(value):
    return pltpu.with_memory_space_constraint(value, pltpu.HBM)


def slot_hits(routes):
    experts = lax.axis_size("fs")
    count = routes.shape[1]
    expert = lax.broadcasted_iota(jnp.int32, (experts, count), 0)
    first = routes[0:1, :] == expert
    second = routes[1:2, :] == expert
    hit = jnp.where(first | second, 1.0, 0.0)
    before = lax.broadcasted_iota(jnp.int32, (count, count), 0) < lax.broadcasted_iota(
        jnp.int32, (count, count), 1
    )
    order = jnp.dot(hit.astype(BF), jnp.where(before, 1.0, 0.0).astype(BF), preferred_element_type=F32)
    return first, hit, order


def pack_kernel(routes_ref, tokens_hbm, down_hbm, out_ref, tokens_ref, down_ref, sems):
    parts = sems.shape[0] - 1
    tokens_copy = pltpu.make_async_copy(tokens_hbm, tokens_ref, sems.at[parts])
    tokens_copy.start()
    step = down_ref.shape[0] // parts
    copies = []
    for p in range(parts):
        piece = pl.ds(p * step, step)
        copies.append(pltpu.make_async_copy(down_hbm.at[piece], down_ref.at[piece], sems.at[p]))
        copies[-1].start()
    _, hit, order = slot_hits(routes_ref[...])
    tokens_copy.wait()
    tokens = tokens_ref[...]
    experts = out_ref.shape[0]
    for s in range(SLOTS):
        chosen = jnp.where((hit > 0.0) & (order == float(s)), 1.0, 0.0).astype(BF)
        rows = jnp.dot(chosen, tokens, preferred_element_type=F32)
        out_ref[:, :, s * 128 : (s + 1) * 128] = rows.reshape(experts, 4, 128).astype(BF)
    base = SLOTS * 128
    for p in range(parts):
        copies[p].wait()
        piece = pl.ds(p * step, step)
        for k in range(4):
            out_ref[piece, :, base + k * 128 : base + (k + 1) * 128] = down_ref[
                piece, 4 * k : 4 * k + 4, :
            ].astype(BF)


def unpack_kernel(got_ref, low_ref, high_ref, down_ref):
    sources = got_ref.shape[0]
    half = low_ref.shape[0]
    blocks = []
    for s in range(SLOTS):
        block = got_ref[:, :, s * 128 : (s + 1) * 128].astype(F32)
        blocks.append(block.reshape(sources, 512).astype(BF))
    low_ref[:sources, :] = blocks[0]
    low_ref[sources:, :] = blocks[1][: half - sources, :]
    high_ref[: 2 * sources - half, :] = blocks[1][half - sources :, :]
    high_ref[2 * sources - half :, :] = blocks[2]
    base = SLOTS * 128
    for k in range(4):
        down_ref[:, 4 * k : 4 * k + 4, :] = got_ref[:, :, base + k * 128 : base + (k + 1) * 128]


def down_kernel(down_ref, out_ref):
    out_ref[...] = down_ref[...].astype(F32).T.astype(BF)


def scale_kernel(low_ref, high_ref, out_ref):
    half = low_ref.shape[1]
    for h, ref in enumerate((low_ref, high_ref)):
        total = None
        for k in range(4):
            value = ref[k].astype(F32)
            part = jnp.sum(value * value, axis=1, keepdims=True)
            total = part if total is None else total + part
        scale = lax.rsqrt(total / 2048.0 + 1e-06)
        out_ref[h * half : (h + 1) * half, :] = jnp.broadcast_to(scale, (half, 128))


def hidden_kernel(low_ref, high_ref, scale_ref, weight_ref, down_ref, out_ref):
    half = low_ref.shape[1]
    total = 2 * half
    for h, ref in enumerate((low_ref, high_ref)):
        acc = None
        for k in range(4):
            part = jnp.dot(ref[k], weight_ref[k], preferred_element_type=F32)
            acc = part if acc is None else acc + part
        scale = scale_ref[h * half : (h + 1) * half, :]
        gate = acc[:, :128] * scale
        up = acc[:, 128:] * scale
        hidden = (gate / (1.0 + jnp.exp(-gate)) * up).astype(BF)
        for k in range(4):
            out_ref[k, h * half : (h + 1) * half, :] = hidden
    for k in range(4):
        out_ref[k, total:, :] = down_ref[k]


def expert_kernel(got_ref, out_ref):
    sources = out_ref.shape[0]
    total = SLOTS * sources
    acc = None
    for k in range(4):
        part = lax.dot_general(
            got_ref[k, :total, :],
            got_ref[k, total:, :],
            (((1,), (1,)), ((), ())),
            preferred_element_type=F32,
        )
        acc = part if acc is None else acc + part
    for s in range(SLOTS):
        rows = acc[s * sources : (s + 1) * sources, :].astype(BF).astype(F32)
        out_ref[:, :, s * 128 : (s + 1) * 128] = rows.reshape(sources, 4, 128).astype(BF)


def share_kernel(routes_ref, weight_ref, high_ref, low_ref):
    first, hit, order = slot_hits(routes_ref[...])
    weight = weight_ref[...]
    share = weight / jnp.sum(weight, axis=0, keepdims=True)
    mine = jnp.where(first, share[0:1, :], share[1:2, :])
    for s in range(SLOTS):
        part = jnp.where((hit > 0.0) & (order == float(s)), mine, 0.0).T
        high = part.astype(BF)
        high_ref[s] = high
        low_ref[s] = (part - high.astype(F32)).astype(BF)


def mix_kernel(high_ref, low_ref, back_ref, out_ref):
    experts = back_ref.shape[0]
    acc = None
    for s in range(SLOTS):
        rows = back_ref[:, :, s * 128 : (s + 1) * 128].astype(F32).reshape(experts, 512).astype(BF)
        part = jnp.dot(high_ref[s], rows, preferred_element_type=F32)
        part = part + jnp.dot(low_ref[s], rows, preferred_element_type=F32)
        acc = part if acc is None else acc + part
    out_ref[...] = acc.astype(BF)


def call(kernel, name, outs, in_specs, args, scratch=()):
    many = isinstance(outs, tuple)
    return pl.pallas_call(
        kernel,
        out_shape=outs,
        in_specs=in_specs,
        out_specs=tuple(vmem(len(outs))) if many else vmem(1)[0],
        scratch_shapes=scratch,
        compiler_params=LIMIT,
        name=name,
    )(*args)


def local(tokens, routes, route_weight, gain, gate_weight, up_weight, down_weight):
    fs = lax.axis_size("fs")
    count = tokens.shape[0]
    rows = SLOTS * fs
    wide = SLOTS * 128 + 512
    hbm = pl.BlockSpec(memory_space=pltpu.HBM)
    plain = jax.ShapeDtypeStruct
    routes = routes.T
    route_weight = route_weight.T

    packed = call(
        pack_kernel,
        "pack",
        plain((fs, 4, wide), BF),
        vmem(1) + [hbm, hbm],
        (far(routes), far(tokens), far(jnp.transpose(down_weight, (0, 2, 1)))),
        [
            pltpu.VMEM((count, 512), BF),
            pltpu.VMEM((fs, 16, 128), F32),
            pltpu.SemaphoreType.DMA((5,)),
        ],
    )
    got = near(lax.all_to_all(packed, "fs", 0, 0, tiled=True))

    gain_rows = gain[None, :, None]
    gate_new = (gain_rows * gate_weight).astype(BF)
    up_new = (gain_rows * up_weight).astype(BF)
    both = lax.all_to_all(jnp.concatenate((gate_new, up_new), axis=2), "fs", 0, 0, tiled=True)

    part = pltpu.VMEM((rows // 2, 512), BF)
    low, high, down = call(
        unpack_kernel, "unpack", (part, part, plain((fs, 16, 128), BF)), vmem(1), (got,)
    )
    low = lax.all_gather(low, "tp", axis=0, tiled=False)
    low, high = lax.optimization_barrier((low, high))
    high = lax.all_gather(high, "tp", axis=0, tiled=False)
    low, high = near(low), near(high)
    scale = call(scale_kernel, "scale", pltpu.VMEM((rows, 128), F32), vmem(2), (low, high))
    payload = call(
        hidden_kernel,
        "hidden",
        plain((4, rows + 512, 128), BF),
        vmem(5),
        (low, high, scale, near(both.reshape(4, 512, 256)), down.reshape(4, 512, 128)),
    )
    payload = near(lax.all_to_all(payload, "tp", 0, 0, tiled=True))
    result = call(expert_kernel, "expert", plain((fs, 4, SLOTS * 128), BF), vmem(1), (payload,))
    back = near(lax.all_to_all(result, "fs", 0, 0, tiled=True))

    pair = pltpu.VMEM((SLOTS, count, fs), BF)
    shares = call(share_kernel, "share", (pair, pair), vmem(2), (routes, route_weight))
    mixed = call(mix_kernel, "mix", plain((count, 512), BF), vmem(3), (*shares, back))
    down_out = call(
        down_kernel, "down", plain((128, fs * 16), BF), vmem(1), (down.reshape(fs * 16, 128),)
    )
    both = both.reshape(1, fs * 16, 256)
    return (both[:, :, :128], both[:, :, 128:], down_out[None], mixed)


def solution(mesh):
    in_specs = (
        P("fs", "tp"),
        P("fs", None),
        P("fs", None),
        P("fs"),
        P(None, "fs", "tp"),
        P(None, "fs", "tp"),
        P(None, "tp", "fs"),
    )
    out_specs = (P("fs", None, "tp"), P("fs", None, "tp"), P("fs", "tp", None), P("fs", "tp"))
    return jax.shard_map(local, mesh=mesh, in_specs=in_specs, out_specs=out_specs, check_vma=False)
```

time: 150 us -> 134 us (0.89)
  starting transfers between devices: 63.3 us -> 32.4 us
  blocking collectives: 11.2 us -> 41.1 us
  Pallas kernels: 20.2 us -> 8.45 us
  local copies, waits for them, and re-layouts: 4.26 us -> 1.06 us
    ppermute x6 -> x0, starting transfers between devices: 19 us -> none  [shifted(): return lax.ppermute(value, 'tp', [(i, (i + k) % 4) for i in range(4)])]
    all_to_all x0 -> x1, blocking collectives: none -> 17.2 us  [local(): payload = near(lax.all_to_all(payload, 'tp', 0, 0, tiled=True))]
    all_gather x1 -> x2, blocking collectives: 11.2 us -> 23.9 us  [the longest x1 12.6 us: local(): low = lax.all_gather(low, 'tp', axis=0, tiled=False)]
    all_to_all x2, starting transfers between devices: 38.4 us -> 26.5 us  [the longest x1 18.6 us: local(): got = near(lax.all_to_all(packed, 'fs', 0, 0, tiled=True))]
    pallas_call x8, Pallas kernels: 20.2 us -> 8.45 us  [call(): pl.pallas_call(kernel, out_shape=outs, in_specs=in_specs, out_specs=tuple...]
    ppermute x6 -> x0, waiting for transfers between devices: 8.41 us -> none  [shifted(): return lax.ppermute(value, 'tp', [(i, (i + k) % 4) for i in range(4)])]
    all_to_all x1, waiting for transfers between devices: 0.01 us -> 6.24 us  [local(): lax.all_to_all(jnp.concatenate((gate_new, up_new), axis=2), 'fs', 0, 0, t...]
    unnamed x26 -> x10, local copies, waits for them, and re-layouts: 3.22 us -> 0.02 us
  transfers between devices with their start and end apart: 9 -> 3, of which waited for: 3 -> 3; matrix products, arithmetic and copies ran while one was open for 2% -> 2% of each run, Pallas kernels for 8% -> 2%
where the time goes in v3:
time: 134 us
  waiting for transfers between devices  49 us (37%)
  blocking collectives  41.1 us (31%)
  starting transfers between devices  32.4 us (24%)
  Pallas kernels  8.45 us (6%)
  other arithmetic  1.34 us (1%)
    all_to_all x1, waiting for transfers between devices, local(): got = near(lax.all_to_all(packed, 'fs', 0, 0, tiled=True))  27.2 us
    all_to_all x1, starting transfers between devices, local(): got = near(lax.all_to_all(packed, 'fs', 0, 0, tiled=True))  18.6 us
    all_to_all x1, blocking collectives, local(): payload = near(lax.all_to_all(payload, 'tp', 0, 0, tiled=True))  17.2 us
    all_to_all x1, waiting for transfers between devices, local(): back = near(lax.all_to_all(result, 'fs', 0, 0, tiled=True))  15.5 us
    all_gather x1, blocking collectives, local(): low = lax.all_gather(low, 'tp', axis=0, tiled=False)  12.6 us
    all_gather x1, blocking collectives, local(): high = lax.all_gather(high, 'tp', axis=0, tiled=False)  11.3 us
    pallas_call x8, Pallas kernels, call(): pl.pallas_call(kernel, out_shape=outs, in_specs=in_specs, out_specs=tuple...  8.45 us
    all_to_all x1, starting transfers between devices, local(): back = near(lax.all_to_all(result, 'fs', 0, 0, tiled=True))  7.92 us
  transfers between devices with their start and end apart: 3, of which 3 were waited for; matrix products, arithmetic and copies ran while one was open for 2% of the time, Pallas kernels for 2%

profile of v3, /device:TPU:1, one launch (start us, length us, event | category | flops | bytes accessed | tf_op | source)
XLA Modules:
  0.0 134.1 jit_solution(7534805782534159531)
XLA Ops:
  0.6 0.0 copy-start.3
  0.6 3.2 %pack.1 = bf16[128,4,896]{2,1,0:T(4,128)(2,1)} custom-call(s32[2,128]{1,0:T(2,128)} %bitcast.18, bf16[128,512]{1,0:T(8,128)(2,1)} %tokens_hbm.1, f32[128,16,128]{2,1,0:T(8,128)} %bitcast.21), custom_call_target="tpu_custom_call" | custom-call | tf_op jit(solution)/shard_map/pack/pallas_call | solution.py:162
  3.9 0.0 copy-start.2
  3.9 0.0 copy-start.4
  3.9 18.6 %all-to-all-start.1 = ((bf16[128,4,896]{2,1,0:T(4,128)(2,1)}), bf16[128,4,896]{2,1,0:T(4,128)(2,1)S(1)}, u32[]{:S(2)}, u32[]{:S(2)}) async-start(bf16[128,4,896]{2,1,0:T(4,128)(2,1)} %pack.1), calls=%async_computation.1 | async-start | bytes 1835008 | tf_op jit(solution)/shard_map/all_to_all | solution.py:195
  22.5 0.0 copy-done.3
  22.5 0.0 copy-done.2
  22.5 0.0 copy-done.4
  22.5 0.2 multiply_convert_fusion.1
  22.7 1.1 pad_maximum_fusion
  23.8 27.2 %all-to-all-done.1.got_ref = bf16[128,4,896]{2,1,0:T(4,128)(2,1)S(1)} async-done(((bf16[128,4,896]{2,1,0:T(4,128)(2,1)}), bf16[128,4,896]{2,1,0:T(4,128)(2,1)S(1)}, u32[]{:S(2)}, u32[]{:S(2)}) %all-to-all-start.1) | async-done | bytes 917536 | tf_op jit(solution)/shard_map/all_to_all | solution.py:195
  51.1 5.9 %all-to-all-start = ((bf16[128,16,256]{2,1,0:T(8,128)(2,1)}), bf16[128,16,256]{2,1,0:T(8,128)(2,1)S(1)}, u32[]{:S(2)}, u32[]{:S(2)}) async-start(bf16[128,16,256]{2,1,0:T(8,128)(2,1)} %pad_maximum_fusion), calls=%async_computation | async-start | bytes 2097152 | tf_op jit(solution)/shard_map/all_to_all | solution.py:200
  57.0 0.4 unpack.1
  57.4 12.6 %all-gather = bf16[768,512]{1,0:T(8,128)(2,1)S(1)} all-gather(bf16[192,512]{1,0:T(8,128)(2,1)S(1)} %get-tuple-element.14), channel_id=2, replica_groups=mesh['fs'=128,'tp'=4] {'tp'}, dimensions={0}, use_global_device_ids=true | all-gather | bytes 983040 | tf_op jit(solution)/shard_map/all_gather | solution.py:206
  70.0 11.3 %all-gather.1 = bf16[768,512]{1,0:T(8,128)(2,1)S(1)} all-gather(bf16[192,512]{1,0:T(8,128)(2,1)S(1)} %get-tuple-element.17), channel_id=3, replica_groups=mesh['fs'=128,'tp'=4] {'tp'}, dimensions={0}, use_global_device_ids=true | all-gather | bytes 983040 | tf_op jit(solution)/shard_map/all_gather | solution.py:208
  81.3 0.4 scale.1.scale_ref
  81.7 6.2 %all-to-all-done = bf16[128,16,256]{2,1,0:T(8,128)(2,1)S(1)} async-done(((bf16[128,16,256]{2,1,0:T(8,128)(2,1)}), bf16[128,16,256]{2,1,0:T(8,128)(2,1)S(1)}, u32[]{:S(2)}, u32[]{:S(2)}) %all-to-all-start) | async-done | bytes 1048608 | tf_op jit(solution)/shard_map/all_to_all | solution.py:200
  87.9 0.6 hidden.1
  88.6 17.2 %all_to_all.20.got_ref = bf16[4,896,128]{2,1,0:T(8,128)(2,1)S(1)} all-to-all(bf16[4,896,128]{2,1,0:T(8,128)(2,1)S(1)} %hidden.1), channel_id=1, replica_groups=mesh['fs'=128,'tp'=4] {'tp'}, dimensions={0} | all-to-all | bytes 1835008 | tf_op jit(solution)/shard_map/all_to_all | solution.py:218
  105.8 0.0 copy-start
  105.8 0.0 copy-start.1
  105.8 1.5 %expert.1 = bf16[128,4,384]{2,1,0:T(4,128)(2,1)} custom-call(bf16[4,896,128]{2,1,0:T(8,128)(2,1)S(1)} %all_to_all.20.got_ref), custom_call_target="tpu_custom_call" | custom-call | tf_op jit(solution)/shard_map/expert/pallas_call | solution.py:162
  107.2 7.9 %all-to-all-start.3 = ((bf16[128,4,384]{2,1,0:T(4,128)(2,1)}), bf16[128,4,384]{2,1,0:T(4,128)(2,1)S(1)}, u32[]{:S(2)}, u32[]{:S(2)}) async-start(bf16[128,4,384]{2,1,0:T(4,128)(2,1)} %expert.1), calls=%async_computation.3 | async-start | bytes 786432 | tf_op jit(solution)/shard_map/all_to_all | solution.py:220
  115.1 0.0 copy-done
  115.1 0.0 copy-done.1
  115.2 0.3 share.1
  115.4 1.0 down.1
  116.4 1.0 fusion
  117.5 15.5 %all-to-all-done.3.back_ref = bf16[128,4,384]{2,1,0:T(4,128)(2,1)S(1)} async-done(((bf16[128,4,384]{2,1,0:T(4,128)(2,1)}), bf16[128,4,384]{2,1,0:T(4,128)(2,1)S(1)}, u32[]{:S(2)}, u32[]{:S(2)}) %all-to-all-start.3) | async-done | bytes 393248 | tf_op jit(solution)/shard_map/all_to_all | solution.py:220
  133.0 1.1 mix.1
Async XLA Ops:
  0.6 21.8 %copy-start.3 = (f32[128,16,128]{2,1,0:T(8,128)S(1)}, f32[128,16,128]{2,1,0:T(8,128)}, u32[]{:S(2)}) copy-start(f32[128,16,128]{2,1,0:T(8,128)} %param.12) | copy-start | bytes 3145732
  3.9 18.6 %copy-start.2 = (f32[128,16,128]{2,1,0:T(8,128)S(1)}, f32[128,16,128]{2,1,0:T(8,128)}, u32[]{:S(2)}) copy-start(f32[128,16,128]{2,1,0:T(8,128)} %param.11) | copy-start | bytes 3145732
  3.9 18.6 %copy-start.4 = (f32[16]{0:T(128)S(1)}, f32[16]{0:T(128)}, u32[]{:S(2)}) copy-start(f32[16]{0:T(128)} %param.10) | copy-start | bytes 196
  3.9 47.1 %all-to-all-start.1 = ((bf16[128,4,896]{2,1,0:T(4,128)(2,1)}), bf16[128,4,896]{2,1,0:T(4,128)(2,1)S(1)}, u32[]{:S(2)}, u32[]{:S(2)}) async-start(bf16[128,4,896]{2,1,0:T(4,128)(2,1)} %pack.1), calls=%async_computation.1 | async-start | bytes 1835008 | tf_op jit(solution)/shard_map/all_to_all | solution.py:195
  51.1 36.9 %all-to-all-start = ((bf16[128,16,256]{2,1,0:T(8,128)(2,1)}), bf16[128,16,256]{2,1,0:T(8,128)(2,1)S(1)}, u32[]{:S(2)}, u32[]{:S(2)}) async-start(bf16[128,16,256]{2,1,0:T(8,128)(2,1)} %pad_maximum_fusion), calls=%async_computation | async-start | bytes 2097152 | tf_op jit(solution)/shard_map/all_to_all | solution.py:200
  105.8 9.4 %copy-start = (s32[128,2]{0,1:T(2,128)S(1)}, s32[128,2]{0,1:T(2,128)}, u32[]{:S(2)}) copy-start(s32[128,2]{0,1:T(2,128)} %param.8) | copy-start | bytes 3076
  105.8 9.4 %copy-start.1 = (f32[128,2]{0,1:T(2,128)S(1)}, f32[128,2]{0,1:T(2,128)}, u32[]{:S(2)}) copy-start(f32[128,2]{0,1:T(2,128)} %param.9) | copy-start | bytes 3076
  107.2 25.8 %all-to-all-start.3 = ((bf16[128,4,384]{2,1,0:T(4,128)(2,1)}), bf16[128,4,384]{2,1,0:T(4,128)(2,1)S(1)}, u32[]{:S(2)}, u32[]{:S(2)}) async-start(bf16[128,4,384]{2,1,0:T(4,128)(2,1)} %expert.1), calls=%async_computation.3 | async-start | bytes 786432 | tf_op jit(solution)/shard_map/all_to_all | solution.py:220

commit v4 on v3

--- a/solution.py
+++ b/solution.py
@@ -39,35 +39,17 @@
     return first, hit, order
 
 
-def pack_kernel(routes_ref, tokens_hbm, down_hbm, out_ref, tokens_ref, down_ref, sems):
-    parts = sems.shape[0] - 1
-    tokens_copy = pltpu.make_async_copy(tokens_hbm, tokens_ref, sems.at[parts])
-    tokens_copy.start()
-    step = down_ref.shape[0] // parts
-    copies = []
-    for p in range(parts):
-        piece = pl.ds(p * step, step)
-        copies.append(pltpu.make_async_copy(down_hbm.at[piece], down_ref.at[piece], sems.at[p]))
-        copies[-1].start()
+def pack_kernel(routes_ref, tokens_ref, out_ref):
     _, hit, order = slot_hits(routes_ref[...])
-    tokens_copy.wait()
     tokens = tokens_ref[...]
     experts = out_ref.shape[0]
     for s in range(SLOTS):
         chosen = jnp.where((hit > 0.0) & (order == float(s)), 1.0, 0.0).astype(BF)
         rows = jnp.dot(chosen, tokens, preferred_element_type=F32)
         out_ref[:, :, s * 128 : (s + 1) * 128] = rows.reshape(experts, 4, 128).astype(BF)
-    base = SLOTS * 128
-    for p in range(parts):
-        copies[p].wait()
-        piece = pl.ds(p * step, step)
-        for k in range(4):
-            out_ref[piece, :, base + k * 128 : base + (k + 1) * 128] = down_ref[
-                piece, 4 * k : 4 * k + 4, :
-            ].astype(BF)
-
-
-def unpack_kernel(got_ref, low_ref, high_ref, down_ref):
+
+
+def unpack_kernel(got_ref, low_ref, high_ref):
     sources = got_ref.shape[0]
     half = low_ref.shape[0]
     blocks = []
@@ -78,13 +60,13 @@
     low_ref[sources:, :] = blocks[1][: half - sources, :]
     high_ref[: 2 * sources - half, :] = blocks[1][half - sources :, :]
     high_ref[2 * sources - half :, :] = blocks[2]
-    base = SLOTS * 128
-    for k in range(4):
-        down_ref[:, 4 * k : 4 * k + 4, :] = got_ref[:, :, base + k * 128 : base + (k + 1) * 128]
-
-
-def down_kernel(down_ref, out_ref):
-    out_ref[...] = down_ref[...].astype(F32).T.astype(BF)
+
+
+def place_kernel(weight_ref, gate_ref, up_ref, down_ref):
+    gate_ref[...] = weight_ref[:, :16, :]
+    up_ref[...] = weight_ref[:, 16:32, :]
+    block = weight_ref[:, 32:, :].reshape(weight_ref.shape[0] * 16, 128)
+    down_ref[...] = block.astype(F32).T.astype(BF)
 
 
 def scale_kernel(low_ref, high_ref, out_ref):
@@ -99,22 +81,29 @@
         out_ref[h * half : (h + 1) * half, :] = jnp.broadcast_to(scale, (half, 128))
 
 
-def hidden_kernel(low_ref, high_ref, scale_ref, weight_ref, down_ref, out_ref):
+def hidden_kernel(low_ref, high_ref, scale_ref, weight_ref, out_ref):
     half = low_ref.shape[1]
     total = 2 * half
-    for h, ref in enumerate((low_ref, high_ref)):
-        acc = None
-        for k in range(4):
-            part = jnp.dot(ref[k], weight_ref[k], preferred_element_type=F32)
-            acc = part if acc is None else acc + part
+    part = weight_ref.shape[0] // 4
+
+    def block(k, kind):
+        piece = weight_ref[k * part : (k + 1) * part, 16 * kind : 16 * kind + 16, :]
+        return piece.reshape(part * 16, 128)
+
+    accs = [None, None]
+    for k in range(4):
+        weight = jnp.concatenate((block(k, 0), block(k, 1)), axis=1)
+        for h, ref in enumerate((low_ref, high_ref)):
+            product = jnp.dot(ref[k], weight, preferred_element_type=F32)
+            accs[h] = product if k == 0 else accs[h] + product
+        out_ref[k, total:, :] = block(k, 2)
+    for h in range(2):
         scale = scale_ref[h * half : (h + 1) * half, :]
-        gate = acc[:, :128] * scale
-        up = acc[:, 128:] * scale
+        gate = accs[h][:, :128] * scale
+        up = accs[h][:, 128:] * scale
         hidden = (gate / (1.0 + jnp.exp(-gate)) * up).astype(BF)
         for k in range(4):
             out_ref[k, h * half : (h + 1) * half, :] = hidden
-    for k in range(4):
-        out_ref[k, total:, :] = down_ref[k]
 
 
 def expert_kernel(got_ref, out_ref):
@@ -174,35 +163,22 @@
     fs = lax.axis_size("fs")
     count = tokens.shape[0]
     rows = SLOTS * fs
-    wide = SLOTS * 128 + 512
-    hbm = pl.BlockSpec(memory_space=pltpu.HBM)
     plain = jax.ShapeDtypeStruct
     routes = routes.T
     route_weight = route_weight.T
 
     packed = call(
-        pack_kernel,
-        "pack",
-        plain((fs, 4, wide), BF),
-        vmem(1) + [hbm, hbm],
-        (far(routes), far(tokens), far(jnp.transpose(down_weight, (0, 2, 1)))),
-        [
-            pltpu.VMEM((count, 512), BF),
-            pltpu.VMEM((fs, 16, 128), F32),
-            pltpu.SemaphoreType.DMA((5,)),
-        ],
+        pack_kernel, "pack", plain((fs, 4, SLOTS * 128), BF), vmem(2), (far(routes), far(tokens))
     )
     got = near(lax.all_to_all(packed, "fs", 0, 0, tiled=True))
 
     gain_rows = gain[None, :, None]
-    gate_new = (gain_rows * gate_weight).astype(BF)
-    up_new = (gain_rows * up_weight).astype(BF)
-    both = lax.all_to_all(jnp.concatenate((gate_new, up_new), axis=2), "fs", 0, 0, tiled=True)
+    parts = (gain_rows * gate_weight, gain_rows * up_weight, jnp.transpose(down_weight, (0, 2, 1)))
+    weights = jnp.concatenate([p.astype(BF) for p in parts], axis=1)
+    weights = near(lax.all_to_all(weights, "fs", 0, 0, tiled=True))
 
     part = pltpu.VMEM((rows // 2, 512), BF)
-    low, high, down = call(
-        unpack_kernel, "unpack", (part, part, plain((fs, 16, 128), BF)), vmem(1), (got,)
-    )
+    low, high = call(unpack_kernel, "unpack", (part, part), vmem(1), (got,))
     low = lax.all_gather(low, "tp", axis=0, tiled=False)
     low, high = lax.optimization_barrier((low, high))
     high = lax.all_gather(high, "tp", axis=0, tiled=False)
@@ -212,8 +188,8 @@
         hidden_kernel,
         "hidden",
         plain((4, rows + 512, 128), BF),
-        vmem(5),
-        (low, high, scale, near(both.reshape(4, 512, 256)), down.reshape(4, 512, 128)),
+        vmem(4),
+        (low, high, scale, weights),
     )
     payload = near(lax.all_to_all(payload, "tp", 0, 0, tiled=True))
     result = call(expert_kernel, "expert", plain((fs, 4, SLOTS * 128), BF), vmem(1), (payload,))
@@ -222,11 +198,12 @@
     pair = pltpu.VMEM((SLOTS, count, fs), BF)
     shares = call(share_kernel, "share", (pair, pair), vmem(2), (routes, route_weight))
     mixed = call(mix_kernel, "mix", plain((count, 512), BF), vmem(3), (*shares, back))
-    down_out = call(
-        down_kernel, "down", plain((128, fs * 16), BF), vmem(1), (down.reshape(fs * 16, 128),)
-    )
-    both = both.reshape(1, fs * 16, 256)
-    return (both[:, :, :128], both[:, :, 128:], down_out[None], mixed)
+    part = plain((fs, 16, 128), BF)
+    gate_out, up_out, down_out = call(
+        place_kernel, "place", (part, part, plain((128, fs * 16), BF)), vmem(1), (weights,)
+    )
+    wide = (1, fs * 16, 128)
+    return (gate_out.reshape(wide), up_out.reshape(wide), down_out[None], mixed)
 
 
 def solution(mesh):

time: 134 us -> 133 us (level)
  other arithmetic: 1.34 us -> 2.81 us
    all_to_all x1, waiting for transfers between devices: 27.2 us -> 15 us  [local(): got = near(lax.all_to_all(packed, 'fs', 0, 0, tiled=True))]
    all_to_all x1, waiting for transfers between devices: 6.24 us -> 16.7 us  [local(): weights = near(lax.all_to_all(weights, 'fs', 0, 0, tiled=True))]
where the time goes in v4:
time: 133 us; the launch traced here: 132 us
  waiting for transfers between devices  48 us (36%)
  blocking collectives  40.6 us (31%)
  starting transfers between devices  32.6 us (25%)
  Pallas kernels  7.58 us (6%)
  other arithmetic  2.81 us (2%)
    all_to_all x1, starting transfers between devices, local(): got = near(lax.all_to_all(packed, 'fs', 0, 0, tiled=True))  18.4 us
    all_to_all x1, waiting for transfers between devices, local(): weights = near(lax.all_to_all(weights, 'fs', 0, 0, tiled=True))  16.7 us
    all_to_all x1, blocking collectives, local(): payload = near(lax.all_to_all(payload, 'tp', 0, 0, tiled=True))  16.6 us
    all_to_all x1, waiting for transfers between devices, local(): back = near(lax.all_to_all(result, 'fs', 0, 0, tiled=True))  16.3 us
    all_to_all x1, waiting for transfers between devices, local(): got = near(lax.all_to_all(packed, 'fs', 0, 0, tiled=True))  15 us
    all_gather x1, blocking collectives, local(): low = lax.all_gather(low, 'tp', axis=0, tiled=False)  12.7 us
    all_gather x1, blocking collectives, local(): high = lax.all_gather(high, 'tp', axis=0, tiled=False)  11.3 us
    all_to_all x1, starting transfers between devices, local(): back = near(lax.all_to_all(result, 'fs', 0, 0, tiled=True))  8.69 us
  transfers between devices with their start and end apart: 3, of which 3 were waited for; matrix products, arithmetic and copies ran while one was open for 2% of the time, Pallas kernels for 2%

profile of v4, /device:TPU:1, one launch (start us, length us, event | category | flops | bytes accessed | tf_op | source)
XLA Modules:
  0.0 132.4 jit_solution(6028441068507146926)
XLA Ops:
  0.6 0.0 copy-start.2
  0.6 0.0 copy-start.4
  0.7 0.0 copy-start.3
  0.7 2.3 %pack.1 = bf16[128,4,384]{2,1,0:T(4,128)(2,1)} custom-call(s32[2,128]{1,0:T(2,128)} %bitcast.13, bf16[128,512]{1,0:T(8,128)(2,1)} %tokens_ref.1), custom_call_target="tpu_custom_call" | custom-call | tf_op jit(solution)/shard_map/pack/pallas_call | solution.py:151
  3.0 18.4 %all-to-all-start.1 = ((bf16[128,4,384]{2,1,0:T(4,128)(2,1)}), bf16[128,4,384]{2,1,0:T(4,128)(2,1)S(1)}, u32[]{:S(2)}, u32[]{:S(2)}) async-start(bf16[128,4,384]{2,1,0:T(4,128)(2,1)} %pack.1), calls=%async_computation.1 | async-start | bytes 786432 | tf_op jit(solution)/shard_map/all_to_all | solution.py:173
  21.4 0.0 copy-done.2
  21.4 0.1 convert_bitcast_fusion
  21.5 0.0 copy-done.4
  21.5 0.0 copy-done.3
  21.5 1.5 %multiply_convert_fusion.1 = (bf16[128,16,128]{2,1,0:T(8,128)(2,1)S(1)}, bf16[128,16,128]{2,1,0:T(8,128)(2,1)S(1)}) fusion(f32[128,16,128]{2,1,0:T(8,128)S(1)} %copy-done.3, f32[16]{0:T(128)S(1)} %copy-done.4, f32[128,16,128]{2,1,0:T(8,128)} %param.12), kind=kLoop, calls=%fused_computation.2 | loop fusion | flops 1048576 | bytes 3145792 | tf_op jit(solution)/shard_map/convert_element_type | solution.py:177
  22.9 1.3 pad_maximum_fusion
  24.2 15.0 %all-to-all-done.1.got_ref = bf16[128,4,384]{2,1,0:T(4,128)(2,1)S(1)} async-done(((bf16[128,4,384]{2,1,0:T(4,128)(2,1)}), bf16[128,4,384]{2,1,0:T(4,128)(2,1)S(1)}, u32[]{:S(2)}, u32[]{:S(2)}) %all-to-all-start.1) | async-done | bytes 393248 | tf_op jit(solution)/shard_map/all_to_all | solution.py:173
  39.2 5.5 %all-to-all-start = ((bf16[128,48,128]{2,1,0:T(8,128)(2,1)}), bf16[128,48,128]{2,1,0:T(8,128)(2,1)S(1)}, u32[]{:S(2)}, u32[]{:S(2)}) async-start(bf16[128,48,128]{2,1,0:T(8,128)(2,1)} %pad_maximum_fusion), calls=%async_computation | async-start | bytes 3145728 | tf_op jit(solution)/shard_map/all_to_all | solution.py:178
  44.7 0.2 unpack.1
  44.9 12.7 %all-gather = bf16[768,512]{1,0:T(8,128)(2,1)S(1)} all-gather(bf16[192,512]{1,0:T(8,128)(2,1)S(1)} %get-tuple-element.18), channel_id=2, replica_groups=mesh['fs'=128,'tp'=4] {'tp'}, dimensions={0}, use_global_device_ids=true | all-gather | bytes 983040 | tf_op jit(solution)/shard_map/all_gather | solution.py:182
  57.6 11.3 %all-gather.1 = bf16[768,512]{1,0:T(8,128)(2,1)S(1)} all-gather(bf16[192,512]{1,0:T(8,128)(2,1)S(1)} %get-tuple-element.21), channel_id=3, replica_groups=mesh['fs'=128,'tp'=4] {'tp'}, dimensions={0}, use_global_device_ids=true | all-gather | bytes 983040 | tf_op jit(solution)/shard_map/all_gather | solution.py:184
  68.9 0.4 scale.1.scale_ref
  69.3 16.7 %all-to-all-done.weight_ref = bf16[128,48,128]{2,1,0:T(8,128)(2,1)S(1)} async-done(((bf16[128,48,128]{2,1,0:T(8,128)(2,1)}), bf16[128,48,128]{2,1,0:T(8,128)(2,1)S(1)}, u32[]{:S(2)}, u32[]{:S(2)}) %all-to-all-start) | async-done | bytes 1572896 | tf_op jit(solution)/shard_map/all_to_all | solution.py:178
  86.0 0.6 hidden.1
  86.7 0.0 copy-start
  86.7 0.0 copy-start.1
  86.7 16.6 %all_to_all.20.got_ref = bf16[4,896,128]{2,1,0:T(8,128)(2,1)S(1)} all-to-all(bf16[4,896,128]{2,1,0:T(8,128)(2,1)S(1)} %hidden.1), channel_id=1, replica_groups=mesh['fs'=128,'tp'=4] {'tp'}, dimensions={0} | all-to-all | bytes 1835008 | tf_op jit(solution)/shard_map/all_to_all | solution.py:194
  103.3 1.5 %expert.1 = bf16[128,4,384]{2,1,0:T(4,128)(2,1)} custom-call(bf16[4,896,128]{2,1,0:T(8,128)(2,1)S(1)} %all_to_all.20.got_ref), custom_call_target="tpu_custom_call" | custom-call | tf_op jit(solution)/shard_map/expert/pallas_call | solution.py:151
  104.7 8.7 %all-to-all-start.3 = ((bf16[128,4,384]{2,1,0:T(4,128)(2,1)}), bf16[128,4,384]{2,1,0:T(4,128)(2,1)S(1)}, u32[]{:S(2)}, u32[]{:S(2)}) async-start(bf16[128,4,384]{2,1,0:T(4,128)(2,1)} %expert.1), calls=%async_computation.3 | async-start | bytes 786432 | tf_op jit(solution)/shard_map/all_to_all | solution.py:196
  113.4 0.0 copy-done
  113.4 0.0 copy-done.1
  113.4 0.3 share.1
  113.7 1.3 place.1
  115.0 16.3 %all-to-all-done.3.back_ref = bf16[128,4,384]{2,1,0:T(4,128)(2,1)S(1)} async-done(((bf16[128,4,384]{2,1,0:T(4,128)(2,1)}), bf16[128,4,384]{2,1,0:T(4,128)(2,1)S(1)}, u32[]{:S(2)}, u32[]{:S(2)}) %all-to-all-start.3) | async-done | bytes 393248 | tf_op jit(solution)/shard_map/all_to_all | solution.py:196
  131.3 1.1 mix.1
Async XLA Ops:
  0.6 20.7 %copy-start.2 = (f32[128,128,16]{1,2,0:T(8,128)S(1)}, f32[128,128,16]{1,2,0:T(8,128)}, u32[]{:S(2)}) copy-start(f32[128,128,16]{1,2,0:T(8,128)} %param.13) | copy-start | bytes 3145732
  0.6 20.8 %copy-start.4 = (f32[16]{0:T(128)S(1)}, f32[16]{0:T(128)}, u32[]{:S(2)}) copy-start(f32[16]{0:T(128)} %param.10) | copy-start | bytes 196
  0.7 20.8 %copy-start.3 = (f32[128,16,128]{2,1,0:T(8,128)S(1)}, f32[128,16,128]{2,1,0:T(8,128)}, u32[]{:S(2)}) copy-start(f32[128,16,128]{2,1,0:T(8,128)} %param.11) | copy-start | bytes 3145732
  3.0 36.3 %all-to-all-start.1 = ((bf16[128,4,384]{2,1,0:T(4,128)(2,1)}), bf16[128,4,384]{2,1,0:T(4,128)(2,1)S(1)}, u32[]{:S(2)}, u32[]{:S(2)}) async-start(bf16[128,4,384]{2,1,0:T(4,128)(2,1)} %pack.1), calls=%async_computation.1 | async-start | bytes 786432 | tf_op jit(solution)/shard_map/all_to_all | solution.py:173
  39.2 46.8 %all-to-all-start = ((bf16[128,48,128]{2,1,0:T(8,128)(2,1)}), bf16[128,48,128]{2,1,0:T(8,128)(2,1)S(1)}, u32[]{:S(2)}, u32[]{:S(2)}) async-start(bf16[128,48,128]{2,1,0:T(8,128)(2,1)} %pad_maximum_fusion), calls=%async_computation | async-start | bytes 3145728 | tf_op jit(solution)/shard_map/all_to_all | solution.py:178
  86.7 26.8 %copy-start = (s32[128,2]{0,1:T(2,128)S(1)}, s32[128,2]{0,1:T(2,128)}, u32[]{:S(2)}) copy-start(s32[128,2]{0,1:T(2,128)} %param.8) | copy-start | bytes 3076
  86.7 26.8 %copy-start.1 = (f32[128,2]{0,1:T(2,128)S(1)}, f32[128,2]{0,1:T(2,128)}, u32[]{:S(2)}) copy-start(f32[128,2]{0,1:T(2,128)} %param.9) | copy-start | bytes 3076
  104.7 26.6 %all-to-all-start.3 = ((bf16[128,4,384]{2,1,0:T(4,128)(2,1)}), bf16[128,4,384]{2,1,0:T(4,128)(2,1)S(1)}, u32[]{:S(2)}, u32[]{:S(2)}) async-start(bf16[128,4,384]{2,1,0:T(4,128)(2,1)} %expert.1), calls=%async_computation.3 | async-start | bytes 786432 | tf_op jit(solution)/shard_map/all_to_all | solution.py:196

commit v5 on v3

--- a/solution.py
+++ b/solution.py
@@ -67,71 +67,93 @@
             ].astype(BF)
 
 
-def unpack_kernel(got_ref, low_ref, high_ref, down_ref):
+def unpack_kernel(place_ref, got_ref, down_ref, main_ref, *piece_refs):
     sources = got_ref.shape[0]
-    half = low_ref.shape[0]
+    main = main_ref.shape[0]
     blocks = []
     for s in range(SLOTS):
         block = got_ref[:, :, s * 128 : (s + 1) * 128].astype(F32)
         blocks.append(block.reshape(sources, 512).astype(BF))
-    low_ref[:sources, :] = blocks[0]
-    low_ref[sources:, :] = blocks[1][: half - sources, :]
-    high_ref[: 2 * sources - half, :] = blocks[1][half - sources :, :]
-    high_ref[2 * sources - half :, :] = blocks[2]
+    main_ref[:sources, :] = blocks[0]
+    main_ref[sources:, :] = blocks[1][: main - sources, :]
+    rest = jnp.concatenate((blocks[1][main - sources :, :], blocks[2]), axis=0)
+    count = rest.shape[0]
+    part = sources // 4
     base = SLOTS * 128
     for k in range(4):
         down_ref[:, 4 * k : 4 * k + 4, :] = got_ref[:, :, base + k * 128 : base + (k + 1) * 128]
-
-
-def down_kernel(down_ref, out_ref):
-    out_ref[...] = down_ref[...].astype(F32).T.astype(BF)
-
-
-def scale_kernel(low_ref, high_ref, out_ref):
-    half = low_ref.shape[1]
-    for h, ref in enumerate((low_ref, high_ref)):
+    for shift, ref in enumerate(piece_refs):
+        for c in range(4):
+            ref[c * count : (c + 1) * count, :] = rest[:, c * 128 : (c + 1) * 128]
+        start = ((place_ref[0] + shift) % 4) * part
+        ref[4 * count :, :] = down_ref[pl.ds(start, part), :, :].reshape(part * 16, 128)
+
+
+def other_rows(ref):
+    count = (ref.shape[0] - 512) // 4
+    return jnp.concatenate([ref[c * count : (c + 1) * count, :] for c in range(4)], axis=1)
+
+
+def scale_kernel(main_ref, p0, p1, p2, p3, out_ref):
+    main = main_ref.shape[1]
+
+    def scales(values):
         total = None
-        for k in range(4):
-            value = ref[k].astype(F32)
+        for value in values:
+            value = value.astype(F32)
             part = jnp.sum(value * value, axis=1, keepdims=True)
             total = part if total is None else total + part
         scale = lax.rsqrt(total / 2048.0 + 1e-06)
-        out_ref[h * half : (h + 1) * half, :] = jnp.broadcast_to(scale, (half, 128))
-
-
-def hidden_kernel(low_ref, high_ref, scale_ref, weight_ref, down_ref, out_ref):
-    half = low_ref.shape[1]
-    total = 2 * half
-    for h, ref in enumerate((low_ref, high_ref)):
-        acc = None
-        for k in range(4):
-            part = jnp.dot(ref[k], weight_ref[k], preferred_element_type=F32)
-            acc = part if acc is None else acc + part
-        scale = scale_ref[h * half : (h + 1) * half, :]
+        return jnp.broadcast_to(scale, (scale.shape[0], 128))
+
+    out_ref[:main, :] = scales([main_ref[k] for k in range(4)])
+    out_ref[main:, :] = scales([other_rows(ref) for ref in (p0, p1, p2, p3)])
+
+
+def hidden_kernel(place_ref, main_ref, p0, p1, p2, p3, scale_ref, weight_ref, out_ref):
+    main = main_ref.shape[1]
+    part = weight_ref.shape[0] // 4
+
+    def product(rows, block):
+        weight = weight_ref[pl.ds(block * part, part), :, :].reshape(part * 16, 256)
+        return jnp.dot(rows, weight, preferred_element_type=F32)
+
+    def finish(acc, start):
+        count = acc.shape[0]
+        scale = scale_ref[start : start + count, :]
         gate = acc[:, :128] * scale
         up = acc[:, 128:] * scale
-        hidden = (gate / (1.0 + jnp.exp(-gate)) * up).astype(BF)
-        for k in range(4):
-            out_ref[k, h * half : (h + 1) * half, :] = hidden
-    for k in range(4):
-        out_ref[k, total:, :] = down_ref[k]
-
-
-def expert_kernel(got_ref, out_ref):
+        out_ref[start : start + count, :] = (gate / (1.0 + jnp.exp(-gate)) * up).astype(BF)
+
+    acc = product(main_ref[0], 0)
+    for k in range(1, 4):
+        acc = acc + product(main_ref[k], k)
+    finish(acc, 0)
+    acc = product(other_rows(p0), place_ref[0])
+    for k, ref in ((1, p1), (2, p2), (3, p3)):
+        acc = acc + product(other_rows(ref), (place_ref[0] + 4 - k) % 4)
+    finish(acc, main)
+
+
+def expert_kernel(place_ref, hidden_ref, p0, p1, p2, p3, out_ref):
     sources = out_ref.shape[0]
-    total = SLOTS * sources
-    acc = None
-    for k in range(4):
-        part = lax.dot_general(
-            got_ref[k, :total, :],
-            got_ref[k, total:, :],
-            (((1,), (1,)), ((), ())),
-            preferred_element_type=F32,
-        )
-        acc = part if acc is None else acc + part
-    for s in range(SLOTS):
-        rows = acc[s * sources : (s + 1) * sources, :].astype(BF).astype(F32)
+    hidden = [hidden_ref[(place_ref[0] + 4 - k) % 4] for k in range(4)]
+    down = [ref[ref.shape[0] - 512 :, :] for ref in (p0, p1, p2, p3)]
+    result = lax.dot_general(
+        jnp.concatenate(hidden, axis=1),
+        jnp.concatenate(down, axis=1),
+        (((1,), (1,)), ((), ())),
+        preferred_element_type=F32,
+    )
+    for s in range(SLOTS):
+        rows = result[s * sources : (s + 1) * sources, :]
         out_ref[:, :, s * 128 : (s + 1) * 128] = rows.reshape(sources, 4, 128).astype(BF)
+
+
+def place_kernel(rows_ref, weight_ref, gate_ref, up_ref, down_ref):
+    gate_ref[...] = weight_ref[:, :, :128]
+    up_ref[...] = weight_ref[:, :, 128:]
+    down_ref[...] = rows_ref[...].astype(F32).T.astype(BF)
 
 
 def share_kernel(routes_ref, weight_ref, high_ref, low_ref):
@@ -171,10 +193,12 @@
 
 
 def local(tokens, routes, route_weight, gain, gate_weight, up_weight, down_weight):
+    place = lax.axis_index("tp").astype(jnp.int32).reshape(1)
     fs = lax.axis_size("fs")
     count = tokens.shape[0]
     rows = SLOTS * fs
-    wide = SLOTS * 128 + 512
+    main = 240
+    scalar = [pl.BlockSpec(memory_space=pltpu.SMEM)]
     hbm = pl.BlockSpec(memory_space=pltpu.HBM)
     plain = jax.ShapeDtypeStruct
     routes = routes.T
@@ -183,7 +207,7 @@
     packed = call(
         pack_kernel,
         "pack",
-        plain((fs, 4, wide), BF),
+        plain((fs, 4, SLOTS * 128 + 512), BF),
         vmem(1) + [hbm, hbm],
         (far(routes), far(tokens), far(jnp.transpose(down_weight, (0, 2, 1)))),
         [
@@ -195,38 +219,57 @@
     got = near(lax.all_to_all(packed, "fs", 0, 0, tiled=True))
 
     gain_rows = gain[None, :, None]
-    gate_new = (gain_rows * gate_weight).astype(BF)
-    up_new = (gain_rows * up_weight).astype(BF)
-    both = lax.all_to_all(jnp.concatenate((gate_new, up_new), axis=2), "fs", 0, 0, tiled=True)
-
-    part = pltpu.VMEM((rows // 2, 512), BF)
-    low, high, down = call(
-        unpack_kernel, "unpack", (part, part, plain((fs, 16, 128), BF)), vmem(1), (got,)
-    )
-    low = lax.all_gather(low, "tp", axis=0, tiled=False)
-    low, high = lax.optimization_barrier((low, high))
-    high = lax.all_gather(high, "tp", axis=0, tiled=False)
-    low, high = near(low), near(high)
-    scale = call(scale_kernel, "scale", pltpu.VMEM((rows, 128), F32), vmem(2), (low, high))
-    payload = call(
+    weights = [(gain_rows * w).astype(BF) for w in (gate_weight, up_weight)]
+    weights = near(lax.all_to_all(jnp.concatenate(weights, axis=2), "fs", 0, 0, tiled=True))
+
+    piece = pltpu.VMEM((4 * (rows - main) + 512, 128), BF)
+    part = plain((fs, 16, 128), BF)
+    down, gathered, *pieces = call(
+        unpack_kernel,
+        "unpack",
+        (part, pltpu.VMEM((main, 512), BF), piece, piece, piece, piece),
+        scalar + vmem(1),
+        (place, got),
+    )
+    own = pieces[0]
+    moved = {
+        k: near(lax.ppermute(pieces[k], "tp", [(i, (i + k) % 4) for i in range(4)]))
+        for k in (1, 3, 2)
+    }
+    pieces = (own, moved[1], moved[2], moved[3])
+    gathered = near(lax.all_gather(gathered, "tp", axis=0, tiled=False))
+    scale = call(
+        scale_kernel, "scale", pltpu.VMEM((rows, 128), F32), vmem(5), (gathered, *pieces)
+    )
+    hidden = call(
         hidden_kernel,
         "hidden",
-        plain((4, rows + 512, 128), BF),
-        vmem(5),
-        (low, high, scale, near(both.reshape(4, 512, 256)), down.reshape(4, 512, 128)),
-    )
-    payload = near(lax.all_to_all(payload, "tp", 0, 0, tiled=True))
-    result = call(expert_kernel, "expert", plain((fs, 4, SLOTS * 128), BF), vmem(1), (payload,))
+        pltpu.VMEM((rows, 128), BF),
+        scalar + vmem(7),
+        (place, gathered, *pieces, scale, weights),
+    )
+    hidden = near(lax.all_gather(hidden, "tp", axis=0, tiled=False))
+    result = call(
+        expert_kernel,
+        "expert",
+        plain((fs, 4, SLOTS * 128), BF),
+        scalar + vmem(5),
+        (place, hidden, *pieces),
+    )
     back = near(lax.all_to_all(result, "fs", 0, 0, tiled=True))
 
     pair = pltpu.VMEM((SLOTS, count, fs), BF)
     shares = call(share_kernel, "share", (pair, pair), vmem(2), (routes, route_weight))
     mixed = call(mix_kernel, "mix", plain((count, 512), BF), vmem(3), (*shares, back))
-    down_out = call(
-        down_kernel, "down", plain((128, fs * 16), BF), vmem(1), (down.reshape(fs * 16, 128),)
-    )
-    both = both.reshape(1, fs * 16, 256)
-    return (both[:, :, :128], both[:, :, 128:], down_out[None], mixed)
+    gate_out, up_out, down_out = call(
+        place_kernel,
+        "place",
+        (part, part, plain((128, fs * 16), BF)),
+        vmem(2),
+        (far(down.reshape(fs * 16, 128)), weights),
+    )
+    wide = (1, fs * 16, 128)
+    return (gate_out.reshape(wide), up_out.reshape(wide), down_out[None], mixed)
 
 
 def solution(mesh):

time: 134 us -> 137 us (1.022)
  starting transfers between devices: 32.4 us -> 51.1 us
  blocking collectives: 41.1 us -> 29.3 us
  waiting for transfers between devices: 49 us -> 43.7 us
    all_to_all x1 -> x0, blocking collectives: 17.2 us -> none  [local(): payload = near(lax.all_to_all(payload, 'tp', 0, 0, tiled=True))]
    ppermute x0 -> x3, starting transfers between devices: none -> 10.5 us  [local(): lax.ppermute(pieces[k], 'tp', [(i, (i + k) % 4) for i in range(4)])]
    all_to_all x1, starting transfers between devices: 7.92 us -> 16.1 us  [local(): back = near(lax.all_to_all(result, 'fs', 0, 0, tiled=True))]
    all_gather x2, blocking collectives: 23.9 us -> 29.3 us  [the longest x1 18.2 us: local(): gathered = near(lax.all_gather(gathered, 'tp', axis=0, tiled=False))]
    all_to_all x1, waiting for transfers between devices: 6.24 us -> 1.32 us  [local(): lax.all_to_all(jnp.concatenate(weights, axis=2), 'fs', 0, 0, tiled=True)]
  transfers between devices with their start and end apart: 3 -> 6, of which waited for: 3 -> 3; matrix products, arithmetic and copies ran while one was open for 2% -> 1% of each run, Pallas kernels for 2% -> 3%
where the time goes in v5:
time: 137 us; the launch traced here: 136 us
  starting transfers between devices  51.1 us (37%)
  waiting for transfers between devices  43.7 us (32%)
  blocking collectives  29.3 us (21%)
  Pallas kernels  9.68 us (7%)
    all_to_all x1, waiting for transfers between devices, local(): got = near(lax.all_to_all(packed, 'fs', 0, 0, tiled=True))  27.2 us
    all_to_all x1, starting transfers between devices, local(): got = near(lax.all_to_all(packed, 'fs', 0, 0, tiled=True))  18.6 us
    all_gather x1, blocking collectives, local(): gathered = near(lax.all_gather(gathered, 'tp', axis=0, tiled=False))  18.2 us
    all_to_all x1, starting transfers between devices, local(): back = near(lax.all_to_all(result, 'fs', 0, 0, tiled=True))  16.1 us
    all_to_all x1, waiting for transfers between devices, local(): back = near(lax.all_to_all(result, 'fs', 0, 0, tiled=True))  15.2 us
    all_gather x1, blocking collectives, local(): hidden = near(lax.all_gather(hidden, 'tp', axis=0, tiled=False))  11.1 us
    ppermute x3, starting transfers between devices, local(): lax.ppermute(pieces[k], 'tp', [(i, (i + k) % 4) for i in range(4)])  10.5 us
    pallas_call x8, Pallas kernels, call(): pl.pallas_call(kernel, out_shape=outs, in_specs=in_specs, out_specs=tuple...  9.68 us
  transfers between devices with their start and end apart: 6, of which 3 were waited for; matrix products, arithmetic and copies ran while one was open for 1% of the time, Pallas kernels for 3%

profile of v5, /device:TPU:1, one launch (start us, length us, event | category | flops | bytes accessed | tf_op | source)
XLA Modules:
  0.0 136.0 jit_solution(14627932912258590012)
XLA Ops:
  0.6 0.0 copy-start.4
  0.6 3.2 %pack.1 = bf16[128,4,896]{2,1,0:T(4,128)(2,1)} custom-call(s32[2,128]{1,0:T(2,128)} %bitcast.14, bf16[128,512]{1,0:T(8,128)(2,1)} %tokens_hbm.1, f32[128,16,128]{2,1,0:T(8,128)} %bitcast.17), custom_call_target="tpu_custom_call" | custom-call | tf_op jit(solution)/shard_map/pack/pallas_call | solution.py:184
  3.9 0.0 copy-start.3
  3.9 0.0 copy-start.5
  3.9 18.6 %all-to-all-start = ((bf16[128,4,896]{2,1,0:T(4,128)(2,1)}), bf16[128,4,896]{2,1,0:T(4,128)(2,1)S(1)}, u32[]{:S(2)}, u32[]{:S(2)}) async-start(bf16[128,4,896]{2,1,0:T(4,128)(2,1)} %pack.1), calls=%async_computation | async-start | bytes 1835008 | tf_op jit(solution)/shard_map/all_to_all | solution.py:219
  22.4 0.0 copy-done.4
  22.5 0.0 copy-done.3
  22.5 0.0 copy-done.5
  22.5 0.2 multiply_convert_fusion.1
  22.7 1.1 pad_maximum_fusion
  23.8 27.2 %all-to-all-done.got_ref = bf16[128,4,896]{2,1,0:T(4,128)(2,1)S(1)} async-done(((bf16[128,4,896]{2,1,0:T(4,128)(2,1)}), bf16[128,4,896]{2,1,0:T(4,128)(2,1)S(1)}, u32[]{:S(2)}, u32[]{:S(2)}) %all-to-all-start) | async-done | bytes 917536 | tf_op jit(solution)/shard_map/all_to_all | solution.py:219
  51.0 5.9 %all-to-all-start.1 = ((bf16[128,16,256]{2,1,0:T(8,128)(2,1)}), bf16[128,16,256]{2,1,0:T(8,128)(2,1)S(1)}, u32[]{:S(2)}, u32[]{:S(2)}) async-start(bf16[128,16,256]{2,1,0:T(8,128)(2,1)} %pad_maximum_fusion), calls=%async_computation.1 | async-start | bytes 2097152 | tf_op jit(solution)/shard_map/all_to_all | solution.py:223
  57.0 0.5 unpack.1
  57.5 0.0 copy-start
  57.5 3.1 %collective-permute-start = (bf16[1088,128]{1,0:T(8,128)(2,1)S(1)}, bf16[1088,128]{1,0:T(8,128)(2,1)S(1)}, u32[]{:S(2)}, u32[]{:S(2)}) collective-permute-start(bf16[1088,128]{1,0:T(8,128)(2,1)S(1)} %get-tuple-element.23), channel_id=1, source_target_pairs={{0,1},{1,2},{2,3},{3,0},{4,5},{5,6},{6,7},{7,4},{8,9},{9,10},{10,1... | collective-permute-start | bytes 835592 | tf_op jit(solution)/shard_map/ppermute | solution.py:236
  60.6 4.4 %collective-permute-start.1 = (bf16[1088,128]{1,0:T(8,128)(2,1)S(1)}, bf16[1088,128]{1,0:T(8,128)(2,1)S(1)}, u32[]{:S(2)}, u32[]{:S(2)}) collective-permute-start(bf16[1088,128]{1,0:T(8,128)(2,1)S(1)} %get-tuple-element.24), channel_id=1, source_target_pairs={{0,2},{1,3},{2,0},{3,1},{4,6},{5,7},{6,4},{7,5},{8,10},{9,11},{10,... | collective-permute-start | bytes 835592 | tf_op jit(solution)/shard_map/ppermute | solution.py:236
  65.0 3.1 %collective-permute-start.2 = (bf16[1088,128]{1,0:T(8,128)(2,1)S(1)}, bf16[1088,128]{1,0:T(8,128)(2,1)S(1)}, u32[]{:S(2)}, u32[]{:S(2)}) collective-permute-start(bf16[1088,128]{1,0:T(8,128)(2,1)S(1)} %get-tuple-element.25), channel_id=1, source_target_pairs={{0,3},{1,0},{2,1},{3,2},{4,7},{5,4},{6,5},{7,6},{8,11},{9,8},{10,9... | collective-permute-start | bytes 835592 | tf_op jit(solution)/shard_map/ppermute | solution.py:236
  68.0 18.2 %all-gather = bf16[960,512]{1,0:T(8,128)(2,1)S(1)} all-gather(bf16[240,512]{1,0:T(8,128)(2,1)S(1)} %get-tuple-element.21), channel_id=2, replica_groups=mesh['fs'=128,'tp'=4] {'tp'}, dimensions={0}, use_global_device_ids=true | all-gather | bytes 1228800 | tf_op jit(solution)/shard_map/all_gather | solution.py:240
  86.2 0.0 collective-permute-done.p1
  86.2 0.0 collective-permute-done.1.p2
  86.2 0.0 collective-permute-done.2.p3
  86.2 0.0 copy-done
  86.2 0.3 scale.1.scale_ref
  86.6 1.3 all-to-all-done.1.weight_ref
  87.9 0.6 hidden.1
  88.5 11.1 %all-gather.1 = bf16[1536,128]{1,0:T(8,128)(2,1)S(1)} all-gather(bf16[384,128]{1,0:T(8,128)(2,1)S(1)} %hidden.1), channel_id=3, replica_groups=mesh['fs'=128,'tp'=4] {'tp'}, dimensions={0}, use_global_device_ids=true | all-gather | bytes 491520 | tf_op jit(solution)/shard_map/all_gather | solution.py:251
  99.7 0.0 copy-start.1
  99.7 0.0 copy-start.2
  99.7 1.3 expert.1
  100.9 16.1 %all-to-all-start.2 = ((bf16[128,4,384]{2,1,0:T(4,128)(2,1)}), bf16[128,4,384]{2,1,0:T(4,128)(2,1)S(1)}, u32[]{:S(2)}, u32[]{:S(2)}) async-start(bf16[128,4,384]{2,1,0:T(4,128)(2,1)} %expert.1), calls=%async_computation.2 | async-start | bytes 786432 | tf_op jit(solution)/shard_map/all_to_all | solution.py:259
  117.1 0.0 copy-done.1
  117.1 0.0 copy-done.2
  117.1 0.3 share.1
  117.4 2.4 %place.1 = (bf16[128,16,128]{2,1,0:T(8,128)(2,1)}, bf16[128,16,128]{2,1,0:T(8,128)(2,1)}, bf16[128,2048]{1,0:T(8,128)(2,1)}) custom-call(bf16[2048,128]{1,0:T(8,128)(2,1)} %bitcast.13, bf16[128,16,256]{2,1,0:T(8,128)(2,1)S(1)} %all-to-all-done.1.weight_ref), custom_call_target="tpu_custom_call" | custom-call | tf_op jit(solution)/shard_map/place/pallas_call | solution.py:184
  119.8 15.2 %all-to-all-done.2.back_ref = bf16[128,4,384]{2,1,0:T(4,128)(2,1)S(1)} async-done(((bf16[128,4,384]{2,1,0:T(4,128)(2,1)}), bf16[128,4,384]{2,1,0:T(4,128)(2,1)S(1)}, u32[]{:S(2)}, u32[]{:S(2)}) %all-to-all-start.2) | async-done | bytes 393248 | tf_op jit(solution)/shard_map/all_to_all | solution.py:259
  134.9 1.1 mix.1
Async XLA Ops:
  0.6 21.8 %copy-start.4 = (f32[128,16,128]{2,1,0:T(8,128)S(1)}, f32[128,16,128]{2,1,0:T(8,128)}, u32[]{:S(2)}) copy-start(f32[128,16,128]{2,1,0:T(8,128)} %param.12) | copy-start | bytes 3145732
  3.9 18.6 %copy-start.3 = (f32[128,16,128]{2,1,0:T(8,128)S(1)}, f32[128,16,128]{2,1,0:T(8,128)}, u32[]{:S(2)}) copy-start(f32[128,16,128]{2,1,0:T(8,128)} %param.11) | copy-start | bytes 3145732
  3.9 18.6 %copy-start.5 = (f32[16]{0:T(128)S(1)}, f32[16]{0:T(128)}, u32[]{:S(2)}) copy-start(f32[16]{0:T(128)} %param.10) | copy-start | bytes 196
  3.9 47.1 %all-to-all-start = ((bf16[128,4,896]{2,1,0:T(4,128)(2,1)}), bf16[128,4,896]{2,1,0:T(4,128)(2,1)S(1)}, u32[]{:S(2)}, u32[]{:S(2)}) async-start(bf16[128,4,896]{2,1,0:T(4,128)(2,1)} %pack.1), calls=%async_computation | async-start | bytes 1835008 | tf_op jit(solution)/shard_map/all_to_all | solution.py:219
  51.0 36.9 %all-to-all-start.1 = ((bf16[128,16,256]{2,1,0:T(8,128)(2,1)}), bf16[128,16,256]{2,1,0:T(8,128)(2,1)S(1)}, u32[]{:S(2)}, u32[]{:S(2)}) async-start(bf16[128,16,256]{2,1,0:T(8,128)(2,1)} %pad_maximum_fusion), calls=%async_computation.1 | async-start | bytes 2097152 | tf_op jit(solution)/shard_map/all_to_all | solution.py:223
  57.5 28.8 %copy-start = (bf16[128,16,128]{2,1,0:T(8,128)(2,1)}, bf16[128,16,128]{2,1,0:T(8,128)(2,1)S(1)}, u32[]{:S(2)}) copy-start(bf16[128,16,128]{2,1,0:T(8,128)(2,1)S(1)} %get-tuple-element.15) | copy-start | bytes 1572868
  57.5 28.7 %collective-permute-start = (bf16[1088,128]{1,0:T(8,128)(2,1)S(1)}, bf16[1088,128]{1,0:T(8,128)(2,1)S(1)}, u32[]{:S(2)}, u32[]{:S(2)}) collective-permute-start(bf16[1088,128]{1,0:T(8,128)(2,1)S(1)} %get-tuple-element.23), channel_id=1, source_target_pairs={{0,1},{1,2},{2,3},{3,0},{4,5},{5,6},{6,7},{7,4},{8,9},{9,10},{10,1... | collective-permute-start | bytes 835592 | tf_op jit(solution)/shard_map/ppermute | solution.py:236
  60.6 25.6 %collective-permute-start.1 = (bf16[1088,128]{1,0:T(8,128)(2,1)S(1)}, bf16[1088,128]{1,0:T(8,128)(2,1)S(1)}, u32[]{:S(2)}, u32[]{:S(2)}) collective-permute-start(bf16[1088,128]{1,0:T(8,128)(2,1)S(1)} %get-tuple-element.24), channel_id=1, source_target_pairs={{0,2},{1,3},{2,0},{3,1},{4,6},{5,7},{6,4},{7,5},{8,10},{9,11},{10,... | collective-permute-start | bytes 835592 | tf_op jit(solution)/shard_map/ppermute | solution.py:236
  65.0 21.3 %collective-permute-start.2 = (bf16[1088,128]{1,0:T(8,128)(2,1)S(1)}, bf16[1088,128]{1,0:T(8,128)(2,1)S(1)}, u32[]{:S(2)}, u32[]{:S(2)}) collective-permute-start(bf16[1088,128]{1,0:T(8,128)(2,1)S(1)} %get-tuple-element.25), channel_id=1, source_target_pairs={{0,3},{1,0},{2,1},{3,2},{4,7},{5,4},{6,5},{7,6},{8,11},{9,8},{10,9... | collective-permute-start | bytes 835592 | tf_op jit(solution)/shard_map/ppermute | solution.py:236
  99.7 17.4 %copy-start.1 = (s32[128,2]{0,1:T(2,128)S(1)}, s32[128,2]{0,1:T(2,128)}, u32[]{:S(2)}) copy-start(s32[128,2]{0,1:T(2,128)} %param.8) | copy-start | bytes 3076
  99.7 17.4 %copy-start.2 = (f32[128,2]{0,1:T(2,128)S(1)}, f32[128,2]{0,1:T(2,128)}, u32[]{:S(2)}) copy-start(f32[128,2]{0,1:T(2,128)} %param.9) | copy-start | bytes 3076
  100.9 34.0 %all-to-all-start.2 = ((bf16[128,4,384]{2,1,0:T(4,128)(2,1)}), bf16[128,4,384]{2,1,0:T(4,128)(2,1)S(1)}, u32[]{:S(2)}, u32[]{:S(2)}) async-start(bf16[128,4,384]{2,1,0:T(4,128)(2,1)} %expert.1), calls=%async_computation.2 | async-start | bytes 786432 | tf_op jit(solution)/shard_map/all_to_all | solution.py:259

commit v6 on v4

--- a/solution.py
+++ b/solution.py
@@ -39,14 +39,24 @@
     return first, hit, order
 
 
-def pack_kernel(routes_ref, tokens_ref, out_ref):
+def pack_kernel(routes_ref, tokens_ref, out_ref, rows_ref, sems):
     _, hit, order = slot_hits(routes_ref[...])
     tokens = tokens_ref[...]
-    experts = out_ref.shape[0]
-    for s in range(SLOTS):
-        chosen = jnp.where((hit > 0.0) & (order == float(s)), 1.0, 0.0).astype(BF)
-        rows = jnp.dot(chosen, tokens, preferred_element_type=F32)
-        out_ref[:, :, s * 128 : (s + 1) * 128] = rows.reshape(experts, 4, 128).astype(BF)
+    step = rows_ref.shape[0] // 2
+    chosen = [jnp.where((hit > 0.0) & (order == float(s)), 1.0, 0.0).astype(BF) for s in range(SLOTS)]
+    copies = []
+    for h in range(2):
+        piece = slice(h * step, (h + 1) * step)
+        rows = jnp.dot(
+            jnp.concatenate([c[piece] for c in chosen], axis=0), tokens, preferred_element_type=F32
+        )
+        for s in range(SLOTS):
+            part = rows[s * step : (s + 1) * step].reshape(step, 4, 128)
+            rows_ref[piece, :, s * 128 : (s + 1) * 128] = part.astype(BF)
+        copies.append(pltpu.make_async_copy(rows_ref.at[piece], out_ref.at[piece], sems.at[h]))
+        copies[-1].start()
+    for copy in copies:
+        copy.wait()
 
 
 def unpack_kernel(got_ref, low_ref, high_ref):
@@ -109,41 +119,40 @@
 def expert_kernel(got_ref, out_ref):
     sources = out_ref.shape[0]
     total = SLOTS * sources
-    acc = None
-    for k in range(4):
-        part = lax.dot_general(
-            got_ref[k, :total, :],
-            got_ref[k, total:, :],
-            (((1,), (1,)), ((), ())),
-            preferred_element_type=F32,
-        )
-        acc = part if acc is None else acc + part
-    for s in range(SLOTS):
-        rows = acc[s * sources : (s + 1) * sources, :].astype(BF).astype(F32)
+    result = lax.dot_general(
+        jnp.concatenate([got_ref[k, :total, :] for k in range(4)], axis=1),
+        jnp.concatenate([got_ref[k, total:, :] for k in range(4)], axis=1),
+        (((1,), (1,)), ((), ())),
+        preferred_element_type=F32,
+    )
+    for s in range(SLOTS):
+        rows = result[s * sources : (s + 1) * sources, :]
         out_ref[:, :, s * 128 : (s + 1) * 128] = rows.reshape(sources, 4, 128).astype(BF)
 
 
-def share_kernel(routes_ref, weight_ref, high_ref, low_ref):
+def share_kernel(routes_ref, weight_ref, out_ref):
     first, hit, order = slot_hits(routes_ref[...])
     weight = weight_ref[...]
     share = weight / jnp.sum(weight, axis=0, keepdims=True)
     mine = jnp.where(first, share[0:1, :], share[1:2, :])
+    count = out_ref.shape[0] // 2
     for s in range(SLOTS):
         part = jnp.where((hit > 0.0) & (order == float(s)), mine, 0.0).T
         high = part.astype(BF)
-        high_ref[s] = high
-        low_ref[s] = (part - high.astype(F32)).astype(BF)
-
-
-def mix_kernel(high_ref, low_ref, back_ref, out_ref):
+        columns = slice(s * part.shape[1], (s + 1) * part.shape[1])
+        out_ref[:count, columns] = high
+        out_ref[count:, columns] = (part - high.astype(F32)).astype(BF)
+
+
+def mix_kernel(share_ref, back_ref, out_ref):
     experts = back_ref.shape[0]
-    acc = None
-    for s in range(SLOTS):
-        rows = back_ref[:, :, s * 128 : (s + 1) * 128].astype(F32).reshape(experts, 512).astype(BF)
-        part = jnp.dot(high_ref[s], rows, preferred_element_type=F32)
-        part = part + jnp.dot(low_ref[s], rows, preferred_element_type=F32)
-        acc = part if acc is None else acc + part
-    out_ref[...] = acc.astype(BF)
+    blocks = []
+    for s in range(SLOTS):
+        block = back_ref[:, :, s * 128 : (s + 1) * 128].astype(F32)
+        blocks.append(block.reshape(experts, 512).astype(BF))
+    both = jnp.dot(share_ref[...], jnp.concatenate(blocks, axis=0), preferred_element_type=F32)
+    count = out_ref.shape[0]
+    out_ref[...] = (both[:count] + both[count:]).astype(BF)
 
 
 def call(kernel, name, outs, in_specs, args, scratch=()):
@@ -167,9 +176,16 @@
     routes = routes.T
     route_weight = route_weight.T
 
-    packed = call(
-        pack_kernel, "pack", plain((fs, 4, SLOTS * 128), BF), vmem(2), (far(routes), far(tokens))
-    )
+    slots = (fs, 4, SLOTS * 128)
+    packed = pl.pallas_call(
+        pack_kernel,
+        out_shape=plain(slots, BF),
+        in_specs=vmem(2),
+        out_specs=pl.BlockSpec(memory_space=pltpu.HBM),
+        scratch_shapes=[pltpu.VMEM(slots, BF), pltpu.SemaphoreType.DMA((2,))],
+        compiler_params=LIMIT,
+        name="pack",
+    )(far(routes), far(tokens))
     got = near(lax.all_to_all(packed, "fs", 0, 0, tiled=True))
 
     gain_rows = gain[None, :, None]
@@ -195,9 +211,10 @@
     result = call(expert_kernel, "expert", plain((fs, 4, SLOTS * 128), BF), vmem(1), (payload,))
     back = near(lax.all_to_all(result, "fs", 0, 0, tiled=True))
 
-    pair = pltpu.VMEM((SLOTS, count, fs), BF)
-    shares = call(share_kernel, "share", (pair, pair), vmem(2), (routes, route_weight))
-    mixed = call(mix_kernel, "mix", plain((count, 512), BF), vmem(3), (*shares, back))
+    shares = call(
+        share_kernel, "share", pltpu.VMEM((2 * count, rows), BF), vmem(2), (routes, route_weight)
+    )
+    mixed = call(mix_kernel, "mix", plain((count, 512), BF), vmem(2), (shares, back))
     part = plain((fs, 16, 128), BF)
     gate_out, up_out, down_out = call(
         place_kernel, "place", (part, part, plain((128, fs * 16), BF)), vmem(1), (weights,)

time: 133 us -> 133 us (level)
    pallas_call x8 -> x7, Pallas kernels: 7.58 us -> 5.07 us  [call(): pl.pallas_call(kernel, out_shape=outs, in_specs=in_specs, out_specs=tuple...]
    pallas_call x0 -> x1, Pallas kernels: none -> 2.23 us  [local(): pl.pallas_call(pack_kernel, out_shape=plain(slots, BF), in_specs=vmem(2),...]
where the time goes in v6:
time: 133 us; the launch traced here: 132 us
  waiting for transfers between devices  48 us (36%)
  blocking collectives  40.6 us (31%)
  starting transfers between devices  32.6 us (25%)
  Pallas kernels  7.3 us (5%)
  other arithmetic  2.8 us (2%)
    all_to_all x1, starting transfers between devices, local(): got = near(lax.all_to_all(packed, 'fs', 0, 0, tiled=True))  18.4 us
    all_to_all x1, waiting for transfers between devices, local(): weights = near(lax.all_to_all(weights, 'fs', 0, 0, tiled=True))  16.7 us
    all_to_all x1, blocking collectives, local(): payload = near(lax.all_to_all(payload, 'tp', 0, 0, tiled=True))  16.6 us
    all_to_all x1, waiting for transfers between devices, local(): back = near(lax.all_to_all(result, 'fs', 0, 0, tiled=True))  16.3 us
    all_to_all x1, waiting for transfers between devices, local(): got = near(lax.all_to_all(packed, 'fs', 0, 0, tiled=True))  15 us
    all_gather x1, blocking collectives, local(): low = lax.all_gather(low, 'tp', axis=0, tiled=False)  12.7 us
    all_gather x1, blocking collectives, local(): high = lax.all_gather(high, 'tp', axis=0, tiled=False)  11.3 us
    all_to_all x1, starting transfers between devices, local(): back = near(lax.all_to_all(result, 'fs', 0, 0, tiled=True))  8.69 us
  transfers between devices with their start and end apart: 3, of which 3 were waited for; matrix products, arithmetic and copies ran while one was open for 2% of the time, Pallas kernels for 2%

profile of v6, /device:TPU:1, one launch (start us, length us, event | category | flops | bytes accessed | tf_op | source)
XLA Modules:
  0.0 132.1 jit_solution(10379337846684880112)
XLA Ops:
  0.6 0.0 copy-start.2
  0.6 0.0 copy-start.4
  0.7 0.0 copy-start.3
  0.7 2.2 %pack.1 = bf16[128,4,384]{2,1,0:T(4,128)(2,1)} custom-call(s32[2,128]{1,0:T(2,128)} %bitcast.13, bf16[128,512]{1,0:T(8,128)(2,1)} %tokens_ref.1), custom_call_target="tpu_custom_call" | custom-call | tf_op jit(solution)/shard_map/pack/pallas_call | solution.py:180
  2.9 18.4 %all-to-all-start.1 = ((bf16[128,4,384]{2,1,0:T(4,128)(2,1)}), bf16[128,4,384]{2,1,0:T(4,128)(2,1)S(1)}, u32[]{:S(2)}, u32[]{:S(2)}) async-start(bf16[128,4,384]{2,1,0:T(4,128)(2,1)} %pack.1), calls=%async_computation.1 | async-start | bytes 786432 | tf_op jit(solution)/shard_map/all_to_all | solution.py:189
  21.3 0.0 copy-done.2
  21.3 0.1 convert_bitcast_fusion
  21.4 0.0 copy-done.4
  21.4 0.0 copy-done.3
  21.4 1.5 %multiply_convert_fusion.1 = (bf16[128,16,128]{2,1,0:T(8,128)(2,1)S(1)}, bf16[128,16,128]{2,1,0:T(8,128)(2,1)S(1)}) fusion(f32[128,16,128]{2,1,0:T(8,128)S(1)} %copy-done.3, f32[16]{0:T(128)S(1)} %copy-done.4, f32[128,16,128]{2,1,0:T(8,128)} %param.12), kind=kLoop, calls=%fused_computation.2 | loop fusion | flops 1048576 | bytes 3145792 | tf_op jit(solution)/shard_map/convert_element_type | solution.py:193
  22.9 1.3 pad_maximum_fusion
  24.2 15.0 %all-to-all-done.1.got_ref = bf16[128,4,384]{2,1,0:T(4,128)(2,1)S(1)} async-done(((bf16[128,4,384]{2,1,0:T(4,128)(2,1)}), bf16[128,4,384]{2,1,0:T(4,128)(2,1)S(1)}, u32[]{:S(2)}, u32[]{:S(2)}) %all-to-all-start.1) | async-done | bytes 393248 | tf_op jit(solution)/shard_map/all_to_all | solution.py:189
  39.2 5.5 %all-to-all-start = ((bf16[128,48,128]{2,1,0:T(8,128)(2,1)}), bf16[128,48,128]{2,1,0:T(8,128)(2,1)S(1)}, u32[]{:S(2)}, u32[]{:S(2)}) async-start(bf16[128,48,128]{2,1,0:T(8,128)(2,1)} %pad_maximum_fusion), calls=%async_computation | async-start | bytes 3145728 | tf_op jit(solution)/shard_map/all_to_all | solution.py:194
  44.7 0.2 unpack.1
  44.9 12.7 %all-gather = bf16[768,512]{1,0:T(8,128)(2,1)S(1)} all-gather(bf16[192,512]{1,0:T(8,128)(2,1)S(1)} %get-tuple-element.14), channel_id=2, replica_groups=mesh['fs'=128,'tp'=4] {'tp'}, dimensions={0}, use_global_device_ids=true | all-gather | bytes 983040 | tf_op jit(solution)/shard_map/all_gather | solution.py:198
  57.6 11.3 %all-gather.1 = bf16[768,512]{1,0:T(8,128)(2,1)S(1)} all-gather(bf16[192,512]{1,0:T(8,128)(2,1)S(1)} %get-tuple-element.17), channel_id=3, replica_groups=mesh['fs'=128,'tp'=4] {'tp'}, dimensions={0}, use_global_device_ids=true | all-gather | bytes 983040 | tf_op jit(solution)/shard_map/all_gather | solution.py:200
  68.9 0.4 scale.1.scale_ref
  69.3 16.7 %all-to-all-done.weight_ref = bf16[128,48,128]{2,1,0:T(8,128)(2,1)S(1)} async-done(((bf16[128,48,128]{2,1,0:T(8,128)(2,1)}), bf16[128,48,128]{2,1,0:T(8,128)(2,1)S(1)}, u32[]{:S(2)}, u32[]{:S(2)}) %all-to-all-start) | async-done | bytes 1572896 | tf_op jit(solution)/shard_map/all_to_all | solution.py:194
  86.0 0.6 hidden.1
  86.6 0.0 copy-start
  86.6 0.0 copy-start.1
  86.6 16.6 %all_to_all.20.got_ref = bf16[4,896,128]{2,1,0:T(8,128)(2,1)S(1)} all-to-all(bf16[4,896,128]{2,1,0:T(8,128)(2,1)S(1)} %hidden.1), channel_id=1, replica_groups=mesh['fs'=128,'tp'=4] {'tp'}, dimensions={0} | all-to-all | bytes 1835008 | tf_op jit(solution)/shard_map/all_to_all | solution.py:210
  103.2 1.2 expert.1
  104.5 8.7 %all-to-all-start.3 = ((bf16[128,4,384]{2,1,0:T(4,128)(2,1)}), bf16[128,4,384]{2,1,0:T(4,128)(2,1)S(1)}, u32[]{:S(2)}, u32[]{:S(2)}) async-start(bf16[128,4,384]{2,1,0:T(4,128)(2,1)} %expert.1), calls=%async_computation.3 | async-start | bytes 786432 | tf_op jit(solution)/shard_map/all_to_all | solution.py:212
  113.2 0.0 copy-done
  113.2 0.0 copy-done.1
  113.2 0.3 share.1.share_ref
  113.5 1.3 place.1
  114.8 16.3 %all-to-all-done.3.back_ref = bf16[128,4,384]{2,1,0:T(4,128)(2,1)S(1)} async-done(((bf16[128,4,384]{2,1,0:T(4,128)(2,1)}), bf16[128,4,384]{2,1,0:T(4,128)(2,1)S(1)}, u32[]{:S(2)}, u32[]{:S(2)}) %all-to-all-start.3) | async-done | bytes 393248 | tf_op jit(solution)/shard_map/all_to_all | solution.py:212
  131.0 1.1 mix.1
Async XLA Ops:
  0.6 20.7 %copy-start.2 = (f32[128,128,16]{1,2,0:T(8,128)S(1)}, f32[128,128,16]{1,2,0:T(8,128)}, u32[]{:S(2)}) copy-start(f32[128,128,16]{1,2,0:T(8,128)} %param.13) | copy-start | bytes 3145732
  0.6 20.8 %copy-start.4 = (f32[16]{0:T(128)S(1)}, f32[16]{0:T(128)}, u32[]{:S(2)}) copy-start(f32[16]{0:T(128)} %param.10) | copy-start | bytes 196
  0.7 20.8 %copy-start.3 = (f32[128,16,128]{2,1,0:T(8,128)S(1)}, f32[128,16,128]{2,1,0:T(8,128)}, u32[]{:S(2)}) copy-start(f32[128,16,128]{2,1,0:T(8,128)} %param.11) | copy-start | bytes 3145732
  2.9 36.3 %all-to-all-start.1 = ((bf16[128,4,384]{2,1,0:T(4,128)(2,1)}), bf16[128,4,384]{2,1,0:T(4,128)(2,1)S(1)}, u32[]{:S(2)}, u32[]{:S(2)}) async-start(bf16[128,4,384]{2,1,0:T(4,128)(2,1)} %pack.1), calls=%async_computation.1 | async-start | bytes 786432 | tf_op jit(solution)/shard_map/all_to_all | solution.py:189
  39.2 46.8 %all-to-all-start = ((bf16[128,48,128]{2,1,0:T(8,128)(2,1)}), bf16[128,48,128]{2,1,0:T(8,128)(2,1)S(1)}, u32[]{:S(2)}, u32[]{:S(2)}) async-start(bf16[128,48,128]{2,1,0:T(8,128)(2,1)} %pad_maximum_fusion), calls=%async_computation | async-start | bytes 3145728 | tf_op jit(solution)/shard_map/all_to_all | solution.py:194
  86.6 26.6 %copy-start = (s32[128,2]{0,1:T(2,128)S(1)}, s32[128,2]{0,1:T(2,128)}, u32[]{:S(2)}) copy-start(s32[128,2]{0,1:T(2,128)} %param.8) | copy-start | bytes 3076
  86.6 26.6 %copy-start.1 = (f32[128,2]{0,1:T(2,128)S(1)}, f32[128,2]{0,1:T(2,128)}, u32[]{:S(2)}) copy-start(f32[128,2]{0,1:T(2,128)} %param.9) | copy-start | bytes 3076
  104.5 26.5 %all-to-all-start.3 = ((bf16[128,4,384]{2,1,0:T(4,128)(2,1)}), bf16[128,4,384]{2,1,0:T(4,128)(2,1)S(1)}, u32[]{:S(2)}, u32[]{:S(2)}) async-start(bf16[128,4,384]{2,1,0:T(4,128)(2,1)} %expert.1), calls=%async_computation.3 | async-start | bytes 786432 | tf_op jit(solution)/shard_map/all_to_all | solution.py:212

commit v7 on v6

--- a/solution.py
+++ b/solution.py
@@ -59,6 +59,19 @@
         copy.wait()
 
 
+def cast_kernel(core_ref, gate_ref, up_ref, down_ref, gain_ref, keep_ref, send_ref):
+    gain = gain_ref[...][None]
+    for target, core in ((keep_ref, core_ref[0]), (send_ref, 1 - core_ref[0])):
+        target[:, :16, :] = (gate_ref[:, core] * gain).astype(BF)
+        target[:, 16:32, :] = (up_ref[:, core] * gain).astype(BF)
+        target[:, 32:, :] = down_ref[:, core].astype(BF)
+
+
+def join_kernel(core_ref, keep_ref, other_ref, out_ref):
+    out_ref[:, core_ref[0]] = keep_ref[...]
+    out_ref[:, 1 - core_ref[0]] = other_ref[...]
+
+
 def unpack_kernel(got_ref, low_ref, high_ref):
     sources = got_ref.shape[0]
     half = low_ref.shape[0]
@@ -155,7 +168,7 @@
     out_ref[...] = (both[:count] + both[count:]).astype(BF)
 
 
-def call(kernel, name, outs, in_specs, args, scratch=()):
+def call(kernel, outs, in_specs, args, scratch=()):
     many = isinstance(outs, tuple)
     return pl.pallas_call(
         kernel,
@@ -164,7 +177,6 @@
         out_specs=tuple(vmem(len(outs))) if many else vmem(1)[0],
         scratch_shapes=scratch,
         compiler_params=LIMIT,
-        name=name,
     )(*args)
 
 
@@ -186,38 +198,52 @@
         compiler_params=LIMIT,
         name="pack",
     )(far(routes), far(tokens))
-    got = near(lax.all_to_all(packed, "fs", 0, 0, tiled=True))
-
-    gain_rows = gain[None, :, None]
-    parts = (gain_rows * gate_weight, gain_rows * up_weight, jnp.transpose(down_weight, (0, 2, 1)))
-    weights = jnp.concatenate([p.astype(BF) for p in parts], axis=1)
-    weights = near(lax.all_to_all(weights, "fs", 0, 0, tiled=True))
+    got = lax.all_to_all(packed, "fs", 0, 0, tiled=True)
+    got = near(got)
+
+    scalar = [pl.BlockSpec(memory_space=pltpu.SMEM)]
+    core = (lax.axis_index("fs") % 2).astype(jnp.int32).reshape(1)
+    chips = fs // 2
+    by_chip = (chips, 2, 16, 128)
+    keep, send = call(
+        cast_kernel,
+        (plain((chips, 48, 128), BF),) * 2,
+        scalar + vmem(4),
+        (
+            core,
+            far(gate_weight.reshape(by_chip)),
+            far(up_weight.reshape(by_chip)),
+            far(jnp.transpose(down_weight, (0, 2, 1)).reshape(by_chip)),
+            jnp.broadcast_to(gain[:, None], (16, 128)),
+        ),
+    )
+    other = lax.ppermute(send, "fs", [(i, i ^ 1) for i in range(fs)])
+    joined = call(
+        join_kernel, plain((chips, 2, 48, 128), BF), scalar + vmem(2), (core, keep, other)
+    )
+    same_core = [[2 * m + c for m in range(chips)] for c in range(2)]
+    weights = lax.all_to_all(joined, "fs", 0, 0, tiled=True, axis_index_groups=same_core)
+    weights = near(weights.reshape(fs, 48, 128))
 
     part = pltpu.VMEM((rows // 2, 512), BF)
-    low, high = call(unpack_kernel, "unpack", (part, part), vmem(1), (got,))
+    low, high = call(unpack_kernel, (part, part), vmem(1), (got,))
     low = lax.all_gather(low, "tp", axis=0, tiled=False)
     low, high = lax.optimization_barrier((low, high))
     high = lax.all_gather(high, "tp", axis=0, tiled=False)
     low, high = near(low), near(high)
-    scale = call(scale_kernel, "scale", pltpu.VMEM((rows, 128), F32), vmem(2), (low, high))
+    scale = call(scale_kernel, pltpu.VMEM((rows, 128), F32), vmem(2), (low, high))
     payload = call(
-        hidden_kernel,
-        "hidden",
-        plain((4, rows + 512, 128), BF),
-        vmem(4),
-        (low, high, scale, weights),
+        hidden_kernel, plain((4, rows + 512, 128), BF), vmem(4), (low, high, scale, weights)
     )
     payload = near(lax.all_to_all(payload, "tp", 0, 0, tiled=True))
-    result = call(expert_kernel, "expert", plain((fs, 4, SLOTS * 128), BF), vmem(1), (payload,))
+    result = call(expert_kernel, plain((fs, 4, SLOTS * 128), BF), vmem(1), (payload,))
     back = near(lax.all_to_all(result, "fs", 0, 0, tiled=True))
 
-    shares = call(
-        share_kernel, "share", pltpu.VMEM((2 * count, rows), BF), vmem(2), (routes, route_weight)
-    )
-    mixed = call(mix_kernel, "mix", plain((count, 512), BF), vmem(2), (shares, back))
+    shares = call(share_kernel, pltpu.VMEM((2 * count, rows), BF), vmem(2), (routes, route_weight))
+    mixed = call(mix_kernel, plain((count, 512), BF), vmem(2), (shares, back))
     part = plain((fs, 16, 128), BF)
     gate_out, up_out, down_out = call(
-        place_kernel, "place", (part, part, plain((128, fs * 16), BF)), vmem(1), (weights,)
+        place_kernel, (part, part, plain((128, fs * 16), BF)), vmem(1), (weights,)
     )
     wide = (1, fs * 16, 128)
     return (gate_out.reshape(wide), up_out.reshape(wide), down_out[None], mixed)
@@ -234,4 +260,5 @@
         P(None, "tp", "fs"),
     )
     out_specs = (P("fs", None, "tp"), P("fs", None, "tp"), P("fs", "tp", None), P("fs", "tp"))
+
     return jax.shard_map(local, mesh=mesh, in_specs=in_specs, out_specs=out_specs, check_vma=False)

time: 133 us -> 137 us (1.030)
  starting transfers between devices: 32.6 us -> 38.1 us
  Pallas kernels: 7.3 us -> 10.5 us
  other arithmetic: 2.8 us -> 0 us
  blocking collectives: 40.6 us -> 38.1 us
    ppermute x0 -> x1, starting transfers between devices: none -> 8.75 us  [local(): other = lax.ppermute(send, 'fs', [(i, i ^ 1) for i in range(fs)])]
    all_to_all x2, starting transfers between devices: 23.9 us -> 16.4 us  [the longest x1 11.7 us: local(): got = lax.all_to_all(packed, 'fs', 0, 0, tiled=True)]
    all_to_all x1, starting transfers between devices: 8.69 us -> 13 us  [local(): back = near(lax.all_to_all(result, 'fs', 0, 0, tiled=True))]
    pallas_call x7 -> x9, Pallas kernels: 5.07 us -> 8.39 us  [call(): pl.pallas_call(kernel, out_shape=outs, in_specs=in_specs, out_specs=tuple...]
    all_to_all x1, blocking collectives: 16.6 us -> 14.4 us  [local(): payload = near(lax.all_to_all(payload, 'tp', 0, 0, tiled=True))]
    convert_element_type x2 -> x0, other arithmetic: 1.54 us -> none  [local(): weights = jnp.concatenate([p.astype(BF) for p in parts], axis=1)]
  transfers between devices with their start and end apart: 3 -> 4, of which waited for: 3 -> 3; matrix products, arithmetic and copies ran while one was open for 2% -> 0% of each run, Pallas kernels for 2% -> 4%
where the time goes in v7:
time: 137 us; the launch traced here: 136 us
  waiting for transfers between devices  48.1 us (35%)
  starting transfers between devices  38.1 us (28%)
  blocking collectives  38.1 us (28%)
  Pallas kernels  10.5 us (8%)
    all_to_all x1, waiting for transfers between devices, local(): got = lax.all_to_all(packed, 'fs', 0, 0, tiled=True)  16.6 us
    all_to_all x1, waiting for transfers between devices, local(): back = near(lax.all_to_all(result, 'fs', 0, 0, tiled=True))  16.3 us
    all_to_all x1, waiting for transfers between devices, local(): lax.all_to_all(joined, 'fs', 0, 0, tiled=True, axis_index_groups=same_core)  15.3 us
    all_to_all x1, blocking collectives, local(): payload = near(lax.all_to_all(payload, 'tp', 0, 0, tiled=True))  14.4 us
    all_to_all x1, starting transfers between devices, local(): back = near(lax.all_to_all(result, 'fs', 0, 0, tiled=True))  13 us
    all_gather x1, blocking collectives, local(): low = lax.all_gather(low, 'tp', axis=0, tiled=False)  12.3 us
    all_to_all x1, starting transfers between devices, local(): got = lax.all_to_all(packed, 'fs', 0, 0, tiled=True)  11.7 us
    all_gather x1, blocking collectives, local(): high = lax.all_gather(high, 'tp', axis=0, tiled=False)  11.4 us
  transfers between devices with their start and end apart: 4, of which 3 were waited for; matrix products, arithmetic and copies ran while one was open for 0% of the time, Pallas kernels for 4%

profile of v7, /device:TPU:1, one launch (start us, length us, event | category | flops | bytes accessed | tf_op | source)
XLA Modules:
  0.0 136.4 jit_solution(2972555166215582342)
XLA Ops:
  0.6 0.7 broadcast_in_dim.4.gain_ref
  1.4 2.1 %shard_map.102 = (bf16[64,48,128]{2,1,0:T(8,128)(2,1)S(1)}, bf16[64,48,128]{2,1,0:T(8,128)(2,1)S(1)}) custom-call(s32[1]{0:T(128)} %bitcast.core_ref, f32[64,2,16,128]{3,2,1,0:T(8,128)} %bitcast.23, f32[64,2,16,128]{3,2,1,0:T(8,128)} %bitcast.24, f32[64,2,16,128]{3,2,1,0:T(8,128)} %bitcast.25, f32[16,128]{1,0:T(8,128)S(1)} %broadcast_in_dim.4.gain_ref), custom_call_target="tpu_custom_call" | custom-call | tf_op jit(solution)/shard_map/pallas_call | solution.py:173
  3.4 8.7 %collective-permute-start = (bf16[64,48,128]{2,1,0:T(8,128)(2,1)S(1)}, bf16[64,48,128]{2,1,0:T(8,128)(2,1)S(1)}, u32[]{:S(2)}, u32[]{:S(2)}) collective-permute-start(bf16[64,48,128]{2,1,0:T(8,128)(2,1)S(1)} %get-tuple-element.14), channel_id=1, source_target_pairs={{0,4},{4,0},{8,12},{12,8},{16,20},{20,16},{24,28},{28,24},{32,36},... | collective-permute-start | bytes 2359304 | tf_op jit(solution)/shard_map/ppermute | solution.py:220
  12.2 2.1 %pack.1 = bf16[128,4,384]{2,1,0:T(4,128)(2,1)} custom-call(s32[2,128]{1,0:T(2,128)} %bitcast.20, bf16[128,512]{1,0:T(8,128)(2,1)} %tokens_ref.1), custom_call_target="tpu_custom_call" | custom-call | tf_op jit(solution)/shard_map/pack/pallas_call | solution.py:192
  14.3 11.7 %all-to-all-start.1 = ((bf16[128,4,384]{2,1,0:T(4,128)(2,1)}), bf16[128,4,384]{2,1,0:T(4,128)(2,1)S(1)}, u32[]{:S(2)}, u32[]{:S(2)}) async-start(bf16[128,4,384]{2,1,0:T(4,128)(2,1)} %pack.1), calls=%async_computation.1 | async-start | bytes 786432 | tf_op jit(solution)/shard_map/all_to_all | solution.py:201
  26.0 0.0 collective-permute-done.other_ref
  26.0 1.3 shard_map.103
  27.3 16.6 %all-to-all-done.1.got_ref = bf16[128,4,384]{2,1,0:T(4,128)(2,1)S(1)} async-done(((bf16[128,4,384]{2,1,0:T(4,128)(2,1)}), bf16[128,4,384]{2,1,0:T(4,128)(2,1)S(1)}, u32[]{:S(2)}, u32[]{:S(2)}) %all-to-all-start.1) | async-done | bytes 393248 | tf_op jit(solution)/shard_map/all_to_all | solution.py:201
  43.8 4.7 %all-to-all-start = ((bf16[64,2,48,128]{3,2,1,0:T(8,128)(2,1)}), bf16[64,2,48,128]{3,2,1,0:T(8,128)(2,1)S(1)}, u32[]{:S(2)}, u32[]{:S(2)}) async-start(bf16[64,2,48,128]{3,2,1,0:T(8,128)(2,1)} %shard_map.103), calls=%async_computation | async-start | bytes 3145728 | tf_op jit(solution)/shard_map/all_to_all | solution.py:225
  48.5 0.2 shard_map.106
  48.7 12.3 %all-gather = bf16[768,512]{1,0:T(8,128)(2,1)S(1)} all-gather(bf16[192,512]{1,0:T(8,128)(2,1)S(1)} %get-tuple-element.18), channel_id=2, replica_groups=mesh['fs'=128,'tp'=4] {'tp'}, dimensions={0}, use_global_device_ids=true | all-gather | bytes 983040 | tf_op jit(solution)/shard_map/all_gather | solution.py:230
  61.0 11.4 %all-gather.1 = bf16[768,512]{1,0:T(8,128)(2,1)S(1)} all-gather(bf16[192,512]{1,0:T(8,128)(2,1)S(1)} %get-tuple-element.21), channel_id=3, replica_groups=mesh['fs'=128,'tp'=4] {'tp'}, dimensions={0}, use_global_device_ids=true | all-gather | bytes 983040 | tf_op jit(solution)/shard_map/all_gather | solution.py:232
  72.4 0.4 shard_map.107.scale_ref
  72.8 15.3 %all-to-all-done = bf16[64,2,48,128]{3,2,1,0:T(8,128)(2,1)S(1)} async-done(((bf16[64,2,48,128]{3,2,1,0:T(8,128)(2,1)}), bf16[64,2,48,128]{3,2,1,0:T(8,128)(2,1)S(1)}, u32[]{:S(2)}, u32[]{:S(2)}) %all-to-all-start) | async-done | bytes 1572896 | tf_op jit(solution)/shard_map/all_to_all | solution.py:225
  88.1 0.6 shard_map.108
  88.7 0.0 copy-start
  88.7 0.0 copy-start.1
  88.7 14.4 %all_to_all.20.got_ref = bf16[4,896,128]{2,1,0:T(8,128)(2,1)S(1)} all-to-all(bf16[4,896,128]{2,1,0:T(8,128)(2,1)S(1)} %shard_map.108), channel_id=1, replica_groups=mesh['fs'=128,'tp'=4] {'tp'}, dimensions={0} | all-to-all | bytes 1835008 | tf_op jit(solution)/shard_map/all_to_all | solution.py:238
  103.2 1.2 shard_map.109
  104.4 13.0 %all-to-all-start.3 = ((bf16[128,4,384]{2,1,0:T(4,128)(2,1)}), bf16[128,4,384]{2,1,0:T(4,128)(2,1)S(1)}, u32[]{:S(2)}, u32[]{:S(2)}) async-start(bf16[128,4,384]{2,1,0:T(4,128)(2,1)} %shard_map.109), calls=%async_computation.3 | async-start | bytes 786432 | tf_op jit(solution)/shard_map/all_to_all | solution.py:240
  117.4 0.0 copy-done
  117.4 0.0 copy-done.1
  117.5 0.3 shard_map.105.share_ref
  117.7 1.3 shard_map.104
  119.0 16.3 %all-to-all-done.3.back_ref = bf16[128,4,384]{2,1,0:T(4,128)(2,1)S(1)} async-done(((bf16[128,4,384]{2,1,0:T(4,128)(2,1)}), bf16[128,4,384]{2,1,0:T(4,128)(2,1)S(1)}, u32[]{:S(2)}, u32[]{:S(2)}) %all-to-all-start.3) | async-done | bytes 393248 | tf_op jit(solution)/shard_map/all_to_all | solution.py:240
  135.3 1.1 shard_map.110
Async XLA Ops:
  3.4 22.6 %collective-permute-start = (bf16[64,48,128]{2,1,0:T(8,128)(2,1)S(1)}, bf16[64,48,128]{2,1,0:T(8,128)(2,1)S(1)}, u32[]{:S(2)}, u32[]{:S(2)}) collective-permute-start(bf16[64,48,128]{2,1,0:T(8,128)(2,1)S(1)} %get-tuple-element.14), channel_id=1, source_target_pairs={{0,4},{4,0},{8,12},{12,8},{16,20},{20,16},{24,28},{28,24},{32,36},... | collective-permute-start | bytes 2359304 | tf_op jit(solution)/shard_map/ppermute | solution.py:220
  14.3 29.6 %all-to-all-start.1 = ((bf16[128,4,384]{2,1,0:T(4,128)(2,1)}), bf16[128,4,384]{2,1,0:T(4,128)(2,1)S(1)}, u32[]{:S(2)}, u32[]{:S(2)}) async-start(bf16[128,4,384]{2,1,0:T(4,128)(2,1)} %pack.1), calls=%async_computation.1 | async-start | bytes 786432 | tf_op jit(solution)/shard_map/all_to_all | solution.py:201
  43.8 44.2 %all-to-all-start = ((bf16[64,2,48,128]{3,2,1,0:T(8,128)(2,1)}), bf16[64,2,48,128]{3,2,1,0:T(8,128)(2,1)S(1)}, u32[]{:S(2)}, u32[]{:S(2)}) async-start(bf16[64,2,48,128]{3,2,1,0:T(8,128)(2,1)} %shard_map.103), calls=%async_computation | async-start | bytes 3145728 | tf_op jit(solution)/shard_map/all_to_all | solution.py:225
  88.7 28.7 %copy-start = (s32[128,2]{0,1:T(2,128)S(1)}, s32[128,2]{0,1:T(2,128)}, u32[]{:S(2)}) copy-start(s32[128,2]{0,1:T(2,128)} %param.8) | copy-start | bytes 3076
  88.7 28.7 %copy-start.1 = (f32[128,2]{0,1:T(2,128)S(1)}, f32[128,2]{0,1:T(2,128)}, u32[]{:S(2)}) copy-start(f32[128,2]{0,1:T(2,128)} %param.9) | copy-start | bytes 3076
  104.4 30.9 %all-to-all-start.3 = ((bf16[128,4,384]{2,1,0:T(4,128)(2,1)}), bf16[128,4,384]{2,1,0:T(4,128)(2,1)S(1)}, u32[]{:S(2)}, u32[]{:S(2)}) async-start(bf16[128,4,384]{2,1,0:T(4,128)(2,1)} %shard_map.109), calls=%async_computation.3 | async-start | bytes 786432 | tf_op jit(solution)/shard_map/all_to_all | solution.py:240

commit v8 on v7

--- a/solution.py
+++ b/solution.py
@@ -129,8 +129,10 @@
             out_ref[k, h * half : (h + 1) * half, :] = hidden
 
 
-def expert_kernel(got_ref, out_ref):
-    sources = out_ref.shape[0]
+def expert_kernel(core_ref, got_ref, keep_ref, send_ref):
+    chips = keep_ref.shape[0]
+    sources = 2 * chips
+    first = core_ref[0] == 0
     total = SLOTS * sources
     result = lax.dot_general(
         jnp.concatenate([got_ref[k, :total, :] for k in range(4)], axis=1),
@@ -139,8 +141,10 @@
         preferred_element_type=F32,
     )
     for s in range(SLOTS):
-        rows = result[s * sources : (s + 1) * sources, :]
-        out_ref[:, :, s * 128 : (s + 1) * 128] = rows.reshape(sources, 4, 128).astype(BF)
+        rows = result[s * sources : (s + 1) * sources, :].reshape(chips, 2, 4, 128)
+        columns = slice(s * 128, (s + 1) * 128)
+        keep_ref[:, :, columns] = jnp.where(first, rows[:, 0], rows[:, 1]).astype(BF)
+        send_ref[:, :, columns] = jnp.where(first, rows[:, 1], rows[:, 0]).astype(BF)
 
 
 def share_kernel(routes_ref, weight_ref, out_ref):
@@ -236,8 +240,14 @@
         hidden_kernel, plain((4, rows + 512, 128), BF), vmem(4), (low, high, scale, weights)
     )
     payload = near(lax.all_to_all(payload, "tp", 0, 0, tiled=True))
-    result = call(expert_kernel, plain((fs, 4, SLOTS * 128), BF), vmem(1), (payload,))
-    back = near(lax.all_to_all(result, "fs", 0, 0, tiled=True))
+    piece = pltpu.VMEM((chips, 4, SLOTS * 128), BF)
+    keep, send = call(expert_kernel, (piece, piece), scalar + vmem(1), (core, payload))
+    other = near(lax.ppermute(send, "fs", [(i, i ^ 1) for i in range(fs)]))
+    joined = call(
+        join_kernel, plain((chips, 2, 4, SLOTS * 128), BF), scalar + vmem(2), (core, keep, other)
+    )
+    back = lax.all_to_all(joined, "fs", 0, 0, tiled=True, axis_index_groups=same_core)
+    back = near(back.reshape(fs, 4, SLOTS * 128))
 
     shares = call(share_kernel, pltpu.VMEM((2 * count, rows), BF), vmem(2), (routes, route_weight))
     mixed = call(mix_kernel, plain((count, 512), BF), vmem(2), (shares, back))

time: 137 us -> 138 us (level)
  waiting for transfers between devices: 48.1 us -> 46.6 us
    all_to_all x1 -> x0, waiting for transfers between devices: 16.3 us -> none  [local(): back = near(lax.all_to_all(result, 'fs', 0, 0, tiled=True))]
    all_to_all x1 -> x2, waiting for transfers between devices: 15.3 us -> 29 us  [local(): lax.all_to_all(joined, 'fs', 0, 0, tiled=True, axis_index_groups=same_core)]
    all_to_all x1 -> x0, starting transfers between devices: 13 us -> none  [local(): back = near(lax.all_to_all(result, 'fs', 0, 0, tiled=True))]
    all_to_all x1 -> x2, starting transfers between devices: 4.67 us -> 13.1 us  [local(): lax.all_to_all(joined, 'fs', 0, 0, tiled=True, axis_index_groups=same_core)]
    ppermute x0 -> x1, starting transfers between devices: none -> 5.93 us  [local(): other = near(lax.ppermute(send, 'fs', [(i, i ^ 1) for i in range(fs)]))]
    pallas_call x9 -> x10, Pallas kernels: 8.39 us -> 8.49 us  [call(): pl.pallas_call(kernel, out_shape=outs, in_specs=in_specs, out_specs=tuple...]
  transfers between devices with their start and end apart: 4 -> 5, of which waited for: 3 -> 4; matrix products, arithmetic and copies ran while one was open for 0% -> 0% of each run, Pallas kernels for 4% -> 4%
where the time goes in v8:
time: 138 us; the launch traced here: 136 us
  waiting for transfers between devices  46.6 us (34%)
  starting transfers between devices  39.4 us (29%)
  blocking collectives  38.1 us (28%)
  Pallas kernels  10.6 us (8%)
    all_to_all x2, waiting for transfers between devices, local(): lax.all_to_all(joined, 'fs', 0, 0, tiled=True, axis_index_groups=same_core)  29 us
    all_to_all x1, waiting for transfers between devices, local(): got = lax.all_to_all(packed, 'fs', 0, 0, tiled=True)  16.6 us
    all_to_all x1, blocking collectives, local(): payload = near(lax.all_to_all(payload, 'tp', 0, 0, tiled=True))  14.4 us
    all_to_all x2, starting transfers between devices, local(): lax.all_to_all(joined, 'fs', 0, 0, tiled=True, axis_index_groups=same_core)  13.1 us
    all_gather x1, blocking collectives, local(): low = lax.all_gather(low, 'tp', axis=0, tiled=False)  12.3 us
    all_to_all x1, starting transfers between devices, local(): got = lax.all_to_all(packed, 'fs', 0, 0, tiled=True)  11.7 us
    all_gather x1, blocking collectives, local(): high = lax.all_gather(high, 'tp', axis=0, tiled=False)  11.4 us
    ppermute x1, starting transfers between devices, local(): other = lax.ppermute(send, 'fs', [(i, i ^ 1) for i in range(fs)])  8.75 us
  transfers between devices with their start and end apart: 5, of which 4 were waited for; matrix products, arithmetic and copies ran while one was open for 0% of the time, Pallas kernels for 4%

profile of v8, /device:TPU:1, one launch (start us, length us, event | category | flops | bytes accessed | tf_op | source)
XLA Modules:
  0.0 136.2 jit_solution(7900172766780491395)
XLA Ops:
  0.6 0.7 broadcast_in_dim.4.gain_ref
  1.4 2.1 %shard_map.102 = (bf16[64,48,128]{2,1,0:T(8,128)(2,1)S(1)}, bf16[64,48,128]{2,1,0:T(8,128)(2,1)S(1)}) custom-call(s32[1]{0:T(128)} %bitcast.core_ref, f32[64,2,16,128]{3,2,1,0:T(8,128)} %bitcast.25, f32[64,2,16,128]{3,2,1,0:T(8,128)} %bitcast.26, f32[64,2,16,128]{3,2,1,0:T(8,128)} %bitcast.27, f32[16,128]{1,0:T(8,128)S(1)} %broadcast_in_dim.4.gain_ref), custom_call_target="tpu_custom_call" | custom-call | tf_op jit(solution)/shard_map/pallas_call | solution.py:177
  3.4 8.7 %collective-permute-start = (bf16[64,48,128]{2,1,0:T(8,128)(2,1)S(1)}, bf16[64,48,128]{2,1,0:T(8,128)(2,1)S(1)}, u32[]{:S(2)}, u32[]{:S(2)}) collective-permute-start(bf16[64,48,128]{2,1,0:T(8,128)(2,1)S(1)} %get-tuple-element.16), channel_id=1, source_target_pairs={{0,4},{4,0},{8,12},{12,8},{16,20},{20,16},{24,28},{28,24},{32,36},... | collective-permute-start | bytes 2359304 | tf_op jit(solution)/shard_map/ppermute | solution.py:224
  12.2 2.1 %pack.1 = bf16[128,4,384]{2,1,0:T(4,128)(2,1)} custom-call(s32[2,128]{1,0:T(2,128)} %bitcast.22, bf16[128,512]{1,0:T(8,128)(2,1)} %tokens_ref.1), custom_call_target="tpu_custom_call" | custom-call | tf_op jit(solution)/shard_map/pack/pallas_call | solution.py:196
  14.3 11.7 %all-to-all-start.1 = ((bf16[128,4,384]{2,1,0:T(4,128)(2,1)}), bf16[128,4,384]{2,1,0:T(4,128)(2,1)S(1)}, u32[]{:S(2)}, u32[]{:S(2)}) async-start(bf16[128,4,384]{2,1,0:T(4,128)(2,1)} %pack.1), calls=%async_computation.1 | async-start | bytes 786432 | tf_op jit(solution)/shard_map/all_to_all | solution.py:205
  26.0 0.0 collective-permute-done.other_ref
  26.0 1.3 shard_map.103
  27.3 16.6 %all-to-all-done.1.got_ref = bf16[128,4,384]{2,1,0:T(4,128)(2,1)S(1)} async-done(((bf16[128,4,384]{2,1,0:T(4,128)(2,1)}), bf16[128,4,384]{2,1,0:T(4,128)(2,1)S(1)}, u32[]{:S(2)}, u32[]{:S(2)}) %all-to-all-start.1) | async-done | bytes 393248 | tf_op jit(solution)/shard_map/all_to_all | solution.py:205
  43.8 4.7 %all-to-all-start = ((bf16[64,2,48,128]{3,2,1,0:T(8,128)(2,1)}), bf16[64,2,48,128]{3,2,1,0:T(8,128)(2,1)S(1)}, u32[]{:S(2)}, u32[]{:S(2)}) async-start(bf16[64,2,48,128]{3,2,1,0:T(8,128)(2,1)} %shard_map.103), calls=%async_computation | async-start | bytes 3145728 | tf_op jit(solution)/shard_map/all_to_all | solution.py:229
  48.5 0.2 shard_map.106
  48.7 12.3 %all-gather = bf16[768,512]{1,0:T(8,128)(2,1)S(1)} all-gather(bf16[192,512]{1,0:T(8,128)(2,1)S(1)} %get-tuple-element.20), channel_id=2, replica_groups=mesh['fs'=128,'tp'=4] {'tp'}, dimensions={0}, use_global_device_ids=true | all-gather | bytes 983040 | tf_op jit(solution)/shard_map/all_gather | solution.py:234
  61.0 11.4 %all-gather.1 = bf16[768,512]{1,0:T(8,128)(2,1)S(1)} all-gather(bf16[192,512]{1,0:T(8,128)(2,1)S(1)} %get-tuple-element.23), channel_id=3, replica_groups=mesh['fs'=128,'tp'=4] {'tp'}, dimensions={0}, use_global_device_ids=true | all-gather | bytes 983040 | tf_op jit(solution)/shard_map/all_gather | solution.py:236
  72.4 0.4 shard_map.107.scale_ref
  72.8 15.3 %all-to-all-done = bf16[64,2,48,128]{3,2,1,0:T(8,128)(2,1)S(1)} async-done(((bf16[64,2,48,128]{3,2,1,0:T(8,128)(2,1)}), bf16[64,2,48,128]{3,2,1,0:T(8,128)(2,1)S(1)}, u32[]{:S(2)}, u32[]{:S(2)}) %all-to-all-start) | async-done | bytes 1572896 | tf_op jit(solution)/shard_map/all_to_all | solution.py:229
  88.1 0.6 shard_map.108
  88.7 14.4 %all_to_all.20.got_ref = bf16[4,896,128]{2,1,0:T(8,128)(2,1)S(1)} all-to-all(bf16[4,896,128]{2,1,0:T(8,128)(2,1)S(1)} %shard_map.108), channel_id=1, replica_groups=mesh['fs'=128,'tp'=4] {'tp'}, dimensions={0} | all-to-all | bytes 1835008 | tf_op jit(solution)/shard_map/all_to_all | solution.py:242
  103.1 0.0 copy-start
  103.1 0.0 copy-start.1
  103.1 0.6 shard_map.109
  103.7 5.9 %collective-permute-start.1 = (bf16[64,4,384]{2,1,0:T(4,128)(2,1)S(1)}, bf16[64,4,384]{2,1,0:T(4,128)(2,1)S(1)}, u32[]{:S(2)}, u32[]{:S(2)}) collective-permute-start(bf16[64,4,384]{2,1,0:T(4,128)(2,1)S(1)} %get-tuple-element.25), channel_id=1, source_target_pairs={{0,4},{4,0},{8,12},{12,8},{16,20},{20,16},{24,28},{28,24},{32,36},... | collective-permute-start | bytes 589832 | tf_op jit(solution)/shard_map/ppermute | solution.py:245
  109.6 1.0 collective-permute-done.1.other_ref
  110.7 0.8 shard_map.110
  111.5 8.4 %all-to-all-start.3 = ((bf16[64,2,4,384]{3,2,1,0:T(4,128)(2,1)}), bf16[64,2,4,384]{3,2,1,0:T(4,128)(2,1)S(1)}, u32[]{:S(2)}, u32[]{:S(2)}) async-start(bf16[64,2,4,384]{3,2,1,0:T(4,128)(2,1)} %shard_map.110), calls=%async_computation.3 | async-start | bytes 786432 | tf_op jit(solution)/shard_map/all_to_all | solution.py:249
  119.9 0.0 copy-done
  119.9 0.0 copy-done.1
  119.9 0.3 shard_map.105.share_ref
  120.2 1.3 shard_map.104
  121.5 13.7 %all-to-all-done.3 = bf16[64,2,4,384]{3,2,1,0:T(4,128)(2,1)S(1)} async-done(((bf16[64,2,4,384]{3,2,1,0:T(4,128)(2,1)}), bf16[64,2,4,384]{3,2,1,0:T(4,128)(2,1)S(1)}, u32[]{:S(2)}, u32[]{:S(2)}) %all-to-all-start.3) | async-done | bytes 393248 | tf_op jit(solution)/shard_map/all_to_all | solution.py:249
  135.2 1.1 shard_map.111
Async XLA Ops:
  3.4 22.6 %collective-permute-start = (bf16[64,48,128]{2,1,0:T(8,128)(2,1)S(1)}, bf16[64,48,128]{2,1,0:T(8,128)(2,1)S(1)}, u32[]{:S(2)}, u32[]{:S(2)}) collective-permute-start(bf16[64,48,128]{2,1,0:T(8,128)(2,1)S(1)} %get-tuple-element.16), channel_id=1, source_target_pairs={{0,4},{4,0},{8,12},{12,8},{16,20},{20,16},{24,28},{28,24},{32,36},... | collective-permute-start | bytes 2359304 | tf_op jit(solution)/shard_map/ppermute | solution.py:224
  14.3 29.6 %all-to-all-start.1 = ((bf16[128,4,384]{2,1,0:T(4,128)(2,1)}), bf16[128,4,384]{2,1,0:T(4,128)(2,1)S(1)}, u32[]{:S(2)}, u32[]{:S(2)}) async-start(bf16[128,4,384]{2,1,0:T(4,128)(2,1)} %pack.1), calls=%async_computation.1 | async-start | bytes 786432 | tf_op jit(solution)/shard_map/all_to_all | solution.py:205
  43.8 44.2 %all-to-all-start = ((bf16[64,2,48,128]{3,2,1,0:T(8,128)(2,1)}), bf16[64,2,48,128]{3,2,1,0:T(8,128)(2,1)S(1)}, u32[]{:S(2)}, u32[]{:S(2)}) async-start(bf16[64,2,48,128]{3,2,1,0:T(8,128)(2,1)} %shard_map.103), calls=%async_computation | async-start | bytes 3145728 | tf_op jit(solution)/shard_map/all_to_all | solution.py:229
  103.1 16.7 %copy-start = (s32[128,2]{0,1:T(2,128)S(1)}, s32[128,2]{0,1:T(2,128)}, u32[]{:S(2)}) copy-start(s32[128,2]{0,1:T(2,128)} %param.8) | copy-start | bytes 3076
  103.1 16.7 %copy-start.1 = (f32[128,2]{0,1:T(2,128)S(1)}, f32[128,2]{0,1:T(2,128)}, u32[]{:S(2)}) copy-start(f32[128,2]{0,1:T(2,128)} %param.9) | copy-start | bytes 3076
  103.7 7.0 %collective-permute-start.1 = (bf16[64,4,384]{2,1,0:T(4,128)(2,1)S(1)}, bf16[64,4,384]{2,1,0:T(4,128)(2,1)S(1)}, u32[]{:S(2)}, u32[]{:S(2)}) collective-permute-start(bf16[64,4,384]{2,1,0:T(4,128)(2,1)S(1)} %get-tuple-element.25), channel_id=1, source_target_pairs={{0,4},{4,0},{8,12},{12,8},{16,20},{20,16},{24,28},{28,24},{32,36},... | collective-permute-start | bytes 589832 | tf_op jit(solution)/shard_map/ppermute | solution.py:245
  111.5 23.7 %all-to-all-start.3 = ((bf16[64,2,4,384]{3,2,1,0:T(4,128)(2,1)}), bf16[64,2,4,384]{3,2,1,0:T(4,128)(2,1)S(1)}, u32[]{:S(2)}, u32[]{:S(2)}) async-start(bf16[64,2,4,384]{3,2,1,0:T(4,128)(2,1)} %shard_map.110), calls=%async_computation.3 | async-start | bytes 786432 | tf_op jit(solution)/shard_map/all_to_all | solution.py:249

commit v9 on v7

--- a/solution.py
+++ b/solution.py
@@ -85,13 +85,6 @@
     high_ref[2 * sources - half :, :] = blocks[2]
 
 
-def place_kernel(weight_ref, gate_ref, up_ref, down_ref):
-    gate_ref[...] = weight_ref[:, :16, :]
-    up_ref[...] = weight_ref[:, 16:32, :]
-    block = weight_ref[:, 32:, :].reshape(weight_ref.shape[0] * 16, 128)
-    down_ref[...] = block.astype(F32).T.astype(BF)
-
-
 def scale_kernel(low_ref, high_ref, out_ref):
     half = low_ref.shape[1]
     for h, ref in enumerate((low_ref, high_ref)):
@@ -129,7 +122,13 @@
             out_ref[k, h * half : (h + 1) * half, :] = hidden
 
 
-def expert_kernel(got_ref, out_ref):
+def expert_kernel(got_ref, weight_ref, out_ref, gate_hbm, up_hbm, sems):
+    copies = [
+        pltpu.make_async_copy(weight_ref.at[:, pl.ds(16 * k, 16), :], ref, sems.at[k])
+        for k, ref in enumerate((gate_hbm, up_hbm))
+    ]
+    for copy in copies:
+        copy.start()
     sources = out_ref.shape[0]
     total = SLOTS * sources
     result = lax.dot_general(
@@ -141,6 +140,8 @@
     for s in range(SLOTS):
         rows = result[s * sources : (s + 1) * sources, :]
         out_ref[:, :, s * 128 : (s + 1) * 128] = rows.reshape(sources, 4, 128).astype(BF)
+    for copy in copies:
+        copy.wait()
 
 
 def share_kernel(routes_ref, weight_ref, out_ref):
@@ -157,7 +158,7 @@
         out_ref[count:, columns] = (part - high.astype(F32)).astype(BF)
 
 
-def mix_kernel(share_ref, back_ref, out_ref):
+def mix_kernel(share_ref, back_ref, weight_ref, out_ref, down_ref):
     experts = back_ref.shape[0]
     blocks = []
     for s in range(SLOTS):
@@ -166,6 +167,8 @@
     both = jnp.dot(share_ref[...], jnp.concatenate(blocks, axis=0), preferred_element_type=F32)
     count = out_ref.shape[0]
     out_ref[...] = (both[:count] + both[count:]).astype(BF)
+    down = weight_ref[:, 32:, :].reshape(weight_ref.shape[0] * 16, 128)
+    down_ref[...] = down.astype(F32).T.astype(BF)
 
 
 def call(kernel, outs, in_specs, args, scratch=()):
@@ -236,14 +239,27 @@
         hidden_kernel, plain((4, rows + 512, 128), BF), vmem(4), (low, high, scale, weights)
     )
     payload = near(lax.all_to_all(payload, "tp", 0, 0, tiled=True))
-    result = call(expert_kernel, plain((fs, 4, SLOTS * 128), BF), vmem(1), (payload,))
+    part = plain((fs, 16, 128), BF)
+    hbm = pl.BlockSpec(memory_space=pltpu.HBM)
+    result, gate_out, up_out = pl.pallas_call(
+        expert_kernel,
+        out_shape=(pltpu.VMEM((fs, 4, SLOTS * 128), BF), part, part),
+        in_specs=vmem(2),
+        out_specs=(vmem(1)[0], hbm, hbm),
+        scratch_shapes=[pltpu.SemaphoreType.DMA((2,))],
+        compiler_params=LIMIT,
+        name="expert",
+    )(payload, weights)
     back = near(lax.all_to_all(result, "fs", 0, 0, tiled=True))
 
-    shares = call(share_kernel, pltpu.VMEM((2 * count, rows), BF), vmem(2), (routes, route_weight))
-    mixed = call(mix_kernel, plain((count, 512), BF), vmem(2), (shares, back))
-    part = plain((fs, 16, 128), BF)
-    gate_out, up_out, down_out = call(
-        place_kernel, (part, part, plain((128, fs * 16), BF)), vmem(1), (weights,)
+    shares = call(
+        share_kernel, pltpu.VMEM((2 * count, rows), BF), vmem(2), (far(routes), far(route_weight))
+    )
+    mixed, down_out = call(
+        mix_kernel,
+        (plain((count, 512), BF), plain((128, fs * 16), BF)),
+        vmem(3),
+        (shares, back, weights),
     )
     wide = (1, fs * 16, 128)
     return (gate_out.reshape(wide), up_out.reshape(wide), down_out[None], mixed)

time: 137 us -> 138 us (level)
    pallas_call x0 -> x1, Pallas kernels: none -> 1.87 us  [local(): pl.pallas_call(expert_kernel, out_shape=(pltpu.VMEM((fs, 4, SLOTS * 128),...]
    pallas_call x9 -> x7, Pallas kernels: 8.39 us -> 6.72 us  [call(): pl.pallas_call(kernel, out_shape=outs, in_specs=in_specs, out_specs=tuple...]
where the time goes in v9:
time: 138 us; the launch traced here: 137 us
  waiting for transfers between devices  48.8 us (35%)
  starting transfers between devices  38.2 us (28%)
  blocking collectives  38.1 us (28%)
  Pallas kernels  10.7 us (8%)
    all_to_all x1, waiting for transfers between devices, local(): back = near(lax.all_to_all(result, 'fs', 0, 0, tiled=True))  16.9 us
    all_to_all x1, waiting for transfers between devices, local(): got = lax.all_to_all(packed, 'fs', 0, 0, tiled=True)  16.6 us
    all_to_all x1, waiting for transfers between devices, local(): lax.all_to_all(joined, 'fs', 0, 0, tiled=True, axis_index_groups=same_core)  15.3 us
    all_to_all x1, blocking collectives, local(): payload = near(lax.all_to_all(payload, 'tp', 0, 0, tiled=True))  14.4 us
    all_to_all x1, starting transfers between devices, local(): back = near(lax.all_to_all(result, 'fs', 0, 0, tiled=True))  13 us
    all_gather x1, blocking collectives, local(): low = lax.all_gather(low, 'tp', axis=0, tiled=False)  12.3 us
    all_to_all x1, starting transfers between devices, local(): got = lax.all_to_all(packed, 'fs', 0, 0, tiled=True)  11.7 us
    all_gather x1, blocking collectives, local(): high = lax.all_gather(high, 'tp', axis=0, tiled=False)  11.4 us
  transfers between devices with their start and end apart: 4, of which 3 were waited for; matrix products, arithmetic and copies ran while one was open for 0% of the time, Pallas kernels for 4%

profile of v9, /device:TPU:1, one launch (start us, length us, event | category | flops | bytes accessed | tf_op | source)
XLA Modules:
  0.0 137.2 jit_solution(9833718085896821607)
XLA Ops:
  0.6 0.7 broadcast_in_dim.4.gain_ref
  1.4 2.1 %shard_map.104 = (bf16[64,48,128]{2,1,0:T(8,128)(2,1)S(1)}, bf16[64,48,128]{2,1,0:T(8,128)(2,1)S(1)}) custom-call(s32[1]{0:T(128)} %bitcast.3.core_ref, f32[64,2,16,128]{3,2,1,0:T(8,128)} %bitcast.21, f32[64,2,16,128]{3,2,1,0:T(8,128)} %bitcast.22, f32[64,2,16,128]{3,2,1,0:T(8,128)} %bitcast.23, f32[16,128]{1,0:T(8,128)S(1)} %broadcast_in_dim.4.gain_ref), custom_call_target="tpu_custom_call" | custom-call | tf_op jit(solution)/shard_map/pallas_call | solution.py:176
  3.4 8.7 %collective-permute-start = (bf16[64,48,128]{2,1,0:T(8,128)(2,1)S(1)}, bf16[64,48,128]{2,1,0:T(8,128)(2,1)S(1)}, u32[]{:S(2)}, u32[]{:S(2)}) collective-permute-start(bf16[64,48,128]{2,1,0:T(8,128)(2,1)S(1)} %get-tuple-element.20), channel_id=1, source_target_pairs={{0,4},{4,0},{8,12},{12,8},{16,20},{20,16},{24,28},{28,24},{32,36},... | collective-permute-start | bytes 2359304 | tf_op jit(solution)/shard_map/ppermute | solution.py:223
  12.2 2.1 %pack.1 = bf16[128,4,384]{2,1,0:T(4,128)(2,1)} custom-call(s32[2,128]{1,0:T(2,128)} %bitcast.24, bf16[128,512]{1,0:T(8,128)(2,1)} %tokens_ref.1), custom_call_target="tpu_custom_call" | custom-call | tf_op jit(solution)/shard_map/pack/pallas_call | solution.py:195
  14.3 11.7 %all-to-all-start = ((bf16[128,4,384]{2,1,0:T(4,128)(2,1)}), bf16[128,4,384]{2,1,0:T(4,128)(2,1)S(1)}, u32[]{:S(2)}, u32[]{:S(2)}) async-start(bf16[128,4,384]{2,1,0:T(4,128)(2,1)} %pack.1), calls=%async_computation | async-start | bytes 786432 | tf_op jit(solution)/shard_map/all_to_all | solution.py:204
  26.0 0.0 collective-permute-done.other_ref
  26.0 1.3 shard_map.105
  27.3 16.6 %all-to-all-done.got_ref = bf16[128,4,384]{2,1,0:T(4,128)(2,1)S(1)} async-done(((bf16[128,4,384]{2,1,0:T(4,128)(2,1)}), bf16[128,4,384]{2,1,0:T(4,128)(2,1)S(1)}, u32[]{:S(2)}, u32[]{:S(2)}) %all-to-all-start) | async-done | bytes 393248 | tf_op jit(solution)/shard_map/all_to_all | solution.py:204
  43.8 4.7 %all-to-all-start.1 = ((bf16[64,2,48,128]{3,2,1,0:T(8,128)(2,1)}), bf16[64,2,48,128]{3,2,1,0:T(8,128)(2,1)S(1)}, u32[]{:S(2)}, u32[]{:S(2)}) async-start(bf16[64,2,48,128]{3,2,1,0:T(8,128)(2,1)} %shard_map.105), calls=%async_computation.1 | async-start | bytes 3145728 | tf_op jit(solution)/shard_map/all_to_all | solution.py:228
  48.5 0.2 shard_map.102
  48.7 12.3 %all-gather = bf16[768,512]{1,0:T(8,128)(2,1)S(1)} all-gather(bf16[192,512]{1,0:T(8,128)(2,1)S(1)} %get-tuple-element.15), channel_id=2, replica_groups=mesh['fs'=128,'tp'=4] {'tp'}, dimensions={0}, use_global_device_ids=true | all-gather | bytes 983040 | tf_op jit(solution)/shard_map/all_gather | solution.py:233
  61.0 11.4 %all-gather.1 = bf16[768,512]{1,0:T(8,128)(2,1)S(1)} all-gather(bf16[192,512]{1,0:T(8,128)(2,1)S(1)} %get-tuple-element.18), channel_id=3, replica_groups=mesh['fs'=128,'tp'=4] {'tp'}, dimensions={0}, use_global_device_ids=true | all-gather | bytes 983040 | tf_op jit(solution)/shard_map/all_gather | solution.py:235
  72.4 0.4 shard_map.103.scale_ref
  72.8 15.3 %all-to-all-done.1 = bf16[64,2,48,128]{3,2,1,0:T(8,128)(2,1)S(1)} async-done(((bf16[64,2,48,128]{3,2,1,0:T(8,128)(2,1)}), bf16[64,2,48,128]{3,2,1,0:T(8,128)(2,1)S(1)}, u32[]{:S(2)}, u32[]{:S(2)}) %all-to-all-start.1) | async-done | bytes 1572896 | tf_op jit(solution)/shard_map/all_to_all | solution.py:228
  88.1 0.6 shard_map.106
  88.7 14.4 %all_to_all.20.got_ref = bf16[4,896,128]{2,1,0:T(8,128)(2,1)S(1)} all-to-all(bf16[4,896,128]{2,1,0:T(8,128)(2,1)S(1)} %shard_map.106), channel_id=1, replica_groups=mesh['fs'=128,'tp'=4] {'tp'}, dimensions={0} | all-to-all | bytes 1835008 | tf_op jit(solution)/shard_map/all_to_all | solution.py:241
  103.1 1.9 %expert.1 = (bf16[128,4,384]{2,1,0:T(4,128)(2,1)}, bf16[128,16,128]{2,1,0:T(8,128)(2,1)}, bf16[128,16,128]{2,1,0:T(8,128)(2,1)}) custom-call(bf16[4,896,128]{2,1,0:T(8,128)(2,1)S(1)} %all_to_all.20.got_ref, bf16[128,48,128]{2,1,0:T(8,128)(2,1)S(1)} %bitcast.15), custom_call_target="tpu_custom_call" | custom-call | tf_op jit(solution)/shard_map/expert/pallas_call | solution.py:244
  105.0 13.0 %all-to-all-start.3 = ((bf16[128,4,384]{2,1,0:T(4,128)(2,1)}), bf16[128,4,384]{2,1,0:T(4,128)(2,1)S(1)}, u32[]{:S(2)}, u32[]{:S(2)}) async-start(bf16[128,4,384]{2,1,0:T(4,128)(2,1)} %get-tuple-element.23), calls=%async_computation.3 | async-start | bytes 786432 | tf_op jit(solution)/shard_map/all_to_all | solution.py:253
  118.1 1.0 shard_map.107.share_ref
  119.0 16.9 %all-to-all-done.3.back_ref = bf16[128,4,384]{2,1,0:T(4,128)(2,1)S(1)} async-done(((bf16[128,4,384]{2,1,0:T(4,128)(2,1)}), bf16[128,4,384]{2,1,0:T(4,128)(2,1)S(1)}, u32[]{:S(2)}, u32[]{:S(2)}) %all-to-all-start.3) | async-done | bytes 393248 | tf_op jit(solution)/shard_map/all_to_all | solution.py:253
  135.9 1.2 shard_map.108
Async XLA Ops:
  3.4 22.6 %collective-permute-start = (bf16[64,48,128]{2,1,0:T(8,128)(2,1)S(1)}, bf16[64,48,128]{2,1,0:T(8,128)(2,1)S(1)}, u32[]{:S(2)}, u32[]{:S(2)}) collective-permute-start(bf16[64,48,128]{2,1,0:T(8,128)(2,1)S(1)} %get-tuple-element.20), channel_id=1, source_target_pairs={{0,4},{4,0},{8,12},{12,8},{16,20},{20,16},{24,28},{28,24},{32,36},... | collective-permute-start | bytes 2359304 | tf_op jit(solution)/shard_map/ppermute | solution.py:223
  14.3 29.6 %all-to-all-start = ((bf16[128,4,384]{2,1,0:T(4,128)(2,1)}), bf16[128,4,384]{2,1,0:T(4,128)(2,1)S(1)}, u32[]{:S(2)}, u32[]{:S(2)}) async-start(bf16[128,4,384]{2,1,0:T(4,128)(2,1)} %pack.1), calls=%async_computation | async-start | bytes 786432 | tf_op jit(solution)/shard_map/all_to_all | solution.py:204
  43.8 44.2 %all-to-all-start.1 = ((bf16[64,2,48,128]{3,2,1,0:T(8,128)(2,1)}), bf16[64,2,48,128]{3,2,1,0:T(8,128)(2,1)S(1)}, u32[]{:S(2)}, u32[]{:S(2)}) async-start(bf16[64,2,48,128]{3,2,1,0:T(8,128)(2,1)} %shard_map.105), calls=%async_computation.1 | async-start | bytes 3145728 | tf_op jit(solution)/shard_map/all_to_all | solution.py:228
  105.0 30.9 %all-to-all-start.3 = ((bf16[128,4,384]{2,1,0:T(4,128)(2,1)}), bf16[128,4,384]{2,1,0:T(4,128)(2,1)S(1)}, u32[]{:S(2)}, u32[]{:S(2)}) async-start(bf16[128,4,384]{2,1,0:T(4,128)(2,1)} %get-tuple-element.23), calls=%async_computation.3 | async-start | bytes 786432 | tf_op jit(solution)/shard_map/all_to_all | solution.py:253

commit v10 on v9

--- a/solution.py
+++ b/solution.py
@@ -97,7 +97,9 @@
         out_ref[h * half : (h + 1) * half, :] = jnp.broadcast_to(scale, (half, 128))
 
 
-def hidden_kernel(low_ref, high_ref, scale_ref, weight_ref, out_ref):
+def hidden_kernel(low_ref, high_ref, scale_ref, weight_ref, out_ref, gate_hbm, sem):
+    copy = pltpu.make_async_copy(weight_ref.at[:, pl.ds(0, 16), :], gate_hbm, sem)
+    copy.start()
     half = low_ref.shape[1]
     total = 2 * half
     part = weight_ref.shape[0] // 4
@@ -120,15 +122,12 @@
         hidden = (gate / (1.0 + jnp.exp(-gate)) * up).astype(BF)
         for k in range(4):
             out_ref[k, h * half : (h + 1) * half, :] = hidden
-
-
-def expert_kernel(got_ref, weight_ref, out_ref, gate_hbm, up_hbm, sems):
-    copies = [
-        pltpu.make_async_copy(weight_ref.at[:, pl.ds(16 * k, 16), :], ref, sems.at[k])
-        for k, ref in enumerate((gate_hbm, up_hbm))
-    ]
-    for copy in copies:
-        copy.start()
+    copy.wait()
+
+
+def expert_kernel(got_ref, weight_ref, out_ref, up_hbm, sem):
+    copy = pltpu.make_async_copy(weight_ref.at[:, pl.ds(16, 16), :], up_hbm, sem)
+    copy.start()
     sources = out_ref.shape[0]
     total = SLOTS * sources
     result = lax.dot_general(
@@ -140,8 +139,7 @@
     for s in range(SLOTS):
         rows = result[s * sources : (s + 1) * sources, :]
         out_ref[:, :, s * 128 : (s + 1) * 128] = rows.reshape(sources, 4, 128).astype(BF)
-    for copy in copies:
-        copy.wait()
+    copy.wait()
 
 
 def share_kernel(routes_ref, weight_ref, out_ref):
@@ -158,7 +156,11 @@
         out_ref[count:, columns] = (part - high.astype(F32)).astype(BF)
 
 
-def mix_kernel(share_ref, back_ref, weight_ref, out_ref, down_ref):
+def mix_kernel(share_ref, back_ref, weight_ref, out_ref, down_hbm, down_ref, sem):
+    down = weight_ref[:, 32:, :].reshape(weight_ref.shape[0] * 16, 128)
+    down_ref[...] = down.astype(F32).T.astype(BF)
+    copy = pltpu.make_async_copy(down_ref, down_hbm, sem)
+    copy.start()
     experts = back_ref.shape[0]
     blocks = []
     for s in range(SLOTS):
@@ -167,8 +169,7 @@
     both = jnp.dot(share_ref[...], jnp.concatenate(blocks, axis=0), preferred_element_type=F32)
     count = out_ref.shape[0]
     out_ref[...] = (both[:count] + both[count:]).astype(BF)
-    down = weight_ref[:, 32:, :].reshape(weight_ref.shape[0] * 16, 128)
-    down_ref[...] = down.astype(F32).T.astype(BF)
+    copy.wait()
 
 
 def call(kernel, outs, in_specs, args, scratch=()):
@@ -235,18 +236,24 @@
     high = lax.all_gather(high, "tp", axis=0, tiled=False)
     low, high = near(low), near(high)
     scale = call(scale_kernel, pltpu.VMEM((rows, 128), F32), vmem(2), (low, high))
-    payload = call(
-        hidden_kernel, plain((4, rows + 512, 128), BF), vmem(4), (low, high, scale, weights)
-    )
-    payload = near(lax.all_to_all(payload, "tp", 0, 0, tiled=True))
     part = plain((fs, 16, 128), BF)
     hbm = pl.BlockSpec(memory_space=pltpu.HBM)
-    result, gate_out, up_out = pl.pallas_call(
+    payload, gate_out = pl.pallas_call(
+        hidden_kernel,
+        out_shape=(plain((4, rows + 512, 128), BF), part),
+        in_specs=vmem(4),
+        out_specs=(vmem(1)[0], hbm),
+        scratch_shapes=[pltpu.SemaphoreType.DMA],
+        compiler_params=LIMIT,
+        name="hidden",
+    )(low, high, scale, weights)
+    payload = near(lax.all_to_all(payload, "tp", 0, 0, tiled=True))
+    result, up_out = pl.pallas_call(
         expert_kernel,
-        out_shape=(pltpu.VMEM((fs, 4, SLOTS * 128), BF), part, part),
+        out_shape=(pltpu.VMEM((fs, 4, SLOTS * 128), BF), part),
         in_specs=vmem(2),
-        out_specs=(vmem(1)[0], hbm, hbm),
-        scratch_shapes=[pltpu.SemaphoreType.DMA((2,))],
+        out_specs=(vmem(1)[0], hbm),
+        scratch_shapes=[pltpu.SemaphoreType.DMA],
         compiler_params=LIMIT,
         name="expert",
     )(payload, weights)
@@ -255,12 +262,15 @@
     shares = call(
         share_kernel, pltpu.VMEM((2 * count, rows), BF), vmem(2), (far(routes), far(route_weight))
     )
-    mixed, down_out = call(
+    mixed, down_out = pl.pallas_call(
         mix_kernel,
-        (plain((count, 512), BF), plain((128, fs * 16), BF)),
-        vmem(3),
-        (shares, back, weights),
-    )
+        out_shape=(plain((count, 512), BF), plain((128, fs * 16), BF)),
+        in_specs=vmem(3),
+        out_specs=(vmem(1)[0], hbm),
+        scratch_shapes=[pltpu.VMEM((128, fs * 16), BF), pltpu.SemaphoreType.DMA],
+        compiler_params=LIMIT,
+        name="mix",
+    )(shares, back, weights)
     wide = (1, fs * 16, 128)
     return (gate_out.reshape(wide), up_out.reshape(wide), down_out[None], mixed)
 

time: 138 us -> 138 us (level)
    pallas_call x0 -> x2, Pallas kernels: none -> 2.69 us  [the longest x1 1.87 us: local(): pl.pallas_call(mix_kernel, out_shape=(plain((count, 512), BF), plain((128...]
    pallas_call x7 -> x5, Pallas kernels: 6.72 us -> 4.87 us  [call(): pl.pallas_call(kernel, out_shape=outs, in_specs=in_specs, out_specs=tuple...]
where the time goes in v10:
time: 138 us
  waiting for transfers between devices  48.8 us (35%)
  starting transfers between devices  38.2 us (28%)
  blocking collectives  38.1 us (28%)
  Pallas kernels  11.3 us (8%)
    all_to_all x1, waiting for transfers between devices, local(): back = near(lax.all_to_all(result, 'fs', 0, 0, tiled=True))  16.9 us
    all_to_all x1, waiting for transfers between devices, local(): got = lax.all_to_all(packed, 'fs', 0, 0, tiled=True)  16.6 us
    all_to_all x1, waiting for transfers between devices, local(): lax.all_to_all(joined, 'fs', 0, 0, tiled=True, axis_index_groups=same_core)  15.3 us
    all_to_all x1, blocking collectives, local(): payload = near(lax.all_to_all(payload, 'tp', 0, 0, tiled=True))  14.4 us
    all_to_all x1, starting transfers between devices, local(): back = near(lax.all_to_all(result, 'fs', 0, 0, tiled=True))  13 us
    all_gather x1, blocking collectives, local(): low = lax.all_gather(low, 'tp', axis=0, tiled=False)  12.3 us
    all_to_all x1, starting transfers between devices, local(): got = lax.all_to_all(packed, 'fs', 0, 0, tiled=True)  11.7 us
    all_gather x1, blocking collectives, local(): high = lax.all_gather(high, 'tp', axis=0, tiled=False)  11.4 us
  transfers between devices with their start and end apart: 4, of which 3 were waited for; matrix products, arithmetic and copies ran while one was open for 0% of the time, Pallas kernels for 4%

profile of v10, /device:TPU:1, one launch (start us, length us, event | category | flops | bytes accessed | tf_op | source)
XLA Modules:
  0.0 137.8 jit_solution(683580024623139401)
XLA Ops:
  0.6 0.7 broadcast_in_dim.4.gain_ref
  1.4 2.1 %shard_map.104 = (bf16[64,48,128]{2,1,0:T(8,128)(2,1)S(1)}, bf16[64,48,128]{2,1,0:T(8,128)(2,1)S(1)}) custom-call(s32[1]{0:T(128)} %bitcast.3.core_ref, f32[64,2,16,128]{3,2,1,0:T(8,128)} %bitcast.21, f32[64,2,16,128]{3,2,1,0:T(8,128)} %bitcast.22, f32[64,2,16,128]{3,2,1,0:T(8,128)} %bitcast.23, f32[16,128]{1,0:T(8,128)S(1)} %broadcast_in_dim.4.gain_ref), custom_call_target="tpu_custom_call" | custom-call | tf_op jit(solution)/shard_map/pallas_call | solution.py:177
  3.4 8.7 %collective-permute-start = (bf16[64,48,128]{2,1,0:T(8,128)(2,1)S(1)}, bf16[64,48,128]{2,1,0:T(8,128)(2,1)S(1)}, u32[]{:S(2)}, u32[]{:S(2)}) collective-permute-start(bf16[64,48,128]{2,1,0:T(8,128)(2,1)S(1)} %get-tuple-element.21), channel_id=1, source_target_pairs={{0,4},{4,0},{8,12},{12,8},{16,20},{20,16},{24,28},{28,24},{32,36},... | collective-permute-start | bytes 2359304 | tf_op jit(solution)/shard_map/ppermute | solution.py:224
  12.2 2.1 %pack.1 = bf16[128,4,384]{2,1,0:T(4,128)(2,1)} custom-call(s32[2,128]{1,0:T(2,128)} %bitcast.24, bf16[128,512]{1,0:T(8,128)(2,1)} %tokens_ref.1), custom_call_target="tpu_custom_call" | custom-call | tf_op jit(solution)/shard_map/pack/pallas_call | solution.py:196
  14.3 11.7 %all-to-all-start = ((bf16[128,4,384]{2,1,0:T(4,128)(2,1)}), bf16[128,4,384]{2,1,0:T(4,128)(2,1)S(1)}, u32[]{:S(2)}, u32[]{:S(2)}) async-start(bf16[128,4,384]{2,1,0:T(4,128)(2,1)} %pack.1), calls=%async_computation | async-start | bytes 786432 | tf_op jit(solution)/shard_map/all_to_all | solution.py:205
  26.0 0.0 collective-permute-done.other_ref
  26.0 1.3 shard_map.105
  27.3 16.6 %all-to-all-done.got_ref = bf16[128,4,384]{2,1,0:T(4,128)(2,1)S(1)} async-done(((bf16[128,4,384]{2,1,0:T(4,128)(2,1)}), bf16[128,4,384]{2,1,0:T(4,128)(2,1)S(1)}, u32[]{:S(2)}, u32[]{:S(2)}) %all-to-all-start) | async-done | bytes 393248 | tf_op jit(solution)/shard_map/all_to_all | solution.py:205
  43.8 4.7 %all-to-all-start.1 = ((bf16[64,2,48,128]{3,2,1,0:T(8,128)(2,1)}), bf16[64,2,48,128]{3,2,1,0:T(8,128)(2,1)S(1)}, u32[]{:S(2)}, u32[]{:S(2)}) async-start(bf16[64,2,48,128]{3,2,1,0:T(8,128)(2,1)} %shard_map.105), calls=%async_computation.1 | async-start | bytes 3145728 | tf_op jit(solution)/shard_map/all_to_all | solution.py:229
  48.5 0.2 shard_map.102
  48.7 12.3 %all-gather = bf16[768,512]{1,0:T(8,128)(2,1)S(1)} all-gather(bf16[192,512]{1,0:T(8,128)(2,1)S(1)} %get-tuple-element.16), channel_id=2, replica_groups=mesh['fs'=128,'tp'=4] {'tp'}, dimensions={0}, use_global_device_ids=true | all-gather | bytes 983040 | tf_op jit(solution)/shard_map/all_gather | solution.py:234
  61.0 11.4 %all-gather.1 = bf16[768,512]{1,0:T(8,128)(2,1)S(1)} all-gather(bf16[192,512]{1,0:T(8,128)(2,1)S(1)} %get-tuple-element.19), channel_id=3, replica_groups=mesh['fs'=128,'tp'=4] {'tp'}, dimensions={0}, use_global_device_ids=true | all-gather | bytes 983040 | tf_op jit(solution)/shard_map/all_gather | solution.py:236
  72.4 0.4 shard_map.103.scale_ref
  72.8 15.3 %all-to-all-done.1 = bf16[64,2,48,128]{3,2,1,0:T(8,128)(2,1)S(1)} async-done(((bf16[64,2,48,128]{3,2,1,0:T(8,128)(2,1)}), bf16[64,2,48,128]{3,2,1,0:T(8,128)(2,1)S(1)}, u32[]{:S(2)}, u32[]{:S(2)}) %all-to-all-start.1) | async-done | bytes 1572896 | tf_op jit(solution)/shard_map/all_to_all | solution.py:229
  88.1 0.8 hidden.1
  88.9 14.4 %all_to_all.20.got_ref = bf16[4,896,128]{2,1,0:T(8,128)(2,1)S(1)} all-to-all(bf16[4,896,128]{2,1,0:T(8,128)(2,1)S(1)} %get-tuple-element.23), channel_id=1, replica_groups=mesh['fs'=128,'tp'=4] {'tp'}, dimensions={0} | all-to-all | bytes 1835008 | tf_op jit(solution)/shard_map/all_to_all | solution.py:250
  103.3 1.7 %expert.1 = (bf16[128,4,384]{2,1,0:T(4,128)(2,1)}, bf16[128,16,128]{2,1,0:T(8,128)(2,1)}) custom-call(bf16[4,896,128]{2,1,0:T(8,128)(2,1)S(1)} %all_to_all.20.got_ref, bf16[128,48,128]{2,1,0:T(8,128)(2,1)S(1)} %bitcast.15), custom_call_target="tpu_custom_call" | custom-call | tf_op jit(solution)/shard_map/expert/pallas_call | solution.py:251
  105.0 13.0 %all-to-all-start.3 = ((bf16[128,4,384]{2,1,0:T(4,128)(2,1)}), bf16[128,4,384]{2,1,0:T(4,128)(2,1)S(1)}, u32[]{:S(2)}, u32[]{:S(2)}) async-start(bf16[128,4,384]{2,1,0:T(4,128)(2,1)} %get-tuple-element.25), calls=%async_computation.3 | async-start | bytes 786432 | tf_op jit(solution)/shard_map/all_to_all | solution.py:260
  118.1 1.0 shard_map.106.share_ref
  119.1 16.9 %all-to-all-done.3.back_ref = bf16[128,4,384]{2,1,0:T(4,128)(2,1)S(1)} async-done(((bf16[128,4,384]{2,1,0:T(4,128)(2,1)}), bf16[128,4,384]{2,1,0:T(4,128)(2,1)S(1)}, u32[]{:S(2)}, u32[]{:S(2)}) %all-to-all-start.3) | async-done | bytes 393248 | tf_op jit(solution)/shard_map/all_to_all | solution.py:260
  135.9 1.9 %mix.1 = (bf16[128,512]{1,0:T(8,128)(2,1)}, bf16[128,2048]{1,0:T(8,128)(2,1)}) custom-call(bf16[256,384]{1,0:T(8,128)(2,1)S(1)} %shard_map.106.share_ref, bf16[128,4,384]{2,1,0:T(4,128)(2,1)S(1)} %all-to-all-done.3.back_ref, bf16[128,48,128]{2,1,0:T(8,128)(2,1)S(1)} %bitcast.16), custom_call_target="tpu_custom_call" | custom-call | tf_op jit(solution)/shard_map/mix/pallas_call | solution.py:265
Async XLA Ops:
  3.4 22.6 %collective-permute-start = (bf16[64,48,128]{2,1,0:T(8,128)(2,1)S(1)}, bf16[64,48,128]{2,1,0:T(8,128)(2,1)S(1)}, u32[]{:S(2)}, u32[]{:S(2)}) collective-permute-start(bf16[64,48,128]{2,1,0:T(8,128)(2,1)S(1)} %get-tuple-element.21), channel_id=1, source_target_pairs={{0,4},{4,0},{8,12},{12,8},{16,20},{20,16},{24,28},{28,24},{32,36},... | collective-permute-start | bytes 2359304 | tf_op jit(solution)/shard_map/ppermute | solution.py:224
  14.3 29.6 %all-to-all-start = ((bf16[128,4,384]{2,1,0:T(4,128)(2,1)}), bf16[128,4,384]{2,1,0:T(4,128)(2,1)S(1)}, u32[]{:S(2)}, u32[]{:S(2)}) async-start(bf16[128,4,384]{2,1,0:T(4,128)(2,1)} %pack.1), calls=%async_computation | async-start | bytes 786432 | tf_op jit(solution)/shard_map/all_to_all | solution.py:205
  43.8 44.2 %all-to-all-start.1 = ((bf16[64,2,48,128]{3,2,1,0:T(8,128)(2,1)}), bf16[64,2,48,128]{3,2,1,0:T(8,128)(2,1)S(1)}, u32[]{:S(2)}, u32[]{:S(2)}) async-start(bf16[64,2,48,128]{3,2,1,0:T(8,128)(2,1)} %shard_map.105), calls=%async_computation.1 | async-start | bytes 3145728 | tf_op jit(solution)/shard_map/all_to_all | solution.py:229
  105.0 30.9 %all-to-all-start.3 = ((bf16[128,4,384]{2,1,0:T(4,128)(2,1)}), bf16[128,4,384]{2,1,0:T(4,128)(2,1)S(1)}, u32[]{:S(2)}, u32[]{:S(2)}) async-start(bf16[128,4,384]{2,1,0:T(4,128)(2,1)} %get-tuple-element.25), calls=%async_computation.3 | async-start | bytes 786432 | tf_op jit(solution)/shard_map/all_to_all | solution.py:260
